TPU v7x, 512 devices: a whole 4x8x8 slice. The times are simulated.
512 devices in a mesh: gr: 2 (over z_hi), fs: 32 (over z_lo, y), tp: 8 (over x, core).
Axes of the slice: x: 4, y: 8, z: 8 (z_hi: 2, z_lo: 4; z = z_hi * 4 + z_lo), core: 2. Of those that a mesh axis runs over, the one named last changes fastest.
Arguments:
- prompt: bfloat16 [20480, 2048], P(('gr', 'fs'), 'tp'), may hold values from -6 to 6
- norm_gain: float32 [2048], P(('gr', 'fs')), may hold values from 0.1 to 1.9
- gate_weight: float32 [32, 2048, 2048], P(None, ('gr', 'fs'), 'tp'), may hold values from -0.125 to 0.125
- up_weight: float32 [32, 2048, 2048], P(None, ('gr', 'fs'), 'tp'), may hold values from -0.125 to 0.125
- down_weight: float32 [32, 2048, 2048], P(None, ('gr', 'fs'), 'tp'), may hold values from -0.125 to 0.125
- routes: int32 [20480, 2], P(('gr', 'fs')), may hold values from 0 to 31, as said below
- route_weight: float32 [20480, 2], P(('gr', 'fs')), may hold values from 0.2 to 1
Outputs:
- gate_new: bfloat16 [32, 2048, 2048], P('fs', None, 'tp')
- up_new: bfloat16 [32, 2048, 2048], P('fs', None, 'tp')
- down_new: bfloat16 [32, 2048, 2048], P('fs', 'tp')
- mixed: bfloat16 [20480, 2048], P(('gr', 'fs'), 'tp')
Inputs may be any that keep to these rules, and one draw needn't show every extreme that they name: `routes`: each row names two different experts of the same group; expert e belongs to group e // 8. Among the 320 rows of one index of gr and fs no expert is named more than 30 times, and in every draw every expert of one group is named exactly 30 times by the rows of every index.
All inputs are finite; a program needn't handle non-finite values.
Results may differ from a plain program's by a relative error of at most 0.015.
Values may be sent and summed in bfloat16 or wider, within the bound.
No kernel may reach another device: no remote copies, remote signals or barrier semaphores. Data moves between devices by JAX's collectives and lax.ppermute only.
A program may use at most 64 MiB of HBM per device.

v0:
```python
import jax
import jax.numpy as jnp
from jax import lax
from jax.sharding import PartitionSpec as P

CAP = 30


def side_by_side(arrays, axis, split_dim, concat_dim, along):
    widths = [a.shape[along] for a in arrays]
    both = jnp.concatenate(arrays, axis=along)
    whole = lax.all_to_all(both, axis, split_axis=split_dim, concat_axis=concat_dim, tiled=True)
    return tuple(jnp.split(whole, [sum(widths[:k]) for k in range(1, len(widths))], axis=along))


def side_by_side_2(arrays, axis, dim, along):
    ends, at = ([], 0)
    for a in arrays[:-1]:
        at += a.shape[along]
        ends.append(at)
    both = jnp.concatenate(arrays, axis=along)
    return tuple(jnp.split(lax.all_gather(both, axis, axis=dim, tiled=True), ends, axis=along))


def copy_for_each(array, axis):
    length = lax.axis_size(axis)
    return lax.all_to_all(
        jnp.broadcast_to(array[None], (length, *array.shape)), axis, 0, 0, tiled=True
    )


def over_copies(array, axis):
    everything = copy_for_each(array, axis)
    return jnp.sum(everything, axis=0)


def body(prompt, norm_gain, gate_weight, up_weight, down_weight, routes, route_weight):
    groups_fs = lax.axis_size("fs")
    groups_tp = lax.axis_size("tp")
    gate_cast = (gate_weight * norm_gain[None, :, None]).astype(jnp.bfloat16)
    up_cast = (up_weight * norm_gain[None, :, None]).astype(jnp.bfloat16)
    down_cast = down_weight.astype(jnp.bfloat16)
    spread = side_by_side((gate_cast, up_cast, down_cast), "fs", 0, 1, 2)
    gate_new, up_new, down_rows = side_by_side_2((spread[0], spread[1], spread[2]), "gr", 1, 0)
    down_new = lax.all_to_all(down_rows, "tp", split_axis=1, concat_axis=2, tiled=True)
    values = prompt.astype(jnp.float32)
    tok_count = prompt.shape[0]
    col_width = prompt.shape[1]
    full_width = col_width * groups_tp
    squares = jnp.sum(values * values, axis=-1, keepdims=True)
    total_squares = over_copies(squares, "tp")
    normed = (values * lax.rsqrt(total_squares / full_width + 1e-06)).astype(jnp.bfloat16)
    expert_total = gate_weight.shape[0]
    per_device = expert_total // groups_fs
    slots_all = expert_total * CAP
    picks_flat = routes.reshape(-1)
    matches = (picks_flat[:, None] == jnp.arange(expert_total, dtype=jnp.int32)[None, :]).astype(
        jnp.int32
    )
    earlier = jnp.cumsum(matches, axis=0) - matches
    slot_of = jnp.sum(earlier * matches, axis=1)
    target = (picks_flat * CAP + slot_of).reshape(tok_count, 2)
    slot_ids = jnp.arange(slots_all, dtype=jnp.int32)[None, :]
    select_first = (target[:, 0:1] == slot_ids).astype(jnp.bfloat16)
    select_second = (target[:, 1:2] == slot_ids).astype(jnp.bfloat16)
    select_both = select_first + select_second
    outbound = jnp.einsum("ts,td->sd", select_both, normed, preferred_element_type=jnp.float32)
    outbound = outbound.astype(jnp.bfloat16).reshape(groups_fs, per_device, CAP, col_width)
    moved_cols = lax.all_to_all(outbound, "fs", split_axis=0, concat_axis=0, tiled=True)
    arrived_rows = lax.all_gather(moved_cols, "tp", axis=3, tiled=True)
    gate_pre = jnp.einsum(
        "sxcd,xdh->sxch", arrived_rows, gate_new, preferred_element_type=jnp.float32
    )
    up_pre = jnp.einsum("sxcd,xdh->sxch", arrived_rows, up_new, preferred_element_type=jnp.float32)
    hidden = (jax.nn.silu(gate_pre) * up_pre).astype(jnp.bfloat16)
    partial_value = jnp.einsum(
        "sxch,xhd->sxcd", hidden, down_new, preferred_element_type=jnp.float32
    )
    summed = lax.psum_scatter(
        partial_value.astype(jnp.bfloat16), "tp", scatter_dimension=3, tiled=True
    )
    returned = lax.all_to_all(summed, "fs", split_axis=0, concat_axis=0, tiled=True)
    returned_flat = returned.reshape(slots_all, returned.shape[3])
    pick_first = jnp.dot(select_first, returned_flat, preferred_element_type=jnp.float32)
    pick_second = jnp.dot(select_second, returned_flat, preferred_element_type=jnp.float32)
    mixed = route_weight[:, 0:1] * pick_first + route_weight[:, 1:2] * pick_second
    return (gate_new, up_new, down_new, mixed.astype(jnp.bfloat16))


def solution(mesh):
    return jax.shard_map(
        body,
        mesh=mesh,
        in_specs=(
            P(("gr", "fs"), "tp"),
            P(("gr", "fs")),
            P(None, ("gr", "fs"), "tp"),
            P(None, ("gr", "fs"), "tp"),
            P(None, ("gr", "fs"), "tp"),
            P(("gr", "fs"), None),
            P(("gr", "fs"), None),
        ),
        out_specs=(
            P("fs", None, "tp"),
            P("fs", None, "tp"),
            P("fs", "tp", None),
            P(("gr", "fs"), "tp"),
        ),
        check_vma=False,
    )
```

profile of v0, /device:TPU:15, one launch (start us, length us, event | category | flops | bytes accessed | tf_op | source)
XLA Modules:
  0.0 307.7 jit_solution(11874860149354385042)
XLA Ops:
  7.2 0.0 all-gather.3.cloned.1.call-start
  7.2 1.4 convert_element_type.48
  8.6 0.1 copy-done
  8.7 1.5 multiply_convert_fusion.1
  10.3 0.1 pad_maximum_fusion
  10.4 51.0 %all_to_all.45 = bf16[32,32,768]{2,1,0:T(8,128)(2,1)S(1)} all-to-all(bf16[32,32,768]{2,1,0:T(8,128)(2,1)S(1)} %pad_maximum_fusion), channel_id=1, replica_groups=mesh['gr'=2,'fs'=32,'tp'=8] {'fs'}, dimensions={0} | all-to-all | bytes 3145728 | tf_op jit(solution)/shard_map/all_to_all | solution.py:12
  61.4 0.1 fusion.55
  61.5 1.4 pad_maximum_fusion.1
  62.9 0.9 copy-done.2
  63.8 0.1 fusion.45
  63.9 0.6 broadcast_in_dim.2
  64.6 7.0 %all-to-all-start.2 = ((f32[8,320,1]{1,2,0:T(1,128)}), f32[8,320,1]{1,2,0:T(1,128)S(1)}, u32[]{:S(2)}, u32[]{:S(2)}) async-start(f32[8,320,1]{1,2,0:T(1,128)} %broadcast_in_dim.2), calls=%async_computation.2 | async-start | bytes 24576 | tf_op jit(solution)/shard_map/all_to_all | solution.py:27
  71.5 0.1 copy.66
  71.7 0.1 eq.59
  71.8 0.1 eq.55
  72.0 1.5 reduce-window.6
  73.4 0.3 slice_reduce_fusion
  73.7 0.1 fusion.51
  73.8 0.1 reduce_sum.30
  74.0 0.1 copy.69
  74.1 0.3 all-to-all-done.2
  74.5 0.7 convolution_convert_fusion
  75.2 0.1 reshape.74
  75.4 21.0 %all_to_all.46 = bf16[32,1,30,256]{3,2,1,0:T(8,128)(2,1)S(1)} all-to-all(bf16[32,1,30,256]{3,2,1,0:T(8,128)(2,1)S(1)} %bitcast.91), channel_id=1, replica_groups=mesh['gr'=2,'fs'=32,'tp'=8] {'fs'}, dimensions={0} | all-to-all | bytes 983040 | tf_op jit(solution)/shard_map/all_to_all | solution.py:69
  96.4 1.1 copy.72
  97.4 0.0 reduce-scatter.2.cloned.1.call-start
  97.5 67.4 %all-gather.3.cloned.1.call-done = bf16[3,2048,256]{2,1,0:T(8,128)(2,1)} async-done(((bf16[3,1024,256]{2,1,0:T(8,128)(2,1)}), bf16[3,2048,256]{2,1,0:T(8,128)(2,1)}) %all-gather.3.cloned.1.call-update) | async-done | bytes 3145744 | tf_op jit(solution)/shard_map/all_gather | solution.py:22
  164.9 3.4 %fusion.54 = (bf16[1,2048,256]{2,1,0:T(8,128)(2,1)S(1)}, bf16[1,2048,256]{2,1,0:T(8,128)(2,1)}, bf16[1,2048,256]{2,1,0:T(8,128)(2,1)}) fusion(bf16[3,2048,256]{2,1,0:T(8,128)(2,1)} %all-gather.3.cloned.1.call-done), kind=kLoop, calls=%fused_computation.59 | loop fusion | bytes 6291456 | tf_op jit(solution)/shard_map/split | solution.py:22
  168.3 11.6 %copy.79 = bf16[1,2048,256]{2,0,1:T(2,128)(2,1)S(1)} copy(bf16[1,2048,256]{2,1,0:T(8,128)(2,1)S(1)} %get-tuple-element.16) | data formatting | bytes 2097152 | tf_op jit(solution)/shard_map/split | solution.py:22
  179.9 0.5 broadcast.41
  180.4 10.6 %reduce.11 = bf16[2048,256]{1,0:T(8,128)(2,1)S(1)} reduce(bf16[2048,1,256]{2,1,0:T(2,128)(2,1)S(1)} %bitcast.88, bf16[]{:T(256)} %broadcast.41), dimensions={1}, to_apply=%bitcast.83.reduce_sub_computation | reduce | bytes 2097154
  191.1 0.3 reshape.88
  191.3 22.2 %all_to_all.47 = bf16[8,2,32768]{2,1,0:T(2,128)(2,1)S(1)} all-to-all(bf16[8,2,32768]{2,1,0:T(2,128)(2,1)S(1)} %reshape.88), channel_id=1, replica_groups=mesh['gr'=2,'fs'=32,'tp'=8] {'tp'}, dimensions={0} | all-to-all | bytes 2097152 | tf_op jit(solution)/shard_map/all_to_all | solution.py:45
  213.5 1.0 reshape.89
  214.6 0.2 copy.75
  214.7 0.6 copy.70
  215.3 0.5 reshape.81
  215.9 4.6 %fusion.4 = f32[32,1,30,256]{3,0,2,1:T(8,128)} fusion(bf16[32,1,30,2048]{3,0,2,1:T(8,128)(2,1)} %all-gather.5.cloned.1.call-done, bf16[1,2048,256]{2,1,0:T(8,128)(2,1)} %get-tuple-element.18), kind=kOutput, calls=%fused_computation.7 | convolution fusion | flops 1006632960 | bytes 5963776 | tf_op jit(solution)/shard_map/sxcd,xdh->sxch/dot_general | solution.py:71
  220.6 8.4 %convert_bitcast_fusion = bf16[32,1,30,2048]{3,0,2,1:T(8,128)(2,1)} fusion(bf16[256,2048,1]{1,0,2:T(8,128)(2,1)S(1)} %reshape.81, bf16[32,1,30,2048]{3,0,2,1:T(8,128)(2,1)} %all-gather.5.cloned.1.call-done, bf16[1,2048,256]{2,1,0:T(8,128)(2,1)S(1)} %copy-done.1, f32[32,1,30,256]{3,0,2,1:T(8,128)} %fusion.4), kind=kOutput, calls=%fused_computation.4 | convolution fusion | flops 2016706560 | bytes 10944512 | tf_op jit(solution)/shard_map/sxch,xhd->sxcd/dot_general | solution.py:76
  229.0 40.6 %reduce-scatter.2.cloned.1.call-done = bf16[32,1,30,256]{3,0,2,1:T(8,128)(2,1)} async-done(((bf16[32,1,30,2048]{3,0,2,1:T(8,128)(2,1)}), bf16[32,1,30,256]{3,0,2,1:T(8,128)(2,1)}) %reduce-scatter.2.cloned.1.call-update) | async-done | bytes 491536 | tf_op jit(solution)/shard_map/reduce_scatter | solution.py:79
  269.6 2.1 copy.73
  271.7 10.1 %all-to-all-start.4 = ((bf16[32,1,30,256]{3,2,1,0:T(8,128)(2,1)}), bf16[32,1,30,256]{3,2,1,0:T(8,128)(2,1)S(1)}, u32[]{:S(2)}, u32[]{:S(2)}) async-start(bf16[32,1,30,256]{3,2,1,0:T(8,128)(2,1)} %copy.73), calls=%async_computation.5 | async-start | bytes 1048576 | tf_op jit(solution)/shard_map/all_to_all | solution.py:82
  281.8 0.5 copy.65
  282.4 1.4 copy.74
  283.8 15.8 %all-to-all-done.4 = bf16[32,1,30,256]{3,2,1,0:T(8,128)(2,1)S(1)} async-done(((bf16[32,1,30,256]{3,2,1,0:T(8,128)(2,1)}), bf16[32,1,30,256]{3,2,1,0:T(8,128)(2,1)S(1)}, u32[]{:S(2)}, u32[]{:S(2)}) %all-to-all-start.4) | async-done | bytes 491552 | tf_op jit(solution)/shard_map/all_to_all | solution.py:82
  299.5 0.1 reshape.78
  299.7 0.4 fusion.23
  300.1 1.1 fusion.26
  (22 shorter events, 0.2 us)
Async XLA Ops:
  7.2 1.4 copy-start.5
  7.2 1.5 copy-start
  7.2 157.7 %all-gather.3.cloned.1.call-start = ((), (), s32[]{:S(2)}) async-start(), calls=%async_computation.6 | async-start | bytes 4718592 | tf_op jit(solution)/shard_map/all_gather | solution.py:22
  62.9 0.9 copy-start.2
  62.9 8.7 %copy-start.3 = (s32[320,2]{0,1:T(2,128)S(1)}, s32[320,2]{0,1:T(2,128)}, u32[]{:S(2)}) copy-start(s32[320,2]{0,1:T(2,128)} %param.12) | copy-start | bytes 7684
  64.6 9.9 %all-to-all-start.2 = ((f32[8,320,1]{1,2,0:T(1,128)}), f32[8,320,1]{1,2,0:T(1,128)S(1)}, u32[]{:S(2)}, u32[]{:S(2)}) async-start(f32[8,320,1]{1,2,0:T(1,128)} %broadcast_in_dim.2), calls=%async_computation.2 | async-start | bytes 24576 | tf_op jit(solution)/shard_map/all_to_all | solution.py:27
  71.5 144.4 %all-gather.5.cloned.1.call-start = ((), (), s32[]{:S(2)}) async-start(), calls=%async_computation.7 | async-start | bytes 4423680 | tf_op jit(solution)/shard_map/all_gather | solution.py:70
  97.4 172.1 %reduce-scatter.2.cloned.1.call-start = ((), (), s32[]{:S(2)}) async-start(), calls=%async_computation.8 | async-start | bytes 4423680 | tf_op jit(solution)/shard_map/reduce_scatter | solution.py:79
  215.9 4.7 %copy-start.1 = (bf16[1,2048,256]{2,1,0:T(8,128)(2,1)S(1)}, bf16[1,2048,256]{2,1,0:T(8,128)(2,1)}, u32[]{:S(2)}) copy-start(bf16[1,2048,256]{2,1,0:T(8,128)(2,1)} %get-tuple-element.17) | copy-start | bytes 3145732
  228.9 52.8 %copy-start.4 = (f32[320,2]{0,1:T(2,128)S(1)}, f32[320,2]{0,1:T(2,128)}, u32[]{:S(2)}) copy-start(f32[320,2]{0,1:T(2,128)} %param.13) | copy-start | bytes 7684
  271.7 27.9 %all-to-all-start.4 = ((bf16[32,1,30,256]{3,2,1,0:T(8,128)(2,1)}), bf16[32,1,30,256]{3,2,1,0:T(8,128)(2,1)S(1)}, u32[]{:S(2)}, u32[]{:S(2)}) async-start(bf16[32,1,30,256]{3,2,1,0:T(8,128)(2,1)} %copy.73), calls=%async_computation.5 | async-start | bytes 1048576 | tf_op jit(solution)/shard_map/all_to_all | solution.py:82
Sparse Core Ops, SparseCore 0:
  63.0 101.8 all-gather.2
  167.6 46.1 all-gather.4
  229.1 40.4 reduce-scatter.1
where the time goes:
time: 308 us
  waiting for transfers between devices  124 us (40%)
  blocking collectives  94.2 us (31%)
  local copies, waits for them, and re-layouts  26.2 us (9%)
  starting transfers between devices  17.2 us (6%)
  other arithmetic  16.8 us (5%)
  matrix products  15.1 us (5%)
  between operations  14 us (5%)
    all_gather x1, waiting for transfers between devices, side_by_side_2(): lax.all_gather(both, axis, axis=dim, tiled=True)  67.4 us
    all_to_all x1, blocking collectives, side_by_side(): lax.all_to_all(both, axis, split_axis=split_dim, concat_axis=concat_dim,...  51 us
    reduce_scatter x1, waiting for transfers between devices, body(): lax.psum_scatter(partial_value.astype(jnp.bfloat16), 'tp', scatter_dimens...  40.6 us
    all_to_all x1, blocking collectives, body(): lax.all_to_all(down_rows, 'tp', split_axis=1, concat_axis=2, tiled=True)  22.2 us
    all_to_all x1, blocking collectives, body(): lax.all_to_all(outbound, 'fs', split_axis=0, concat_axis=0, tiled=True)  21 us
    all_to_all x1, waiting for transfers between devices, body(): lax.all_to_all(summed, 'fs', split_axis=0, concat_axis=0, tiled=True)  15.8 us
    split x2, local copies, waits for them, and re-layouts, side_by_side_2(): jnp.split(lax.all_gather(both, axis, axis=dim, tiled=True), ends, axis=al...  15 us
    unnamed x1, other arithmetic  10.6 us
  transfers between devices with their start and end apart: 5, of which 4 were waited for; matrix products, arithmetic and copies ran while one was open for 12% of the time, Pallas kernels for 0%

commit v1 on v0

v1 whole, which is shorter than its diff:
```python
import functools

import jax
import jax.numpy as jnp
from jax import lax
from jax.experimental import pallas as pl
from jax.experimental.pallas import tpu as pltpu
from jax.sharding import PartitionSpec as P

SLOTS = 32
BF = jnp.bfloat16
F32 = jnp.float32


def pieces_dot(ref, weights, width):
    acc = None
    for k in range(ref.shape[0]):
        part = jnp.dot(
            ref[k], weights[k * width : (k + 1) * width, :], preferred_element_type=F32
        )
        acc = part if acc is None else acc + part
    return acc


def hidden_kernel(rows, gate_up, out):
    width = rows.shape[2]
    total = rows.shape[0] * width
    acc = pieces_dot(rows, gate_up, width)
    squares = None
    for k in range(rows.shape[0]):
        values = rows[k].astype(F32)
        part = jnp.sum(values * values, axis=-1, keepdims=True)
        squares = part if squares is None else squares + part
    acc = acc * lax.rsqrt(squares / total + 1e-06)
    half = out.shape[1]
    gate, up = acc[:, :half], acc[:, half:]
    out[...] = (gate / (1.0 + jnp.exp(-gate)) * up).astype(out.dtype)


def out_kernel(rows, down, out):
    out[...] = pieces_dot(rows, down, rows.shape[2]).astype(out.dtype)


def row_call(kernel, name, rows, weights, out_width, steps=4):
    pieces, count, width = rows.shape
    block = count // steps
    return pl.pallas_call(
        kernel,
        name=name,
        grid=(steps,),
        in_specs=[
            pl.BlockSpec((pieces, block, width), lambda i: (0, i, 0)),
            pl.BlockSpec(weights.shape, lambda i: (0, 0)),
        ],
        out_specs=pl.BlockSpec((block, out_width), lambda i: (i, 0)),
        out_shape=jax.ShapeDtypeStruct((count, out_width), BF),
    )(rows, weights)


def after(value, *others):
    return lax.optimization_barrier((value, *others))[0]


def both_groups(array):
    copies = jnp.broadcast_to(array[None], (lax.axis_size("gr"), *array.shape))
    return copies.reshape(-1, *array.shape[1:])


def body(prompt, norm_gain, gate_weight, up_weight, down_weight, routes, route_weight):
    experts, rows, cols = gate_weight.shape
    tok_count, width = prompt.shape
    slots_all = experts * SLOTS
    tp = lax.axis_size("tp")

    expert_ids = jnp.arange(experts, dtype=jnp.int32)[None, :]
    first = routes[:, 0:1] == expert_ids
    second = routes[:, 1:2] == expert_ids
    named = (first | second).astype(BF)
    order = jnp.arange(tok_count, dtype=jnp.int32)
    before = (order[None, :] < order[:, None]).astype(BF)
    earlier = jnp.dot(before, named, preferred_element_type=F32)
    slot_first = jnp.sum(jnp.where(first, earlier, 0.0), axis=1).astype(jnp.int32)
    slot_second = jnp.sum(jnp.where(second, earlier, 0.0), axis=1).astype(jnp.int32)
    target_first = routes[:, 0] * SLOTS + slot_first
    target_second = routes[:, 1] * SLOTS + slot_second
    slot_ids = jnp.arange(slots_all, dtype=jnp.int32)[None, :]
    select_first = (target_first[:, None] == slot_ids).astype(BF)
    select_second = (target_second[:, None] == slot_ids).astype(BF)
    outbound = jnp.einsum(
        "ts,td->sd", select_first + select_second, prompt, preferred_element_type=F32
    ).astype(BF)
    moved = lax.all_to_all(
        outbound.reshape(experts, SLOTS, width), "fs", split_axis=0, concat_axis=0, tiled=True
    )
    arrived = lax.all_gather(moved.reshape(1, slots_all, width), "tp", axis=0, tiled=True)

    gain = norm_gain[None, :, None]
    gate_up = jnp.concatenate(
        [(gate_weight * gain).astype(BF), (up_weight * gain).astype(BF)], axis=2
    )
    gate_up = after(both_groups(gate_up), moved)
    gate_up = lax.all_to_all(gate_up, ("gr", "fs"), split_axis=0, concat_axis=0, tiled=True)
    gate_up = gate_up.reshape(-1, 2 * cols)
    gate_new, up_new = gate_up[None, :, :cols], gate_up[None, :, cols:]

    hidden = row_call(hidden_kernel, "hidden", arrived, gate_up, cols)
    hidden_all = lax.all_gather(hidden[None], "tp", axis=0, tiled=True)

    down = after(both_groups(down_weight.astype(BF)), hidden)
    down = lax.all_to_all(down, ("gr", "fs"), split_axis=0, concat_axis=0, tiled=True)
    down = down.reshape(-1, cols)
    summed = row_call(out_kernel, "expert_out", hidden_all, down, cols)
    returned = lax.all_to_all(
        summed.reshape(experts, SLOTS, width), "fs", split_axis=0, concat_axis=0, tiled=True
    ).reshape(slots_all, width)
    down_new = lax.all_to_all(
        after(down, returned).reshape(tp, -1, cols), "tp", split_axis=0, concat_axis=2, tiled=True
    )

    pick_first = jnp.dot(select_first, returned, preferred_element_type=F32)
    pick_second = jnp.dot(select_second, returned, preferred_element_type=F32)
    mixed = route_weight[:, 0:1] * pick_first + route_weight[:, 1:2] * pick_second
    return (gate_new, up_new, down_new, mixed.astype(BF))


def solution(mesh):
    return jax.shard_map(
        body,
        mesh=mesh,
        in_specs=(
            P(("gr", "fs"), "tp"),
            P(("gr", "fs")),
            P(None, ("gr", "fs"), "tp"),
            P(None, ("gr", "fs"), "tp"),
            P(None, ("gr", "fs"), "tp"),
            P(("gr", "fs"), None),
            P(("gr", "fs"), None),
        ),
        out_specs=(
            P("fs", None, "tp"),
            P("fs", None, "tp"),
            P("fs", "tp", None),
            P(("gr", "fs"), "tp"),
        ),
        check_vma=False,
    )
```

time: 308 us -> 204 us (0.66)
  the two profiles are of different devices: /device:TPU:15 before, /device:TPU:8 now
where the time goes in v1:
time: 204 us; the launch traced here: 203 us
  blocking collectives  127 us (62%)
  waiting for transfers between devices  30.8 us (15%)
  between operations  14.2 us (7%)
  starting transfers between devices  12.1 us (6%)
  Pallas kernels  11.4 us (6%)
  local copies, waits for them, and re-layouts  4.58 us (2%)
  matrix products  2.31 us (1%)
    all_to_all x1, blocking collectives, body(): lax.all_to_all(gate_up, ('gr', 'fs'), split_axis=0, concat_axis=0, tiled=...  60.8 us
    all_to_all x1, blocking collectives, body(): lax.all_to_all(down, ('gr', 'fs'), split_axis=0, concat_axis=0, tiled=True)  35.2 us
    all_to_all x1, blocking collectives, body(): lax.all_to_all(outbound.reshape(experts, SLOTS, width), 'fs', split_axis=...  30.7 us
    all_to_all x1, waiting for transfers between devices, body(): lax.all_to_all(summed.reshape(experts, SLOTS, width), 'fs', split_axis=0,...  17.9 us
    all_to_all x1, waiting for transfers between devices, body(): lax.all_to_all(after(down, returned).reshape(tp, -1, cols), 'tp', split_a...  12.9 us
    pallas_call x2, Pallas kernels, row_call(): pl.pallas_call(kernel, name=name, grid=(steps,), in_specs=[pl.BlockSpec((...  11.4 us
    all_to_all x1, starting transfers between devices, body(): lax.all_to_all(summed.reshape(experts, SLOTS, width), 'fs', split_axis=0,...  8.43 us
  transfers between devices with their start and end apart: 4, of which 2 were waited for; matrix products, arithmetic and copies ran while one was open for 2% of the time, Pallas kernels for 0%

profile of v1, /device:TPU:8, one launch (start us, length us, event | category | flops | bytes accessed | tf_op | source)
XLA Modules:
  0.0 203.3 jit_solution(9950435943199976286)
XLA Ops:
  7.2 0.0 copy-start
  7.2 0.0 all-gather.4.cloned.1.call-start
  7.2 0.8 slice_reduce_fusion.3
  8.0 0.2 select_reduce_fusion.1
  8.2 0.8 add_reduce_fusion.1
  9.0 0.0 copy-done
  9.0 0.0 copy-start.4
  9.0 0.7 convolution_convert_fusion
  9.7 0.0 copy-start.3
  9.7 0.0 copy-start.8
  9.7 30.7 %all_to_all.38 = bf16[32,32,256]{2,1,0:T(8,128)(2,1)} all-to-all(bf16[32,32,256]{2,1,0:T(8,128)(2,1)S(1)} %bitcast.33), channel_id=1, replica_groups=mesh['gr'=2,'fs'=32,'tp'=8] {'fs'}, dimensions={0} | all-to-all | bytes 1048576 | tf_op jit(solution)/shard_map/all_to_all | solution.py:92
  40.4 0.0 all-gather.4.cloned.1.call-update
  40.4 0.0 all-gather.6.cloned.1.call-start
  40.5 0.0 copy-done.4
  40.5 0.0 copy-done.3
  40.5 0.0 copy-done.8
  40.5 0.3 multiply_convert_fusion.1
  40.8 0.1 pad_maximum_fusion
  40.9 0.3 broadcast_in_dim.15
  41.2 60.8 %all_to_all.39 = bf16[64,32,512]{2,1,0:T(8,128)(2,1)} all-to-all(bf16[64,32,512]{2,1,0:T(8,128)(2,1)S(1)} %bitcast.24), channel_id=1, replica_groups=mesh['gr'=2,'fs'=32,'tp'=8] {'gr','fs'}, dimensions={0} | all-to-all | bytes 4194304 | tf_op jit(solution)/shard_map/all_to_all | solution.py:102
  102.0 0.0 all-gather.4.cloned.1.call-done.rows
  102.0 0.0 copy-start.2
  102.0 6.3 %hidden.1 = bf16[1024,256]{1,0:T(8,128)(2,1)} custom-call(bf16[8,1024,256]{2,1,0:T(8,128)(2,1)} %all-gather.4.cloned.1.call-done.rows, bf16[2048,512]{1,0:T(8,128)(2,1)} %bitcast.22), custom_call_target="tpu_custom_call" | custom-call | tf_op jit(solution)/shard_map/hidden/pallas_call | solution.py:47
  108.3 0.0 all-gather.6.cloned.1.call-update
  108.4 0.0 copy-done.2
  108.4 0.1 convert_element_type.58
  108.5 0.1 broadcast_in_dim.19
  108.6 35.2 %all_to_all.40 = bf16[64,32,256]{2,1,0:T(8,128)(2,1)} all-to-all(bf16[64,32,256]{2,1,0:T(8,128)(2,1)S(1)} %bitcast.27), channel_id=1, replica_groups=mesh['gr'=2,'fs'=32,'tp'=8] {'gr','fs'}, dimensions={0} | all-to-all | bytes 2097152 | tf_op jit(solution)/shard_map/all_to_all | solution.py:110
  143.8 0.0 all-gather.6.cloned.1.call-done
  143.8 0.0 copy-start.7
  143.8 5.0 %expert_out.1 = bf16[1024,256]{1,0:T(8,128)(2,1)} custom-call(bf16[8,1024,256]{2,1,0:T(8,128)(2,1)} %bitcast.25, bf16[2048,256]{1,0:T(8,128)(2,1)} %bitcast.7.down), custom_call_target="tpu_custom_call" | custom-call | tf_op jit(solution)/shard_map/expert_out/pallas_call | solution.py:47
  148.8 8.4 %all-to-all-start.3 = ((bf16[32,32,256]{2,1,0:T(8,128)(2,1)}), bf16[32,32,256]{2,1,0:T(8,128)(2,1)S(1)}, u32[]{:S(2)}, u32[]{:S(2)}) async-start(bf16[32,32,256]{2,1,0:T(8,128)(2,1)} %bitcast.29), calls=%async_computation.3 | async-start | bytes 1048576 | tf_op jit(solution)/shard_map/all_to_all | solution.py:113
  157.2 0.0 copy-done.7
  157.3 0.0 copy-start.1
  157.3 17.9 %all-to-all-done.3 = bf16[32,32,256]{2,1,0:T(8,128)(2,1)S(1)} async-done(((bf16[32,32,256]{2,1,0:T(8,128)(2,1)}), bf16[32,32,256]{2,1,0:T(8,128)(2,1)S(1)}, u32[]{:S(2)}, u32[]{:S(2)}) %all-to-all-start.3) | async-done | bytes 524320 | tf_op jit(solution)/shard_map/all_to_all | solution.py:113
  175.1 0.0 copy-start.5
  175.2 0.8 copy-done.5
  175.9 3.6 %all-to-all-start.4 = ((bf16[8,256,256]{2,1,0:T(8,128)(2,1)}), bf16[8,256,256]{2,1,0:T(8,128)(2,1)S(1)}, u32[]{:S(2)}, u32[]{:S(2)}) async-start(bf16[8,256,256]{2,1,0:T(8,128)(2,1)} %bitcast.11), calls=%async_computation.4 | async-start | bytes 2097152 | tf_op jit(solution)/shard_map/all_to_all | solution.py:116
  179.5 0.0 copy-done.1
  179.5 0.0 copy-start.6
  179.5 1.5 slice_bitcast_fusion
  181.0 0.0 copy-done.6
  181.0 0.4 fusion.6
  181.4 1.1 fusion.7
  182.4 12.9 %all-to-all-done.4 = bf16[8,256,256]{2,1,0:T(8,128)(2,1)S(1)} async-done(((bf16[8,256,256]{2,1,0:T(8,128)(2,1)}), bf16[8,256,256]{2,1,0:T(8,128)(2,1)S(1)}, u32[]{:S(2)}, u32[]{:S(2)}) %all-to-all-start.4) | async-done | bytes 1048608 | tf_op jit(solution)/shard_map/all_to_all | solution.py:116
  195.4 1.1 copy.13
  (3 shorter events, 0.0 us)
Async XLA Ops:
  7.2 1.9 copy-start
  7.2 94.8 %all-gather.4.cloned.1.call-start = ((), (), s32[]{:S(2)}) async-start(), calls=%async_computation.5 | async-start | bytes 4718592 | tf_op jit(solution)/shard_map/all_gather | solution.py:95
  9.0 31.4 %copy-start.4 = (f32[32,32,256]{2,1,0:T(8,128)S(1)}, f32[32,32,256]{2,1,0:T(8,128)}, u32[]{:S(2)}) copy-start(f32[32,32,256]{2,1,0:T(8,128)} %param.10) | copy-start | bytes 3145732
  9.7 30.8 %copy-start.3 = (f32[32,32,256]{2,1,0:T(8,128)S(1)}, f32[32,32,256]{2,1,0:T(8,128)}, u32[]{:S(2)}) copy-start(f32[32,32,256]{2,1,0:T(8,128)} %param.9) | copy-start | bytes 3145732
  9.7 30.8 %copy-start.8 = (f32[32]{0:T(128)S(1)}, f32[32]{0:T(128)}, u32[]{:S(2)}) copy-start(f32[32]{0:T(128)} %param.8) | copy-start | bytes 388
  40.4 103.3 %all-gather.6.cloned.1.call-start = ((), (), s32[]{:S(2)}) async-start(), calls=%async_computation.6 | async-start | bytes 4718592 | tf_op jit(solution)/shard_map/all_gather | solution.py:107
  102.0 6.3 %copy-start.2 = (f32[32,32,256]{2,1,0:T(8,128)S(1)}, f32[32,32,256]{2,1,0:T(8,128)}, u32[]{:S(2)}) copy-start(f32[32,32,256]{2,1,0:T(8,128)} %param.11) | copy-start | bytes 3145732
  143.8 13.5 %copy-start.7 = (f32[320,2]{0,1:T(2,128)S(1)}, f32[320,2]{0,1:T(2,128)}, u32[]{:S(2)}) copy-start(f32[320,2]{0,1:T(2,128)} %param.13) | copy-start | bytes 7684
  148.8 26.3 %all-to-all-start.3 = ((bf16[32,32,256]{2,1,0:T(8,128)(2,1)}), bf16[32,32,256]{2,1,0:T(8,128)(2,1)S(1)}, u32[]{:S(2)}, u32[]{:S(2)}) async-start(bf16[32,32,256]{2,1,0:T(8,128)(2,1)} %bitcast.29), calls=%async_computation.3 | async-start | bytes 1048576 | tf_op jit(solution)/shard_map/all_to_all | solution.py:113
  157.3 22.2 %copy-start.1 = (bf16[64,32,512]{2,1,0:T(8,128)(2,1)S(1)}, bf16[64,32,512]{2,1,0:T(8,128)(2,1)}, u32[]{:S(2)}) copy-start(bf16[64,32,512]{2,1,0:T(8,128)(2,1)} %all_to_all.39) | copy-start | bytes 6291460
  175.1 0.8 copy-start.5
  175.9 19.4 %all-to-all-start.4 = ((bf16[8,256,256]{2,1,0:T(8,128)(2,1)}), bf16[8,256,256]{2,1,0:T(8,128)(2,1)S(1)}, u32[]{:S(2)}, u32[]{:S(2)}) async-start(bf16[8,256,256]{2,1,0:T(8,128)(2,1)} %bitcast.11), calls=%async_computation.4 | async-start | bytes 2097152 | tf_op jit(solution)/shard_map/all_to_all | solution.py:116
  179.5 1.5 copy-start.6
Sparse Core Ops, SparseCore 0:
  40.5 35.6 all-gather.3
  108.5 32.9 all-gather.5

commit v2 on v1

--- a/solution.py
+++ b/solution.py
@@ -1,5 +1,3 @@
-import functools
-
 import jax
 import jax.numpy as jnp
 from jax import lax
@@ -7,25 +5,21 @@
 from jax.experimental.pallas import tpu as pltpu
 from jax.sharding import PartitionSpec as P
 
+
 SLOTS = 32
 BF = jnp.bfloat16
 F32 = jnp.float32
 
 
-def pieces_dot(ref, weights, width):
-    acc = None
-    for k in range(ref.shape[0]):
-        part = jnp.dot(
-            ref[k], weights[k * width : (k + 1) * width, :], preferred_element_type=F32
-        )
-        acc = part if acc is None else acc + part
-    return acc
+def pieces_dot(ref, weights):
+    rows = jnp.concatenate([ref[k] for k in range(ref.shape[0])], axis=1)
+    return jnp.dot(rows, weights[...], preferred_element_type=F32)
 
 
 def hidden_kernel(rows, gate_up, out):
     width = rows.shape[2]
     total = rows.shape[0] * width
-    acc = pieces_dot(rows, gate_up, width)
+    acc = pieces_dot(rows, gate_up)
     squares = None
     for k in range(rows.shape[0]):
         values = rows[k].astype(F32)
@@ -38,15 +32,14 @@
 
 
 def out_kernel(rows, down, out):
-    out[...] = pieces_dot(rows, down, rows.shape[2]).astype(out.dtype)
+    out[...] = pieces_dot(rows, down).astype(out.dtype)
 
 
-def row_call(kernel, name, rows, weights, out_width, steps=4):
+def row_call(kernel, rows, weights, out_width, steps=4):
     pieces, count, width = rows.shape
     block = count // steps
     return pl.pallas_call(
         kernel,
-        name=name,
         grid=(steps,),
         in_specs=[
             pl.BlockSpec((pieces, block, width), lambda i: (0, i, 0)),
@@ -55,6 +48,37 @@
         out_specs=pl.BlockSpec((block, out_width), lambda i: (i, 0)),
         out_shape=jax.ShapeDtypeStruct((count, out_width), BF),
     )(rows, weights)
+
+
+def place_kernel(here, *refs):
+    pieces, out = refs[:-1], refs[-1]
+    for k, piece in enumerate(pieces):
+
+        @pl.when(pl.program_id(0) == k)
+        def _(piece=piece):
+            out[...] = piece[...]
+
+
+def exchange_units(array, axis):
+    count, here = lax.axis_size(axis), lax.axis_index(axis)
+    rows, cols = array.shape[0] // count, array.shape[1]
+    pieces = []
+    for k in range(count):
+        block = lax.dynamic_slice_in_dim(array, (here + k) % count * rows, rows, 0)
+        if k:
+            block = lax.ppermute(block, axis, [(i, (i + k) % count) for i in range(count)])
+        pieces.append(block)
+    return pl.pallas_call(
+        place_kernel,
+        name="place",
+        grid_spec=pltpu.PrefetchScalarGridSpec(
+            num_scalar_prefetch=1,
+            grid=(count,),
+            in_specs=[pl.BlockSpec((rows, cols), lambda k, at: (0, 0))] * count,
+            out_specs=pl.BlockSpec((rows, cols), lambda k, at: (0, (at[0] - k + count) % count)),
+        ),
+        out_shape=jax.ShapeDtypeStruct((rows, count * cols), array.dtype),
+    )(here.reshape(1).astype(jnp.int32), *pieces)
 
 
 def after(value, *others):
@@ -67,10 +91,9 @@
 
 
 def body(prompt, norm_gain, gate_weight, up_weight, down_weight, routes, route_weight):
-    experts, rows, cols = gate_weight.shape
+    experts, _, cols = gate_weight.shape
     tok_count, width = prompt.shape
     slots_all = experts * SLOTS
-    tp = lax.axis_size("tp")
 
     expert_ids = jnp.arange(experts, dtype=jnp.int32)[None, :]
     first = routes[:, 0:1] == expert_ids
@@ -103,24 +126,23 @@
     gate_up = gate_up.reshape(-1, 2 * cols)
     gate_new, up_new = gate_up[None, :, :cols], gate_up[None, :, cols:]
 
-    hidden = row_call(hidden_kernel, "hidden", arrived, gate_up, cols)
+    hidden = row_call(hidden_kernel, arrived, gate_up, cols)
     hidden_all = lax.all_gather(hidden[None], "tp", axis=0, tiled=True)
 
     down = after(both_groups(down_weight.astype(BF)), hidden)
     down = lax.all_to_all(down, ("gr", "fs"), split_axis=0, concat_axis=0, tiled=True)
     down = down.reshape(-1, cols)
-    summed = row_call(out_kernel, "expert_out", hidden_all, down, cols)
+    summed = row_call(out_kernel, hidden_all, down, cols)
     returned = lax.all_to_all(
         summed.reshape(experts, SLOTS, width), "fs", split_axis=0, concat_axis=0, tiled=True
-    ).reshape(slots_all, width)
-    down_new = lax.all_to_all(
-        after(down, returned).reshape(tp, -1, cols), "tp", split_axis=0, concat_axis=2, tiled=True
     )
+    returned = returned.reshape(slots_all, width)
+    down_new = exchange_units(down, "tp")
 
     pick_first = jnp.dot(select_first, returned, preferred_element_type=F32)
     pick_second = jnp.dot(select_second, returned, preferred_element_type=F32)
     mixed = route_weight[:, 0:1] * pick_first + route_weight[:, 1:2] * pick_second
-    return (gate_new, up_new, down_new, mixed.astype(BF))
+    return (gate_new, up_new, down_new[None], mixed.astype(BF))
 
 
 def solution(mesh):

time: 204 us -> 197 us (0.966)
  the two profiles are of different devices: /device:TPU:8 before, /device:TPU:1 now
where the time goes in v2:
time: 197 us
  blocking collectives  123 us (62%)
  starting transfers between devices  27.8 us (14%)
  Pallas kernels  15.4 us (8%)
  between operations  14.5 us (7%)
  waiting for transfers between devices  6.66 us (3%)
  matrix products  4.4 us (2%)
  local copies, waits for them, and re-layouts  4.08 us (2%)
    all_to_all x1, blocking collectives, body(): lax.all_to_all(gate_up, ('gr', 'fs'), split_axis=0, concat_axis=0, tiled=...  60 us
    all_to_all x1, blocking collectives, body(): lax.all_to_all(down, ('gr', 'fs'), split_axis=0, concat_axis=0, tiled=True)  33.9 us
    all_to_all x1, blocking collectives, body(): lax.all_to_all(outbound.reshape(experts, SLOTS, width), 'fs', split_axis=...  28.7 us
    ppermute x7, starting transfers between devices, exchange_units(): lax.ppermute(block, axis, [(i, (i + k) % count) for i in range(count)])  17.4 us
    pallas_call x2, Pallas kernels, row_call(): pl.pallas_call(kernel, grid=(steps,), in_specs=[pl.BlockSpec((pieces, blo...  11.3 us
    all_to_all x1, starting transfers between devices, body(): lax.all_to_all(summed.reshape(experts, SLOTS, width), 'fs', split_axis=0,...  10.4 us
    pallas_call x1, Pallas kernels, exchange_units(): pl.pallas_call(place_kernel, name='place', grid_spec=pltpu.PrefetchScalar...  4.09 us
  transfers between devices with their start and end apart: 10, of which 3 were waited for; matrix products, arithmetic and copies ran while one was open for 2% of the time, Pallas kernels for 2%

profile of v2, /device:TPU:1, one launch (start us, length us, event | category | flops | bytes accessed | tf_op | source)
XLA Modules:
  0.0 196.7 jit_solution(10129975630560161041)
XLA Ops:
  7.2 0.0 copy-start
  7.2 0.0 all-gather.4.cloned.1.call-start
  7.2 0.8 slice_reduce_fusion.3
  8.0 0.2 select_reduce_fusion.1
  8.2 0.8 add_reduce_fusion.1
  9.0 0.0 copy-done
  9.0 0.0 copy-start.5
  9.0 0.7 convolution_convert_fusion
  9.7 0.0 copy-start.4
  9.7 0.0 copy-start.14
  9.7 28.7 %all_to_all.20 = bf16[32,32,256]{2,1,0:T(8,128)(2,1)} all-to-all(bf16[32,32,256]{2,1,0:T(8,128)(2,1)S(1)} %bitcast.28), channel_id=1, replica_groups=mesh['gr'=2,'fs'=32,'tp'=8] {'fs'}, dimensions={0} | all-to-all | bytes 1048576 | tf_op jit(solution)/shard_map/all_to_all | solution.py:115
  38.4 0.0 all-gather.4.cloned.1.call-update
  38.5 0.0 all-gather.6.cloned.1.call-start
  38.5 0.3 multiply_convert_fusion.1
  38.9 0.1 pad_maximum_fusion
  39.0 0.3 broadcast_in_dim.17
  39.2 60.0 %all_to_all.21 = bf16[64,32,512]{2,1,0:T(8,128)(2,1)} all-to-all(bf16[64,32,512]{2,1,0:T(8,128)(2,1)S(1)} %bitcast.22), channel_id=1, replica_groups=mesh['gr'=2,'fs'=32,'tp'=8] {'gr','fs'}, dimensions={0} | all-to-all | bytes 4194304 | tf_op jit(solution)/shard_map/all_to_all | solution.py:125
  99.2 6.3 %shard_map.102 = bf16[1024,256]{1,0:T(8,128)(2,1)} custom-call(bf16[8,1024,256]{2,1,0:T(8,128)(2,1)} %all-gather.4.cloned.1.call-done.rows, bf16[2048,512]{1,0:T(8,128)(2,1)} %bitcast.18), custom_call_target="tpu_custom_call" | custom-call | tf_op jit(solution)/shard_map/pallas_call | solution.py:41
  105.5 0.0 all-gather.6.cloned.1.call-update
  105.6 0.1 convert_element_type.58
  105.7 0.1 broadcast_in_dim.40
  105.8 33.9 %all_to_all.22 = bf16[64,32,256]{2,1,0:T(8,128)(2,1)} all-to-all(bf16[64,32,256]{2,1,0:T(8,128)(2,1)S(1)} %bitcast.24), channel_id=1, replica_groups=mesh['gr'=2,'fs'=32,'tp'=8] {'gr','fs'}, dimensions={0} | all-to-all | bytes 2097152 | tf_op jit(solution)/shard_map/all_to_all | solution.py:133
  139.7 3.1 %all-gather.6.cloned.1.call-done = bf16[8192,256]{1,0:T(8,128)(2,1)} async-done(((bf16[1024,256]{1,0:T(8,128)(2,1)}), bf16[8192,256]{1,0:T(8,128)(2,1)}) %all-gather.6.cloned.1.call-update) | async-done | bytes 4194320 | tf_op jit(solution)/shard_map/all_gather | solution.py:130
  142.8 5.0 %shard_map.103 = bf16[1024,256]{1,0:T(8,128)(2,1)} custom-call(bf16[8,1024,256]{2,1,0:T(8,128)(2,1)} %bitcast.23, bf16[2048,256]{1,0:T(8,128)(2,1)} %bitcast.20), custom_call_target="tpu_custom_call" | custom-call | tf_op jit(solution)/shard_map/pallas_call | solution.py:41
  147.9 10.4 %all-to-all-start.3 = ((bf16[32,32,256]{2,1,0:T(8,128)(2,1)}), bf16[32,32,256]{2,1,0:T(8,128)(2,1)}, u32[]{:S(2)}, u32[]{:S(2)}) async-start(bf16[32,32,256]{2,1,0:T(8,128)(2,1)} %bitcast.26), calls=%async_computation.3 | async-start | bytes 1048576 | tf_op jit(solution)/shard_map/all_to_all | solution.py:136
  158.2 0.0 copy-start.13
  158.2 0.0 copy-start.1
  158.4 0.7 constant_dynamic-slice_fusion
  159.1 0.6 collective-permute-start
  159.7 2.8 %collective-permute-start.1 = (bf16[256,256]{1,0:T(8,128)(2,1)S(1)}, bf16[256,256]{1,0:T(8,128)(2,1)S(1)}, u32[]{:S(2)}, u32[]{:S(2)}) collective-permute-start(bf16[256,256]{1,0:T(8,128)(2,1)S(1)} %get-tuple-element.23), channel_id=1, source_target_pairs={{0,2},{1,3},{2,4},{3,5},{4,6},{5,7},{6,0},{7,1},{8,10},{9,11},{10,... | collective-permute-start | bytes 393224 | tf_op jit(solution)/shard_map/ppermute | solution.py:69
  162.6 2.9 %collective-permute-start.2 = (bf16[256,256]{1,0:T(8,128)(2,1)S(1)}, bf16[256,256]{1,0:T(8,128)(2,1)S(1)}, u32[]{:S(2)}, u32[]{:S(2)}) collective-permute-start(bf16[256,256]{1,0:T(8,128)(2,1)S(1)} %get-tuple-element.22), channel_id=1, source_target_pairs={{0,3},{1,4},{2,5},{3,6},{4,7},{5,0},{6,1},{7,2},{8,11},{9,12},{10,... | collective-permute-start | bytes 393224 | tf_op jit(solution)/shard_map/ppermute | solution.py:69
  165.4 3.7 %collective-permute-start.3 = (bf16[256,256]{1,0:T(8,128)(2,1)S(1)}, bf16[256,256]{1,0:T(8,128)(2,1)S(1)}, u32[]{:S(2)}, u32[]{:S(2)}) collective-permute-start(bf16[256,256]{1,0:T(8,128)(2,1)S(1)} %get-tuple-element.21), channel_id=1, source_target_pairs={{0,4},{1,5},{2,6},{3,7},{4,0},{5,1},{6,2},{7,3},{8,12},{9,13},{10,... | collective-permute-start | bytes 393224 | tf_op jit(solution)/shard_map/ppermute | solution.py:69
  169.2 4.5 %collective-permute-start.4 = (bf16[256,256]{1,0:T(8,128)(2,1)S(1)}, bf16[256,256]{1,0:T(8,128)(2,1)S(1)}, u32[]{:S(2)}, u32[]{:S(2)}) collective-permute-start(bf16[256,256]{1,0:T(8,128)(2,1)S(1)} %get-tuple-element.20), channel_id=1, source_target_pairs={{0,5},{1,6},{2,7},{3,0},{4,1},{5,2},{6,3},{7,4},{8,13},{9,14},{10,... | collective-permute-start | bytes 393224 | tf_op jit(solution)/shard_map/ppermute | solution.py:69
  173.7 0.0 collective-permute-done.refs_1_
  173.7 1.9 collective-permute-start.5
  175.7 0.0 collective-permute-done.1.refs_2_
  175.7 0.9 collective-permute-start.6
  176.6 1.5 slice_bitcast_fusion
  178.1 0.0 collective-permute-done.2.refs_3_
  178.1 0.0 collective-permute-done.3.refs_4_
  178.1 0.0 collective-permute-done.4.refs_5_
  178.1 2.7 %collective-permute-done.5.refs_6_ = bf16[256,256]{1,0:T(8,128)(2,1)S(1)} collective-permute-done((bf16[256,256]{1,0:T(8,128)(2,1)S(1)}, bf16[256,256]{1,0:T(8,128)(2,1)S(1)}, u32[]{:S(2)}, u32[]{:S(2)}) %collective-permute-start.5) | collective-permute-done | bytes 131104 | tf_op jit(solution)/shard_map/ppermute | solution.py:69
  180.8 0.8 collective-permute-done.6.refs_7_
  181.6 0.6 copy-done.12
  182.3 4.1 %place.1 = bf16[256,2048]{1,0:T(8,128)(2,1)} custom-call(s32[1]{0:T(128)} %bitcast.5.here, bf16[256,256]{1,0:T(8,128)(2,1)} %get-tuple-element.25.refs_0_, bf16[256,256]{1,0:T(8,128)(2,1)} %copy-done.6, bf16[256,256]{1,0:T(8,128)(2,1)} %copy-done.7, bf16[256,256]{1,0:T(8,128)(2,1)} %copy-done.8, bf16[256,256]{1,0:T(8,128)(2,1)} %copy-done.9, ...), custom_call_target="tpu_custom_call" | custom-call | tf_op jit(solution)/shard_map/place/pallas_call | solution.py:71
  186.4 0.0 all-to-all-done.3
  186.4 1.4 fusion.6
  187.8 2.1 %fusion.7 = bf16[320,256]{1,0:T(8,128)(2,1)} fusion(f32[320,256]{1,0:T(8,128)S(1)} %fusion.6, bf16[1024,256]{1,0:T(8,128)(2,1)} %bitcast.12, s32[320]{0:T(512)S(1)} %get-tuple-element.12, f32[320]{0:T(512)S(1)} %get-tuple-element.10), kind=kOutput, calls=%fused_computation.10 | convolution fusion | flops 168345600 | bytes 1018368 | tf_op jit(solution)/shard_map/dot_general | solution.py:142
  (26 shorter events, 0.1 us)
Async XLA Ops:
  7.2 1.9 copy-start
  7.2 92.0 %all-gather.4.cloned.1.call-start = ((), (), s32[]{:S(2)}) async-start(), calls=%async_computation.4 | async-start | bytes 4718592 | tf_op jit(solution)/shard_map/all_gather | solution.py:118
  9.0 29.5 %copy-start.5 = (f32[32,32,256]{2,1,0:T(8,128)S(1)}, f32[32,32,256]{2,1,0:T(8,128)}, u32[]{:S(2)}) copy-start(f32[32,32,256]{2,1,0:T(8,128)} %param.10) | copy-start | bytes 3145732
  9.7 28.8 %copy-start.4 = (f32[32,32,256]{2,1,0:T(8,128)S(1)}, f32[32,32,256]{2,1,0:T(8,128)}, u32[]{:S(2)}) copy-start(f32[32,32,256]{2,1,0:T(8,128)} %param.9) | copy-start | bytes 3145732
  9.7 28.8 %copy-start.14 = (f32[32]{0:T(128)S(1)}, f32[32]{0:T(128)}, u32[]{:S(2)}) copy-start(f32[32]{0:T(128)} %param.8) | copy-start | bytes 388
  38.5 104.4 %all-gather.6.cloned.1.call-start = ((), (), s32[]{:S(2)}) async-start(), calls=%async_computation.5 | async-start | bytes 4718592 | tf_op jit(solution)/shard_map/all_gather | solution.py:130
  99.2 6.3 %copy-start.3 = (f32[32,32,256]{2,1,0:T(8,128)S(1)}, f32[32,32,256]{2,1,0:T(8,128)}, u32[]{:S(2)}) copy-start(f32[32,32,256]{2,1,0:T(8,128)} %param.11) | copy-start | bytes 3145732
  147.9 10.5 %copy-start.2 = (bf16[64,32,256]{2,1,0:T(8,128)(2,1)S(1)}, bf16[64,32,256]{2,1,0:T(8,128)(2,1)}, u32[]{:S(2)}) copy-start(bf16[64,32,256]{2,1,0:T(8,128)(2,1)} %all_to_all.22) | copy-start | bytes 3145732
  147.9 38.5 %all-to-all-start.3 = ((bf16[32,32,256]{2,1,0:T(8,128)(2,1)}), bf16[32,32,256]{2,1,0:T(8,128)(2,1)}, u32[]{:S(2)}, u32[]{:S(2)}) async-start(bf16[32,32,256]{2,1,0:T(8,128)(2,1)} %bitcast.26), calls=%async_computation.3 | async-start | bytes 1048576 | tf_op jit(solution)/shard_map/all_to_all | solution.py:136
  158.2 4.3 %copy-start.13 = (f32[320,2]{0,1:T(2,128)S(1)}, f32[320,2]{0,1:T(2,128)}, u32[]{:S(2)}) copy-start(f32[320,2]{0,1:T(2,128)} %param.13) | copy-start | bytes 7684
  158.2 18.4 %copy-start.1 = (bf16[64,32,512]{2,1,0:T(8,128)(2,1)S(1)}, bf16[64,32,512]{2,1,0:T(8,128)(2,1)}, u32[]{:S(2)}) copy-start(bf16[64,32,512]{2,1,0:T(8,128)(2,1)} %all_to_all.21) | copy-start | bytes 6291460
  159.1 14.6 %collective-permute-start = (bf16[256,256]{1,0:T(8,128)(2,1)S(1)}, bf16[256,256]{1,0:T(8,128)(2,1)S(1)}, u32[]{:S(2)}, u32[]{:S(2)}) collective-permute-start(bf16[256,256]{1,0:T(8,128)(2,1)S(1)} %get-tuple-element.24), channel_id=1, source_target_pairs={{0,1},{1,2},{2,3},{3,4},{4,5},{5,6},{6,7},{7,0},{8,9},{9,10},{10,1... | collective-permute-start | bytes 393224 | tf_op jit(solution)/shard_map/ppermute | solution.py:69
  159.7 15.9 %collective-permute-start.1 = (bf16[256,256]{1,0:T(8,128)(2,1)S(1)}, bf16[256,256]{1,0:T(8,128)(2,1)S(1)}, u32[]{:S(2)}, u32[]{:S(2)}) collective-permute-start(bf16[256,256]{1,0:T(8,128)(2,1)S(1)} %get-tuple-element.23), channel_id=1, source_target_pairs={{0,2},{1,3},{2,4},{3,5},{4,6},{5,7},{6,0},{7,1},{8,10},{9,11},{10,... | collective-permute-start | bytes 393224 | tf_op jit(solution)/shard_map/ppermute | solution.py:69
  162.6 15.5 %collective-permute-start.2 = (bf16[256,256]{1,0:T(8,128)(2,1)S(1)}, bf16[256,256]{1,0:T(8,128)(2,1)S(1)}, u32[]{:S(2)}, u32[]{:S(2)}) collective-permute-start(bf16[256,256]{1,0:T(8,128)(2,1)S(1)} %get-tuple-element.22), channel_id=1, source_target_pairs={{0,3},{1,4},{2,5},{3,6},{4,7},{5,0},{6,1},{7,2},{8,11},{9,12},{10,... | collective-permute-start | bytes 393224 | tf_op jit(solution)/shard_map/ppermute | solution.py:69
  165.4 12.6 %collective-permute-start.3 = (bf16[256,256]{1,0:T(8,128)(2,1)S(1)}, bf16[256,256]{1,0:T(8,128)(2,1)S(1)}, u32[]{:S(2)}, u32[]{:S(2)}) collective-permute-start(bf16[256,256]{1,0:T(8,128)(2,1)S(1)} %get-tuple-element.21), channel_id=1, source_target_pairs={{0,4},{1,5},{2,6},{3,7},{4,0},{5,1},{6,2},{7,3},{8,12},{9,13},{10,... | collective-permute-start | bytes 393224 | tf_op jit(solution)/shard_map/ppermute | solution.py:69
  169.2 8.9 %collective-permute-start.4 = (bf16[256,256]{1,0:T(8,128)(2,1)S(1)}, bf16[256,256]{1,0:T(8,128)(2,1)S(1)}, u32[]{:S(2)}, u32[]{:S(2)}) collective-permute-start(bf16[256,256]{1,0:T(8,128)(2,1)S(1)} %get-tuple-element.20), channel_id=1, source_target_pairs={{0,5},{1,6},{2,7},{3,0},{4,1},{5,2},{6,3},{7,4},{8,13},{9,14},{10,... | collective-permute-start | bytes 393224 | tf_op jit(solution)/shard_map/ppermute | solution.py:69
  173.7 4.3 %copy-start.6 = (bf16[256,256]{1,0:T(8,128)(2,1)}, bf16[256,256]{1,0:T(8,128)(2,1)S(1)}, u32[]{:S(2)}) copy-start(bf16[256,256]{1,0:T(8,128)(2,1)S(1)} %collective-permute-done.refs_1_) | copy-start | bytes 393220
  173.7 7.1 %collective-permute-start.5 = (bf16[256,256]{1,0:T(8,128)(2,1)S(1)}, bf16[256,256]{1,0:T(8,128)(2,1)S(1)}, u32[]{:S(2)}, u32[]{:S(2)}) collective-permute-start(bf16[256,256]{1,0:T(8,128)(2,1)S(1)} %get-tuple-element.19), channel_id=1, source_target_pairs={{0,6},{1,7},{2,0},{3,1},{4,2},{5,3},{6,4},{7,5},{8,14},{9,15},{10,... | collective-permute-start | bytes 393224 | tf_op jit(solution)/shard_map/ppermute | solution.py:69
  175.7 2.4 %copy-start.7 = (bf16[256,256]{1,0:T(8,128)(2,1)}, bf16[256,256]{1,0:T(8,128)(2,1)S(1)}, u32[]{:S(2)}) copy-start(bf16[256,256]{1,0:T(8,128)(2,1)S(1)} %collective-permute-done.1.refs_2_) | copy-start | bytes 393220
  175.7 5.9 %collective-permute-start.6 = (bf16[256,256]{1,0:T(8,128)(2,1)S(1)}, bf16[256,256]{1,0:T(8,128)(2,1)S(1)}, u32[]{:S(2)}, u32[]{:S(2)}) collective-permute-start(bf16[256,256]{1,0:T(8,128)(2,1)S(1)} %get-tuple-element.18), channel_id=1, source_target_pairs={{0,7},{1,0},{2,1},{3,2},{4,3},{5,4},{6,5},{7,6},{8,15},{9,8},{10,9... | collective-permute-start | bytes 393224 | tf_op jit(solution)/shard_map/ppermute | solution.py:69
  178.1 3.6 %copy-start.8 = (bf16[256,256]{1,0:T(8,128)(2,1)}, bf16[256,256]{1,0:T(8,128)(2,1)S(1)}, u32[]{:S(2)}) copy-start(bf16[256,256]{1,0:T(8,128)(2,1)S(1)} %collective-permute-done.2.refs_3_) | copy-start | bytes 393220
  178.1 3.6 %copy-start.9 = (bf16[256,256]{1,0:T(8,128)(2,1)}, bf16[256,256]{1,0:T(8,128)(2,1)S(1)}, u32[]{:S(2)}) copy-start(bf16[256,256]{1,0:T(8,128)(2,1)S(1)} %collective-permute-done.3.refs_4_) | copy-start | bytes 393220
  178.1 3.5 %copy-start.10 = (bf16[256,256]{1,0:T(8,128)(2,1)}, bf16[256,256]{1,0:T(8,128)(2,1)S(1)}, u32[]{:S(2)}) copy-start(bf16[256,256]{1,0:T(8,128)(2,1)S(1)} %collective-permute-done.4.refs_5_) | copy-start | bytes 393220
  180.8 0.8 copy-start.11
  181.6 0.6 copy-start.12
Sparse Core Ops, SparseCore 0:
  38.6 38.8 all-gather.3
  105.7 37.0 all-gather.5

commit v3 on v2

--- a/solution.py
+++ b/solution.py
@@ -7,47 +7,96 @@
 
 
 SLOTS = 32
+LANES = 128
 BF = jnp.bfloat16
 F32 = jnp.float32
 
 
-def pieces_dot(ref, weights):
-    rows = jnp.concatenate([ref[k] for k in range(ref.shape[0])], axis=1)
-    return jnp.dot(rows, weights[...], preferred_element_type=F32)
-
-
-def hidden_kernel(rows, gate_up, out):
-    width = rows.shape[2]
-    total = rows.shape[0] * width
-    acc = pieces_dot(rows, gate_up)
+def pieces_dot(sender, pieces, weights):
+    acc = None
+    for k, piece in enumerate(pieces):
+        at = pl.multiple_of(sender[k] * piece.shape[1], piece.shape[1])
+        part = jnp.dot(
+            piece[...], weights[pl.ds(at, piece.shape[1]), :], preferred_element_type=F32
+        )
+        acc = part if acc is None else acc + part
+    return acc
+
+
+def scale_kernel(*refs):
+    pieces, out = refs[:-1], refs[-1]
+    total = sum(piece.shape[1] for piece in pieces)
     squares = None
-    for k in range(rows.shape[0]):
-        values = rows[k].astype(F32)
+    for piece in pieces:
+        values = piece[...].astype(F32)
         part = jnp.sum(values * values, axis=-1, keepdims=True)
         squares = part if squares is None else squares + part
-    acc = acc * lax.rsqrt(squares / total + 1e-06)
+    out[...] = jnp.broadcast_to(lax.rsqrt(squares / total + 1e-06), out.shape)
+
+
+def row_scale(pieces, steps=4):
+    count, width = pieces[0].shape
+    block = count // steps
+    return pl.pallas_call(
+        scale_kernel,
+        name="row_scale",
+        grid=(steps,),
+        in_specs=[pl.BlockSpec((block, width), lambda i: (i, 0))] * len(pieces),
+        out_specs=pl.BlockSpec((block, LANES), lambda i: (i, 0)),
+        out_shape=jax.ShapeDtypeStruct((count, LANES), F32),
+        compiler_params=pltpu.CompilerParams(vmem_limit_bytes=8 * 1024 * 1024),
+    )(*pieces)
+
+
+def hidden_kernel(sender, *refs):
+    pieces, scale, gate_up, out = refs[:-3], refs[-3], refs[-2], refs[-1]
     half = out.shape[1]
+    acc = pieces_dot(sender, pieces, gate_up) * scale[:, :1]
     gate, up = acc[:, :half], acc[:, half:]
     out[...] = (gate / (1.0 + jnp.exp(-gate)) * up).astype(out.dtype)
 
 
-def out_kernel(rows, down, out):
-    out[...] = pieces_dot(rows, down).astype(out.dtype)
-
-
-def row_call(kernel, rows, weights, out_width, steps=4):
-    pieces, count, width = rows.shape
+def out_kernel(sender, *refs):
+    out = refs[-1]
+    out[...] = pieces_dot(sender, refs[:-2], refs[-2]).astype(out.dtype)
+
+
+def row_call(kernel, sender, rows, weights, out_width, steps=4):
+    count = rows[0].shape[0]
     block = count // steps
     return pl.pallas_call(
         kernel,
-        grid=(steps,),
-        in_specs=[
-            pl.BlockSpec((pieces, block, width), lambda i: (0, i, 0)),
-            pl.BlockSpec(weights.shape, lambda i: (0, 0)),
-        ],
-        out_specs=pl.BlockSpec((block, out_width), lambda i: (i, 0)),
+        grid_spec=pltpu.PrefetchScalarGridSpec(
+            num_scalar_prefetch=1,
+            grid=(steps,),
+            in_specs=[pl.BlockSpec((block, r.shape[1]), lambda i, at: (i, 0)) for r in rows]
+            + [pl.BlockSpec(weights.shape, lambda i, at: (0, 0))],
+            out_specs=pl.BlockSpec((block, out_width), lambda i, at: (i, 0)),
+        ),
         out_shape=jax.ShapeDtypeStruct((count, out_width), BF),
-    )(rows, weights)
+    )(sender, *rows, weights)
+
+
+def gather_pieces(piece, axis):
+    count = lax.axis_size(axis)
+
+    def shift(value, by):
+        return lax.ppermute(value, axis, [(i, (i + by) % count) for i in range(count)])
+
+    def partner(value):
+        return lax.ppermute(value, axis, [(i, i ^ 1) for i in range(count)])
+
+    steps = [2, count - 2] + list(range(4, count - 2, 2))
+    same = [shift(piece, by) for by in steps]
+    own = [piece, *same]
+    return own + [partner(value) for value in own]
+
+
+def piece_senders(axis):
+    count, here = lax.axis_size(axis), lax.axis_index(axis)
+    steps = jnp.array([0, 2, count - 2] + list(range(4, count - 2, 2)), jnp.int32)
+    other = here + 1 - 2 * (here % 2)
+    return jnp.concatenate([(here - steps) % count, (other - steps) % count]).astype(jnp.int32)
 
 
 def place_kernel(here, *refs):
@@ -78,6 +127,7 @@
             out_specs=pl.BlockSpec((rows, cols), lambda k, at: (0, (at[0] - k + count) % count)),
         ),
         out_shape=jax.ShapeDtypeStruct((rows, count * cols), array.dtype),
+        compiler_params=pltpu.CompilerParams(vmem_limit_bytes=8 * 1024 * 1024),
     )(here.reshape(1).astype(jnp.int32), *pieces)
 
 
@@ -109,13 +159,20 @@
     slot_ids = jnp.arange(slots_all, dtype=jnp.int32)[None, :]
     select_first = (target_first[:, None] == slot_ids).astype(BF)
     select_second = (target_second[:, None] == slot_ids).astype(BF)
+    weighted = jnp.where(
+        target_first[:, None] == slot_ids,
+        route_weight[:, 0:1],
+        jnp.where(target_second[:, None] == slot_ids, route_weight[:, 1:2], 0.0),
+    ).astype(BF)
     outbound = jnp.einsum(
         "ts,td->sd", select_first + select_second, prompt, preferred_element_type=F32
     ).astype(BF)
     moved = lax.all_to_all(
         outbound.reshape(experts, SLOTS, width), "fs", split_axis=0, concat_axis=0, tiled=True
     )
-    arrived = lax.all_gather(moved.reshape(1, slots_all, width), "tp", axis=0, tiled=True)
+    arrived = gather_pieces(moved.reshape(slots_all, width), "tp")
+    scale = row_scale(arrived)
+    sender = piece_senders("tp")
 
     gain = norm_gain[None, :, None]
     gate_up = jnp.concatenate(
@@ -126,22 +183,20 @@
     gate_up = gate_up.reshape(-1, 2 * cols)
     gate_new, up_new = gate_up[None, :, :cols], gate_up[None, :, cols:]
 
-    hidden = row_call(hidden_kernel, arrived, gate_up, cols)
-    hidden_all = lax.all_gather(hidden[None], "tp", axis=0, tiled=True)
-
-    down = after(both_groups(down_weight.astype(BF)), hidden)
+    down = after(both_groups(down_weight.astype(BF)), gate_up)
     down = lax.all_to_all(down, ("gr", "fs"), split_axis=0, concat_axis=0, tiled=True)
     down = down.reshape(-1, cols)
-    summed = row_call(out_kernel, hidden_all, down, cols)
+
+    hidden = row_call(hidden_kernel, sender, [*arrived, scale], gate_up, cols)
+    hidden_all = gather_pieces(hidden, "tp")
+    summed = row_call(out_kernel, sender, hidden_all, down, cols)
     returned = lax.all_to_all(
         summed.reshape(experts, SLOTS, width), "fs", split_axis=0, concat_axis=0, tiled=True
     )
     returned = returned.reshape(slots_all, width)
     down_new = exchange_units(down, "tp")
 
-    pick_first = jnp.dot(select_first, returned, preferred_element_type=F32)
-    pick_second = jnp.dot(select_second, returned, preferred_element_type=F32)
-    mixed = route_weight[:, 0:1] * pick_first + route_weight[:, 1:2] * pick_second
+    mixed = jnp.dot(weighted, returned, preferred_element_type=F32)
     return (gate_new, up_new, down_new[None], mixed.astype(BF))
 
 

time: 197 us -> 212 us (1.076)
  blocking collectives: 123 us -> 0 us
  starting transfers between devices: 27.8 us -> 113 us
  waiting for transfers between devices: 6.66 us -> 61.9 us
  between operations: 14.5 us -> 1.35 us
  local copies, waits for them, and re-layouts: 4.08 us -> 8.75 us
  Pallas kernels: 15.4 us -> 19.1 us
    all_to_all x3 -> x0, blocking collectives: 123 us -> none  [the longest x1 60 us: body(): lax.all_to_all(gate_up, ('gr', 'fs'), split_axis=0, concat_axis=0, tiled=...]
    all_to_all x0 -> x3, waiting for transfers between devices: none -> 52.2 us  [the longest x1 37.4 us: body(): lax.all_to_all(gate_up, ('gr', 'fs'), split_axis=0, concat_axis=0, tiled=...]
    ppermute x0 -> x14, starting transfers between devices: none -> 51.5 us  [the longest x8 31.6 us: partner(): return lax.ppermute(value, axis, [(i, i ^ 1) for i in range(count)])]
    all_to_all x0 -> x3, starting transfers between devices: none -> 34.1 us  [the longest x1 13.5 us: body(): lax.all_to_all(outbound.reshape(experts, SLOTS, width), 'fs', split_axis=...]
    ppermute x0 -> x14, waiting for transfers between devices: none -> 7.12 us  [the longest x6 3.83 us: shift(): lax.ppermute(value, axis, [(i, (i + by) % count) for i in range(count)])]
    pallas_call x2 -> x3, Pallas kernels: 11.3 us -> 16.3 us  [the longest x2 13.2 us: row_call(): pl.pallas_call(kernel, grid_spec=pltpu.PrefetchScalarGridSpec(num_scalar_...]
    all_gather x2 -> x0, waiting for transfers between devices: 3.1 us -> none  [the longest x1 3.1 us: body(): hidden_all = lax.all_gather(hidden[None], 'tp', axis=0, tiled=True)]
    dot_general x2 -> x1, matrix products: 3.53 us -> 1.17 us  [body(): mixed = jnp.dot(weighted, returned, preferred_element_type=F32)]
  transfers between devices with their start and end apart: 10 -> 25, of which waited for: 3 -> 6; matrix products, arithmetic and copies ran while one was open for 2% -> 4% of each run, Pallas kernels for 2% -> 6%
where the time goes in v3:
time: 212 us; the launch traced here: 210 us
  starting transfers between devices  113 us (53%)
  waiting for transfers between devices  61.9 us (29%)
  Pallas kernels  19.1 us (9%)
  local copies, waits for them, and re-layouts  8.75 us (4%)
  other arithmetic  3.12 us (1%)
  matrix products  2.83 us (1%)
    all_to_all x1, waiting for transfers between devices, body(): lax.all_to_all(gate_up, ('gr', 'fs'), split_axis=0, concat_axis=0, tiled=...  37.4 us
    ppermute x8, starting transfers between devices, partner(): return lax.ppermute(value, axis, [(i, i ^ 1) for i in range(count)])  31.6 us
    ppermute x6, starting transfers between devices, shift(): lax.ppermute(value, axis, [(i, (i + by) % count) for i in range(count)])  19.9 us
    ppermute x7, starting transfers between devices, exchange_units(): lax.ppermute(block, axis, [(i, (i + k) % count) for i in range(count)])  18.1 us
    all_to_all x1, waiting for transfers between devices, body(): lax.all_to_all(outbound.reshape(experts, SLOTS, width), 'fs', split_axis=...  14.8 us
    all_to_all x1, starting transfers between devices, body(): lax.all_to_all(outbound.reshape(experts, SLOTS, width), 'fs', split_axis=...  13.5 us
    pallas_call x2, Pallas kernels, row_call(): pl.pallas_call(kernel, grid_spec=pltpu.PrefetchScalarGridSpec(num_scalar_...  13.2 us
    all_to_all x1, starting transfers between devices, body(): lax.all_to_all(gate_up, ('gr', 'fs'), split_axis=0, concat_axis=0, tiled=...  11.5 us
  transfers between devices with their start and end apart: 25, of which 6 were waited for; matrix products, arithmetic and copies ran while one was open for 4% of the time, Pallas kernels for 6%

profile of v3, /device:TPU:1, one launch (start us, length us, event | category | flops | bytes accessed | tf_op | source)
XLA Modules:
  0.0 210.2 jit_solution(18049437307697781907)
XLA Ops:
  0.6 0.8 slice_reduce_fusion.3
  1.4 0.2 select_reduce_fusion.1
  1.7 0.8 add_reduce_fusion.1
  2.5 1.4 convolution_convert_fusion
  3.9 13.5 %all-to-all-start = ((bf16[32,32,256]{2,1,0:T(8,128)(2,1)}), bf16[32,32,256]{2,1,0:T(8,128)(2,1)S(1)}, u32[]{:S(2)}, u32[]{:S(2)}) async-start(bf16[32,32,256]{2,1,0:T(8,128)(2,1)} %bitcast.1), calls=%async_computation | async-start | bytes 1048576 | tf_op jit(solution)/shard_map/all_to_all | solution.py:170
  17.4 0.3 multiply_convert_fusion.1
  17.8 14.8 %all-to-all-done = bf16[32,32,256]{2,1,0:T(8,128)(2,1)S(1)} async-done(((bf16[32,32,256]{2,1,0:T(8,128)(2,1)}), bf16[32,32,256]{2,1,0:T(8,128)(2,1)S(1)}, u32[]{:S(2)}, u32[]{:S(2)}) %all-to-all-start) | async-done | bytes 524320 | tf_op jit(solution)/shard_map/all_to_all | solution.py:170
  32.6 1.6 broadcast_in_dim.59
  34.2 11.5 %all-to-all-start.1 = ((bf16[64,32,512]{2,1,0:T(8,128)(2,1)}), bf16[64,32,512]{2,1,0:T(8,128)(2,1)}, u32[]{:S(2)}, u32[]{:S(2)}) async-start(bf16[64,32,512]{2,1,0:T(8,128)(2,1)} %bitcast), calls=%async_computation.1 | async-start | bytes 4194304 | tf_op jit(solution)/shard_map/all_to_all | solution.py:182
  45.8 3.1 %collective-permute-start.7 = (bf16[1024,256]{1,0:T(8,128)(2,1)S(1)}, bf16[1024,256]{1,0:T(8,128)(2,1)S(1)}, u32[]{:S(2)}, u32[]{:S(2)}) collective-permute-start(bf16[1024,256]{1,0:T(8,128)(2,1)S(1)} %bitcast.16), channel_id=1, source_target_pairs={{0,2},{1,3},{2,4},{3,5},{4,6},{5,7},{6,0},{7,1},{8,10},{9,11},{10,... | collective-permute-start | bytes 1572872 | tf_op jit(solution)/shard_map/ppermute | solution.py:84
  48.9 3.4 %collective-permute-start.8 = (bf16[1024,256]{1,0:T(8,128)(2,1)S(1)}, bf16[1024,256]{1,0:T(8,128)(2,1)S(1)}, u32[]{:S(2)}, u32[]{:S(2)}) collective-permute-start(bf16[1024,256]{1,0:T(8,128)(2,1)S(1)} %bitcast.17), channel_id=1, source_target_pairs={{0,6},{1,7},{2,0},{3,1},{4,2},{5,3},{6,4},{7,5},{8,14},{9,15},{10,... | collective-permute-start | bytes 1572872 | tf_op jit(solution)/shard_map/ppermute | solution.py:84
  52.3 3.4 %collective-permute-start.9 = (bf16[1024,256]{1,0:T(8,128)(2,1)S(1)}, bf16[1024,256]{1,0:T(8,128)(2,1)S(1)}, u32[]{:S(2)}, u32[]{:S(2)}) collective-permute-start(bf16[1024,256]{1,0:T(8,128)(2,1)S(1)} %bitcast.18), channel_id=1, source_target_pairs={{0,4},{1,5},{2,6},{3,7},{4,0},{5,1},{6,2},{7,3},{8,12},{9,13},{10,... | collective-permute-start | bytes 1572872 | tf_op jit(solution)/shard_map/ppermute | solution.py:84
  55.7 1.3 convert_element_type.61
  57.0 37.4 %all-to-all-done.1 = bf16[64,32,512]{2,1,0:T(8,128)(2,1)} async-done(((bf16[64,32,512]{2,1,0:T(8,128)(2,1)}), bf16[64,32,512]{2,1,0:T(8,128)(2,1)}, u32[]{:S(2)}, u32[]{:S(2)}) %all-to-all-start.1) | async-done | bytes 2097184 | tf_op jit(solution)/shard_map/all_to_all | solution.py:182
  94.4 1.1 broadcast_in_dim.63
  95.5 9.1 %all-to-all-start.2 = ((bf16[64,32,256]{2,1,0:T(8,128)(2,1)}), bf16[64,32,256]{2,1,0:T(8,128)(2,1)}, u32[]{:S(2)}, u32[]{:S(2)}) async-start(bf16[64,32,256]{2,1,0:T(8,128)(2,1)} %bitcast.6), calls=%async_computation.2 | async-start | bytes 2097152 | tf_op jit(solution)/shard_map/all_to_all | solution.py:187
  104.6 5.2 %collective-permute-start.10 = (bf16[1024,256]{1,0:T(8,128)(2,1)S(1)}, bf16[1024,256]{1,0:T(8,128)(2,1)S(1)}, u32[]{:S(2)}, u32[]{:S(2)}) collective-permute-start(bf16[1024,256]{1,0:T(8,128)(2,1)S(1)} %bitcast.19), channel_id=1, source_target_pairs={{0,1},{1,0},{2,3},{3,2},{4,5},{5,4},{6,7},{7,6},{8,9},{9,8},{10,11... | collective-permute-start | bytes 1572872 | tf_op jit(solution)/shard_map/ppermute | solution.py:87
  109.8 1.9 collective-permute-start.11
  111.8 2.4 %collective-permute-start.12 = (bf16[1024,256]{1,0:T(8,128)(2,1)S(1)}, bf16[1024,256]{1,0:T(8,128)(2,1)}, u32[]{:S(2)}, u32[]{:S(2)}) collective-permute-start(bf16[1024,256]{1,0:T(8,128)(2,1)S(1)} %collective-permute-done.8.refs_2_), channel_id=1, source_target_pairs={{0,1},{1,0},{2,3},{3,2},{4,5},{5,4},{6,7},{7,6},{8,9},{9,8},{10,11... | collective-permute-start | bytes 1572872 | tf_op jit(solution)/shard_map/ppermute | solution.py:87
  114.2 1.9 collective-permute-start.13
  116.2 0.6 pad_add_fusion.sender
  116.8 1.3 collective-permute-done.13.refs_7_
  118.1 3.1 %row_scale.1.refs_8_ = f32[1024,128]{1,0:T(8,128)S(1)} custom-call(bf16[1024,256]{1,0:T(8,128)(2,1)S(1)} %bitcast.20, bf16[1024,256]{1,0:T(8,128)(2,1)S(1)} %collective-permute-done.7.refs_1_, bf16[1024,256]{1,0:T(8,128)(2,1)S(1)} %collective-permute-done.8.refs_2_, bf16[1024,256]{1,0:T(8,128)(2,1)S(1)} %collective-permute-done.9.refs_3_, ...), custom_call_target="tpu_custom_call" | custom-call | tf_op jit(solution)/shard_map/row_scale/pallas_call | solution.py:40
  121.3 0.8 copy-done.7
  122.1 7.2 %shard_map.111.refs_0_ = bf16[1024,256]{1,0:T(8,128)(2,1)} custom-call(s32[8]{0:T(128)} %pad_add_fusion.sender, bf16[1024,256]{1,0:T(8,128)(2,1)} %bitcast.21, bf16[1024,256]{1,0:T(8,128)(2,1)} %copy-done.2, bf16[1024,256]{1,0:T(8,128)(2,1)} %copy-done.3, bf16[1024,256]{1,0:T(8,128)(2,1)} %copy-done.4, bf16[1024,256]{1,0:T(8,128)(2,1)} %copy-done.5, ...), custom_call_target="tpu_custom_call" | custom-call | tf_op jit(solution)/shard_map/pallas_call | solution.py:67
  129.3 3.1 %collective-permute-start.14 = (bf16[1024,256]{1,0:T(8,128)(2,1)}, bf16[1024,256]{1,0:T(8,128)(2,1)S(1)}, u32[]{:S(2)}, u32[]{:S(2)}) collective-permute-start(bf16[1024,256]{1,0:T(8,128)(2,1)} %shard_map.111.refs_0_), channel_id=1, source_target_pairs={{0,2},{1,3},{2,4},{3,5},{4,6},{5,7},{6,0},{7,1},{8,10},{9,11},{10,... | collective-permute-start | bytes 1572872 | tf_op jit(solution)/shard_map/ppermute | solution.py:84
  132.4 3.4 %collective-permute-start.15 = (bf16[1024,256]{1,0:T(8,128)(2,1)}, bf16[1024,256]{1,0:T(8,128)(2,1)S(1)}, u32[]{:S(2)}, u32[]{:S(2)}) collective-permute-start(bf16[1024,256]{1,0:T(8,128)(2,1)} %shard_map.111.refs_0_), channel_id=1, source_target_pairs={{0,6},{1,7},{2,0},{3,1},{4,2},{5,3},{6,4},{7,5},{8,14},{9,15},{10,... | collective-permute-start | bytes 1572872 | tf_op jit(solution)/shard_map/ppermute | solution.py:84
  135.8 3.4 %collective-permute-start.16 = (bf16[1024,256]{1,0:T(8,128)(2,1)}, bf16[1024,256]{1,0:T(8,128)(2,1)S(1)}, u32[]{:S(2)}, u32[]{:S(2)}) collective-permute-start(bf16[1024,256]{1,0:T(8,128)(2,1)} %shard_map.111.refs_0_), channel_id=1, source_target_pairs={{0,4},{1,5},{2,6},{3,7},{4,0},{5,1},{6,2},{7,3},{8,12},{9,13},{10,... | collective-permute-start | bytes 1572872 | tf_op jit(solution)/shard_map/ppermute | solution.py:84
  139.2 2.9 %collective-permute-start.17 = (bf16[1024,256]{1,0:T(8,128)(2,1)}, bf16[1024,256]{1,0:T(8,128)(2,1)S(1)}, u32[]{:S(2)}, u32[]{:S(2)}) collective-permute-start(bf16[1024,256]{1,0:T(8,128)(2,1)} %shard_map.111.refs_0_), channel_id=1, source_target_pairs={{0,1},{1,0},{2,3},{3,2},{4,5},{5,4},{6,7},{7,6},{8,9},{9,8},{10,11... | collective-permute-start | bytes 1572872 | tf_op jit(solution)/shard_map/ppermute | solution.py:87
  142.1 3.8 %collective-permute-done.14.refs_1_ = bf16[1024,256]{1,0:T(8,128)(2,1)S(1)} collective-permute-done((bf16[1024,256]{1,0:T(8,128)(2,1)}, bf16[1024,256]{1,0:T(8,128)(2,1)S(1)}, u32[]{:S(2)}, u32[]{:S(2)}) %collective-permute-start.14) | collective-permute-done | bytes 524320 | tf_op jit(solution)/shard_map/ppermute | solution.py:84
  145.9 2.9 %collective-permute-start.18 = (bf16[1024,256]{1,0:T(8,128)(2,1)S(1)}, bf16[1024,256]{1,0:T(8,128)(2,1)S(1)}, u32[]{:S(2)}, u32[]{:S(2)}) collective-permute-start(bf16[1024,256]{1,0:T(8,128)(2,1)S(1)} %collective-permute-done.14.refs_1_), channel_id=1, source_target_pairs={{0,1},{1,0},{2,3},{3,2},{4,5},{5,4},{6,7},{7,6},{8,9},{9,8},{10,11... | collective-permute-start | bytes 1572872 | tf_op jit(solution)/shard_map/ppermute | solution.py:87
  148.9 12.5 %collective-permute-start.19 = (bf16[1024,256]{1,0:T(8,128)(2,1)S(1)}, bf16[1024,256]{1,0:T(8,128)(2,1)S(1)}, u32[]{:S(2)}, u32[]{:S(2)}) collective-permute-start(bf16[1024,256]{1,0:T(8,128)(2,1)S(1)} %collective-permute-done.15.refs_2_), channel_id=1, source_target_pairs={{0,1},{1,0},{2,3},{3,2},{4,5},{5,4},{6,7},{7,6},{8,9},{9,8},{10,11... | collective-permute-start | bytes 1572872 | tf_op jit(solution)/shard_map/ppermute | solution.py:87
  161.4 1.9 collective-permute-start.20
  163.4 1.9 collective-permute-done.20.refs_7_
  165.4 6.0 %shard_map.112 = bf16[1024,256]{1,0:T(8,128)(2,1)} custom-call(s32[8]{0:T(128)} %pad_add_fusion.sender, bf16[1024,256]{1,0:T(8,128)(2,1)} %shard_map.111.refs_0_, bf16[1024,256]{1,0:T(8,128)(2,1)} %copy-done.10, bf16[1024,256]{1,0:T(8,128)(2,1)} %copy-done.11, bf16[1024,256]{1,0:T(8,128)(2,1)} %copy-done.12, bf16[1024,256]{1,0:T(8,128)(2,1)} %copy-done.13, ...), custom_call_target="tpu_custom_call" | custom-call | tf_op jit(solution)/shard_map/pallas_call | solution.py:67
  171.4 9.6 %all-to-all-start.3 = ((bf16[32,32,256]{2,1,0:T(8,128)(2,1)}), bf16[32,32,256]{2,1,0:T(8,128)(2,1)S(1)}, u32[]{:S(2)}, u32[]{:S(2)}) async-start(bf16[32,32,256]{2,1,0:T(8,128)(2,1)} %bitcast.22), calls=%async_computation.3 | async-start | bytes 1048576 | tf_op jit(solution)/shard_map/all_to_all | solution.py:193
  181.1 1.4 constant_dynamic-slice_fusion
  182.4 0.7 collective-permute-start
  183.1 1.9 collective-permute-start.1
  185.1 6.4 %collective-permute-start.2 = (bf16[256,256]{1,0:T(8,128)(2,1)S(1)}, bf16[256,256]{1,0:T(8,128)(2,1)S(1)}, u32[]{:S(2)}, u32[]{:S(2)}) collective-permute-start(bf16[256,256]{1,0:T(8,128)(2,1)S(1)} %get-tuple-element.22), channel_id=1, source_target_pairs={{0,3},{1,4},{2,5},{3,6},{4,7},{5,0},{6,1},{7,2},{8,11},{9,12},{10,... | collective-permute-start | bytes 393224 | tf_op jit(solution)/shard_map/ppermute | solution.py:118
  191.4 1.9 collective-permute-start.3
  193.4 4.2 %collective-permute-start.4 = (bf16[256,256]{1,0:T(8,128)(2,1)S(1)}, bf16[256,256]{1,0:T(8,128)(2,1)S(1)}, u32[]{:S(2)}, u32[]{:S(2)}) collective-permute-start(bf16[256,256]{1,0:T(8,128)(2,1)S(1)} %get-tuple-element.20), channel_id=1, source_target_pairs={{0,5},{1,6},{2,7},{3,0},{4,1},{5,2},{6,3},{7,4},{8,13},{9,14},{10,... | collective-permute-start | bytes 393224 | tf_op jit(solution)/shard_map/ppermute | solution.py:118
  197.5 2.8 %collective-permute-start.5 = (bf16[256,256]{1,0:T(8,128)(2,1)S(1)}, bf16[256,256]{1,0:T(8,128)(2,1)S(1)}, u32[]{:S(2)}, u32[]{:S(2)}) collective-permute-start(bf16[256,256]{1,0:T(8,128)(2,1)S(1)} %get-tuple-element.19), channel_id=1, source_target_pairs={{0,6},{1,7},{2,0},{3,1},{4,2},{5,3},{6,4},{7,5},{8,14},{9,15},{10,... | collective-permute-start | bytes 393224 | tf_op jit(solution)/shard_map/ppermute | solution.py:118
  200.3 0.3 collective-permute-start.6
  200.6 3.0 %slice_bitcast_fusion = (bf16[1,2048,256]{2,1,0:T(8,128)(2,1)}, bf16[1,2048,256]{2,1,0:T(8,128)(2,1)}) fusion(bf16[2048,512]{1,0:T(8,128)(2,1)} %bitcast.2.refs_9_), kind=kLoop, calls=%fused_computation.7 | loop fusion | bytes 4194304 | tf_op jit(solution)/shard_map/broadcast_in_dim | solution.py:184
  203.6 2.6 %collective-permute-done.6.refs_7_ = bf16[256,256]{1,0:T(8,128)(2,1)S(1)} collective-permute-done((bf16[256,256]{1,0:T(8,128)(2,1)S(1)}, bf16[256,256]{1,0:T(8,128)(2,1)S(1)}, u32[]{:S(2)}, u32[]{:S(2)}) %collective-permute-start.6) | collective-permute-done | bytes 131104 | tf_op jit(solution)/shard_map/ppermute | solution.py:118
  206.2 2.8 %place.1 = bf16[256,2048]{1,0:T(8,128)(2,1)} custom-call(s32[1]{0:T(128)} %bitcast.5.here, bf16[256,256]{1,0:T(8,128)(2,1)S(1)} %get-tuple-element.25.refs_0_, bf16[256,256]{1,0:T(8,128)(2,1)S(1)} %collective-permute-done.refs_1_, bf16[256,256]{1,0:T(8,128)(2,1)S(1)} %collective-permute-done.1.refs_2_, bf16[256,256]{1,0:T(8,128)(2,1)S(1)} %collective-permute-done.2.refs_3_, ...), custom_call_target="tpu_custom_call" | custom-call | tf_op jit(solution)/shard_map/place/pallas_call | solution.py:120
  209.0 1.2 convolution_convert_fusion.1
  (61 shorter events, 0.3 us)
Async XLA Ops:
  0.6 1.8 copy-start
  2.5 14.9 %copy-start.8 = (f32[32,32,256]{2,1,0:T(8,128)S(1)}, f32[32,32,256]{2,1,0:T(8,128)}, u32[]{:S(2)}) copy-start(f32[32,32,256]{2,1,0:T(8,128)} %param.10) | copy-start | bytes 3145732
  2.5 14.9 %copy-start.9 = (f32[32,32,256]{2,1,0:T(8,128)S(1)}, f32[32,32,256]{2,1,0:T(8,128)}, u32[]{:S(2)}) copy-start(f32[32,32,256]{2,1,0:T(8,128)} %param.11) | copy-start | bytes 3145732
  2.5 14.9 %copy-start.18 = (f32[32]{0:T(128)S(1)}, f32[32]{0:T(128)}, u32[]{:S(2)}) copy-start(f32[32]{0:T(128)} %param.9) | copy-start | bytes 388
  3.9 28.7 %all-to-all-start = ((bf16[32,32,256]{2,1,0:T(8,128)(2,1)}), bf16[32,32,256]{2,1,0:T(8,128)(2,1)S(1)}, u32[]{:S(2)}, u32[]{:S(2)}) async-start(bf16[32,32,256]{2,1,0:T(8,128)(2,1)} %bitcast.1), calls=%async_computation | async-start | bytes 1048576 | tf_op jit(solution)/shard_map/all_to_all | solution.py:170
  32.6 85.5 %copy-start.1 = (bf16[32,32,256]{2,1,0:T(8,128)(2,1)}, bf16[32,32,256]{2,1,0:T(8,128)(2,1)S(1)}, u32[]{:S(2)}) copy-start(bf16[32,32,256]{2,1,0:T(8,128)(2,1)S(1)} %all-to-all-done) | copy-start | bytes 1572868
  34.2 60.2 %all-to-all-start.1 = ((bf16[64,32,512]{2,1,0:T(8,128)(2,1)}), bf16[64,32,512]{2,1,0:T(8,128)(2,1)}, u32[]{:S(2)}, u32[]{:S(2)}) async-start(bf16[64,32,512]{2,1,0:T(8,128)(2,1)} %bitcast), calls=%async_computation.1 | async-start | bytes 4194304 | tf_op jit(solution)/shard_map/all_to_all | solution.py:182
  45.8 64.0 %collective-permute-start.7 = (bf16[1024,256]{1,0:T(8,128)(2,1)S(1)}, bf16[1024,256]{1,0:T(8,128)(2,1)S(1)}, u32[]{:S(2)}, u32[]{:S(2)}) collective-permute-start(bf16[1024,256]{1,0:T(8,128)(2,1)S(1)} %bitcast.16), channel_id=1, source_target_pairs={{0,2},{1,3},{2,4},{3,5},{4,6},{5,7},{6,0},{7,1},{8,10},{9,11},{10,... | collective-permute-start | bytes 1572872 | tf_op jit(solution)/shard_map/ppermute | solution.py:84
  48.9 62.8 %collective-permute-start.8 = (bf16[1024,256]{1,0:T(8,128)(2,1)S(1)}, bf16[1024,256]{1,0:T(8,128)(2,1)S(1)}, u32[]{:S(2)}, u32[]{:S(2)}) collective-permute-start(bf16[1024,256]{1,0:T(8,128)(2,1)S(1)} %bitcast.17), channel_id=1, source_target_pairs={{0,6},{1,7},{2,0},{3,1},{4,2},{5,3},{6,4},{7,5},{8,14},{9,15},{10,... | collective-permute-start | bytes 1572872 | tf_op jit(solution)/shard_map/ppermute | solution.py:84
  52.3 61.9 %collective-permute-start.9 = (bf16[1024,256]{1,0:T(8,128)(2,1)S(1)}, bf16[1024,256]{1,0:T(8,128)(2,1)S(1)}, u32[]{:S(2)}, u32[]{:S(2)}) collective-permute-start(bf16[1024,256]{1,0:T(8,128)(2,1)S(1)} %bitcast.18), channel_id=1, source_target_pairs={{0,4},{1,5},{2,6},{3,7},{4,0},{5,1},{6,2},{7,3},{8,12},{9,13},{10,... | collective-permute-start | bytes 1572872 | tf_op jit(solution)/shard_map/ppermute | solution.py:84
  95.5 20.6 %copy-start.17 = (s32[4]{0:T(128)S(1)}, s32[4]{0:T(128)}, u32[]{:S(2)}) copy-start(s32[4]{0:T(128)} %constant.94) | copy-start | bytes 52
  95.5 69.8 %all-to-all-start.2 = ((bf16[64,32,256]{2,1,0:T(8,128)(2,1)}), bf16[64,32,256]{2,1,0:T(8,128)(2,1)}, u32[]{:S(2)}, u32[]{:S(2)}) async-start(bf16[64,32,256]{2,1,0:T(8,128)(2,1)} %bitcast.6), calls=%async_computation.2 | async-start | bytes 2097152 | tf_op jit(solution)/shard_map/all_to_all | solution.py:187
  104.6 12.2 %collective-permute-start.10 = (bf16[1024,256]{1,0:T(8,128)(2,1)S(1)}, bf16[1024,256]{1,0:T(8,128)(2,1)S(1)}, u32[]{:S(2)}, u32[]{:S(2)}) collective-permute-start(bf16[1024,256]{1,0:T(8,128)(2,1)S(1)} %bitcast.19), channel_id=1, source_target_pairs={{0,1},{1,0},{2,3},{3,2},{4,5},{5,4},{6,7},{7,6},{8,9},{9,8},{10,11... | collective-permute-start | bytes 1572872 | tf_op jit(solution)/shard_map/ppermute | solution.py:87
  109.8 11.4 %copy-start.2 = (bf16[1024,256]{1,0:T(8,128)(2,1)}, bf16[1024,256]{1,0:T(8,128)(2,1)S(1)}, u32[]{:S(2)}) copy-start(bf16[1024,256]{1,0:T(8,128)(2,1)S(1)} %collective-permute-done.7.refs_1_) | copy-start | bytes 1572868
  109.8 7.0 %collective-permute-start.11 = (bf16[1024,256]{1,0:T(8,128)(2,1)S(1)}, bf16[1024,256]{1,0:T(8,128)(2,1)S(1)}, u32[]{:S(2)}, u32[]{:S(2)}) collective-permute-start(bf16[1024,256]{1,0:T(8,128)(2,1)S(1)} %collective-permute-done.7.refs_1_), channel_id=1, source_target_pairs={{0,1},{1,0},{2,3},{3,2},{4,5},{5,4},{6,7},{7,6},{8,9},{9,8},{10,11... | collective-permute-start | bytes 1572872 | tf_op jit(solution)/shard_map/ppermute | solution.py:87
  111.7 9.5 %copy-start.3 = (bf16[1024,256]{1,0:T(8,128)(2,1)}, bf16[1024,256]{1,0:T(8,128)(2,1)S(1)}, u32[]{:S(2)}) copy-start(bf16[1024,256]{1,0:T(8,128)(2,1)S(1)} %collective-permute-done.8.refs_2_) | copy-start | bytes 1572868
  111.8 5.0 %collective-permute-start.12 = (bf16[1024,256]{1,0:T(8,128)(2,1)S(1)}, bf16[1024,256]{1,0:T(8,128)(2,1)}, u32[]{:S(2)}, u32[]{:S(2)}) collective-permute-start(bf16[1024,256]{1,0:T(8,128)(2,1)S(1)} %collective-permute-done.8.refs_2_), channel_id=1, source_target_pairs={{0,1},{1,0},{2,3},{3,2},{4,5},{5,4},{6,7},{7,6},{8,9},{9,8},{10,11... | collective-permute-start | bytes 1572872 | tf_op jit(solution)/shard_map/ppermute | solution.py:87
  114.2 7.1 %copy-start.4 = (bf16[1024,256]{1,0:T(8,128)(2,1)}, bf16[1024,256]{1,0:T(8,128)(2,1)S(1)}, u32[]{:S(2)}) copy-start(bf16[1024,256]{1,0:T(8,128)(2,1)S(1)} %collective-permute-done.9.refs_3_) | copy-start | bytes 1572868
  114.2 3.9 %collective-permute-start.13 = (bf16[1024,256]{1,0:T(8,128)(2,1)S(1)}, bf16[1024,256]{1,0:T(8,128)(2,1)}, u32[]{:S(2)}, u32[]{:S(2)}) collective-permute-start(bf16[1024,256]{1,0:T(8,128)(2,1)S(1)} %collective-permute-done.9.refs_3_), channel_id=1, source_target_pairs={{0,1},{1,0},{2,3},{3,2},{4,5},{5,4},{6,7},{7,6},{8,9},{9,8},{10,11... | collective-permute-start | bytes 1572872 | tf_op jit(solution)/shard_map/ppermute | solution.py:87
  116.8 4.5 %copy-start.5 = (bf16[1024,256]{1,0:T(8,128)(2,1)}, bf16[1024,256]{1,0:T(8,128)(2,1)S(1)}, u32[]{:S(2)}) copy-start(bf16[1024,256]{1,0:T(8,128)(2,1)S(1)} %collective-permute-done.10.refs_4_) | copy-start | bytes 1572868
  116.8 4.5 %copy-start.6 = (bf16[1024,256]{1,0:T(8,128)(2,1)}, bf16[1024,256]{1,0:T(8,128)(2,1)S(1)}, u32[]{:S(2)}) copy-start(bf16[1024,256]{1,0:T(8,128)(2,1)S(1)} %collective-permute-done.11.refs_5_) | copy-start | bytes 1572868
  121.3 0.8 copy-start.7
  129.3 16.6 %collective-permute-start.14 = (bf16[1024,256]{1,0:T(8,128)(2,1)}, bf16[1024,256]{1,0:T(8,128)(2,1)S(1)}, u32[]{:S(2)}, u32[]{:S(2)}) collective-permute-start(bf16[1024,256]{1,0:T(8,128)(2,1)} %shard_map.111.refs_0_), channel_id=1, source_target_pairs={{0,2},{1,3},{2,4},{3,5},{4,6},{5,7},{6,0},{7,1},{8,10},{9,11},{10,... | collective-permute-start | bytes 1572872 | tf_op jit(solution)/shard_map/ppermute | solution.py:84
  132.4 16.4 %collective-permute-start.15 = (bf16[1024,256]{1,0:T(8,128)(2,1)}, bf16[1024,256]{1,0:T(8,128)(2,1)S(1)}, u32[]{:S(2)}, u32[]{:S(2)}) collective-permute-start(bf16[1024,256]{1,0:T(8,128)(2,1)} %shard_map.111.refs_0_), channel_id=1, source_target_pairs={{0,6},{1,7},{2,0},{3,1},{4,2},{5,3},{6,4},{7,5},{8,14},{9,15},{10,... | collective-permute-start | bytes 1572872 | tf_op jit(solution)/shard_map/ppermute | solution.py:84
  135.8 25.6 %collective-permute-start.16 = (bf16[1024,256]{1,0:T(8,128)(2,1)}, bf16[1024,256]{1,0:T(8,128)(2,1)S(1)}, u32[]{:S(2)}, u32[]{:S(2)}) collective-permute-start(bf16[1024,256]{1,0:T(8,128)(2,1)} %shard_map.111.refs_0_), channel_id=1, source_target_pairs={{0,4},{1,5},{2,6},{3,7},{4,0},{5,1},{6,2},{7,3},{8,12},{9,13},{10,... | collective-permute-start | bytes 1572872 | tf_op jit(solution)/shard_map/ppermute | solution.py:84
  139.2 24.1 %collective-permute-start.17 = (bf16[1024,256]{1,0:T(8,128)(2,1)}, bf16[1024,256]{1,0:T(8,128)(2,1)S(1)}, u32[]{:S(2)}, u32[]{:S(2)}) collective-permute-start(bf16[1024,256]{1,0:T(8,128)(2,1)} %shard_map.111.refs_0_), channel_id=1, source_target_pairs={{0,1},{1,0},{2,3},{3,2},{4,5},{5,4},{6,7},{7,6},{8,9},{9,8},{10,11... | collective-permute-start | bytes 1572872 | tf_op jit(solution)/shard_map/ppermute | solution.py:87
  145.9 19.4 %copy-start.10 = (bf16[1024,256]{1,0:T(8,128)(2,1)}, bf16[1024,256]{1,0:T(8,128)(2,1)S(1)}, u32[]{:S(2)}) copy-start(bf16[1024,256]{1,0:T(8,128)(2,1)S(1)} %collective-permute-done.14.refs_1_) | copy-start | bytes 1572868
  145.9 17.4 %collective-permute-start.18 = (bf16[1024,256]{1,0:T(8,128)(2,1)S(1)}, bf16[1024,256]{1,0:T(8,128)(2,1)S(1)}, u32[]{:S(2)}, u32[]{:S(2)}) collective-permute-start(bf16[1024,256]{1,0:T(8,128)(2,1)S(1)} %collective-permute-done.14.refs_1_), channel_id=1, source_target_pairs={{0,1},{1,0},{2,3},{3,2},{4,5},{5,4},{6,7},{7,6},{8,9},{9,8},{10,11... | collective-permute-start | bytes 1572872 | tf_op jit(solution)/shard_map/ppermute | solution.py:87
  148.8 16.5 %copy-start.11 = (bf16[1024,256]{1,0:T(8,128)(2,1)}, bf16[1024,256]{1,0:T(8,128)(2,1)S(1)}, u32[]{:S(2)}) copy-start(bf16[1024,256]{1,0:T(8,128)(2,1)S(1)} %collective-permute-done.15.refs_2_) | copy-start | bytes 1572868
  148.9 14.5 %collective-permute-start.19 = (bf16[1024,256]{1,0:T(8,128)(2,1)S(1)}, bf16[1024,256]{1,0:T(8,128)(2,1)S(1)}, u32[]{:S(2)}, u32[]{:S(2)}) collective-permute-start(bf16[1024,256]{1,0:T(8,128)(2,1)S(1)} %collective-permute-done.15.refs_2_), channel_id=1, source_target_pairs={{0,1},{1,0},{2,3},{3,2},{4,5},{5,4},{6,7},{7,6},{8,9},{9,8},{10,11... | collective-permute-start | bytes 1572872 | tf_op jit(solution)/shard_map/ppermute | solution.py:87
  161.4 4.0 %copy-start.12 = (bf16[1024,256]{1,0:T(8,128)(2,1)}, bf16[1024,256]{1,0:T(8,128)(2,1)S(1)}, u32[]{:S(2)}) copy-start(bf16[1024,256]{1,0:T(8,128)(2,1)S(1)} %collective-permute-done.16.refs_3_) | copy-start | bytes 1572868
  161.4 3.9 %collective-permute-start.20 = (bf16[1024,256]{1,0:T(8,128)(2,1)S(1)}, bf16[1024,256]{1,0:T(8,128)(2,1)}, u32[]{:S(2)}, u32[]{:S(2)}) collective-permute-start(bf16[1024,256]{1,0:T(8,128)(2,1)S(1)} %collective-permute-done.16.refs_3_), channel_id=1, source_target_pairs={{0,1},{1,0},{2,3},{3,2},{4,5},{5,4},{6,7},{7,6},{8,9},{9,8},{10,11... | collective-permute-start | bytes 1572872 | tf_op jit(solution)/shard_map/ppermute | solution.py:87
  163.3 2.0 copy-start.13
  163.4 2.0 copy-start.14
  163.4 2.0 copy-start.15
  171.4 37.6 %all-to-all-start.3 = ((bf16[32,32,256]{2,1,0:T(8,128)(2,1)}), bf16[32,32,256]{2,1,0:T(8,128)(2,1)S(1)}, u32[]{:S(2)}, u32[]{:S(2)}) async-start(bf16[32,32,256]{2,1,0:T(8,128)(2,1)} %bitcast.22), calls=%async_computation.3 | async-start | bytes 1048576 | tf_op jit(solution)/shard_map/all_to_all | solution.py:193
  180.9 4.1 %copy-start.16 = (f32[320,2]{0,1:T(2,128)S(1)}, f32[320,2]{0,1:T(2,128)}, u32[]{:S(2)}) copy-start(f32[320,2]{0,1:T(2,128)} %param.14) | copy-start | bytes 7684
  182.4 15.1 %collective-permute-start = (bf16[256,256]{1,0:T(8,128)(2,1)S(1)}, bf16[256,256]{1,0:T(8,128)(2,1)S(1)}, u32[]{:S(2)}, u32[]{:S(2)}) collective-permute-start(bf16[256,256]{1,0:T(8,128)(2,1)S(1)} %get-tuple-element.24), channel_id=1, source_target_pairs={{0,1},{1,2},{2,3},{3,4},{4,5},{5,6},{6,7},{7,0},{8,9},{9,10},{10,1... | collective-permute-start | bytes 393224 | tf_op jit(solution)/shard_map/ppermute | solution.py:118
  183.1 17.2 %collective-permute-start.1 = (bf16[256,256]{1,0:T(8,128)(2,1)S(1)}, bf16[256,256]{1,0:T(8,128)(2,1)S(1)}, u32[]{:S(2)}, u32[]{:S(2)}) collective-permute-start(bf16[256,256]{1,0:T(8,128)(2,1)S(1)} %get-tuple-element.23), channel_id=1, source_target_pairs={{0,2},{1,3},{2,4},{3,5},{4,6},{5,7},{6,0},{7,1},{8,10},{9,11},{10,... | collective-permute-start | bytes 393224 | tf_op jit(solution)/shard_map/ppermute | solution.py:118
  185.1 18.5 %collective-permute-start.2 = (bf16[256,256]{1,0:T(8,128)(2,1)S(1)}, bf16[256,256]{1,0:T(8,128)(2,1)S(1)}, u32[]{:S(2)}, u32[]{:S(2)}) collective-permute-start(bf16[256,256]{1,0:T(8,128)(2,1)S(1)} %get-tuple-element.22), channel_id=1, source_target_pairs={{0,3},{1,4},{2,5},{3,6},{4,7},{5,0},{6,1},{7,2},{8,11},{9,12},{10,... | collective-permute-start | bytes 393224 | tf_op jit(solution)/shard_map/ppermute | solution.py:118
  191.4 12.2 %collective-permute-start.3 = (bf16[256,256]{1,0:T(8,128)(2,1)S(1)}, bf16[256,256]{1,0:T(8,128)(2,1)S(1)}, u32[]{:S(2)}, u32[]{:S(2)}) collective-permute-start(bf16[256,256]{1,0:T(8,128)(2,1)S(1)} %get-tuple-element.21), channel_id=1, source_target_pairs={{0,4},{1,5},{2,6},{3,7},{4,0},{5,1},{6,2},{7,3},{8,12},{9,13},{10,... | collective-permute-start | bytes 393224 | tf_op jit(solution)/shard_map/ppermute | solution.py:118
  193.4 10.2 %collective-permute-start.4 = (bf16[256,256]{1,0:T(8,128)(2,1)S(1)}, bf16[256,256]{1,0:T(8,128)(2,1)S(1)}, u32[]{:S(2)}, u32[]{:S(2)}) collective-permute-start(bf16[256,256]{1,0:T(8,128)(2,1)S(1)} %get-tuple-element.20), channel_id=1, source_target_pairs={{0,5},{1,6},{2,7},{3,0},{4,1},{5,2},{6,3},{7,4},{8,13},{9,14},{10,... | collective-permute-start | bytes 393224 | tf_op jit(solution)/shard_map/ppermute | solution.py:118
  197.5 6.1 %collective-permute-start.5 = (bf16[256,256]{1,0:T(8,128)(2,1)S(1)}, bf16[256,256]{1,0:T(8,128)(2,1)S(1)}, u32[]{:S(2)}, u32[]{:S(2)}) collective-permute-start(bf16[256,256]{1,0:T(8,128)(2,1)S(1)} %get-tuple-element.19), channel_id=1, source_target_pairs={{0,6},{1,7},{2,0},{3,1},{4,2},{5,3},{6,4},{7,5},{8,14},{9,15},{10,... | collective-permute-start | bytes 393224 | tf_op jit(solution)/shard_map/ppermute | solution.py:118
  200.3 5.9 %collective-permute-start.6 = (bf16[256,256]{1,0:T(8,128)(2,1)S(1)}, bf16[256,256]{1,0:T(8,128)(2,1)S(1)}, u32[]{:S(2)}, u32[]{:S(2)}) collective-permute-start(bf16[256,256]{1,0:T(8,128)(2,1)S(1)} %get-tuple-element.18), channel_id=1, source_target_pairs={{0,7},{1,0},{2,1},{3,2},{4,3},{5,4},{6,5},{7,6},{8,15},{9,8},{10,9... | collective-permute-start | bytes 393224 | tf_op jit(solution)/shard_map/ppermute | solution.py:118

commit v4 on v3

v4 whole, which is shorter than its diff:
```python
import functools

import jax
import jax.numpy as jnp
from jax import lax
from jax.experimental import pallas as pl
from jax.experimental.pallas import tpu as pltpu
from jax.sharding import PartitionSpec as P


SLOTS = 32
LANES = 128
STEPS = 2
BF = jnp.bfloat16
F32 = jnp.float32


def block_of(piece):
    if isinstance(piece, tuple):
        return jnp.where(pl.program_id(0) == 0, piece[0][...], piece[1][...])
    return piece[...]


def paired(refs, layout):
    refs = list(refs)
    return [
        (refs.pop(0), refs.pop(0)) if isinstance(piece, tuple) else refs.pop(0) for piece in layout
    ]


def flat(pieces):
    return [r for piece in pieces for r in (piece if isinstance(piece, tuple) else (piece,))]


def pieces_dot(sender, pieces, weights):
    acc = None
    for k, piece in enumerate(pieces):
        block = block_of(piece)
        at = pl.multiple_of(sender[k] * block.shape[1], block.shape[1])
        part = jnp.dot(block, weights[pl.ds(at, block.shape[1]), :], preferred_element_type=F32)
        acc = part if acc is None else acc + part
    return acc


def scale_kernel(layout, *refs):
    pieces, out = paired(refs[:-1], layout), refs[-1]
    squares, total = None, 0
    for piece in pieces:
        values = block_of(piece).astype(F32)
        total += values.shape[1]
        part = jnp.sum(values * values, axis=-1, keepdims=True)
        squares = part if squares is None else squares + part
    out[...] = jnp.broadcast_to(lax.rsqrt(squares / total + 1e-06), out.shape)


def row_specs(pieces, block):
    return [
        pl.BlockSpec((block, r.shape[1]), lambda i, *_, half=r.shape[0] == block: (0 if half else i, 0))
        for r in flat(pieces)
    ]


def row_scale(pieces):
    count = pieces[0].shape[0]
    return pl.pallas_call(
        functools.partial(scale_kernel, pieces),
        name="row_scale",
        grid=(STEPS,),
        in_specs=row_specs(pieces, count // STEPS),
        out_specs=pl.BlockSpec((count // STEPS, LANES), lambda i: (i, 0)),
        out_shape=jax.ShapeDtypeStruct((count, LANES), F32),
        compiler_params=pltpu.CompilerParams(vmem_limit_bytes=12 * 1024 * 1024),
    )(*flat(pieces))


def hidden_kernel(layout, sender, *refs):
    scale, gate_up, out = refs[-3:]
    half = out.shape[1]
    acc = pieces_dot(sender, paired(refs[:-3], layout), gate_up) * scale[:, :1]
    gate, up = acc[:, :half], acc[:, half:]
    out[...] = (gate / (1.0 + jnp.exp(-gate)) * up).astype(out.dtype)


def out_kernel(layout, sender, *refs):
    down, out = refs[-2:]
    out[...] = pieces_dot(sender, paired(refs[:-2], layout), down).astype(out.dtype)


def row_call(kernel, sender, pieces, others, weights, out_width):
    count = pieces[0].shape[0]
    block = count // STEPS
    return pl.pallas_call(
        functools.partial(kernel, pieces),
        grid_spec=pltpu.PrefetchScalarGridSpec(
            num_scalar_prefetch=1,
            grid=(STEPS,),
            in_specs=row_specs([*pieces, *others], block)
            + [pl.BlockSpec(weights.shape, lambda i, at: (0, 0))],
            out_specs=pl.BlockSpec((block, out_width), lambda i, at: (i, 0)),
        ),
        out_shape=jax.ShapeDtypeStruct((count, out_width), BF),
    )(sender, *flat(pieces), *others, weights)


def shift(value, axis, by):
    count = lax.axis_size(axis)
    return lax.ppermute(value, axis, [(i, (i + by) % count) for i in range(count)])


def partner(value, axis):
    return lax.ppermute(value, axis, [(i, i ^ 1) for i in range(lax.axis_size(axis))])


def gather_pieces(piece, axis):
    half = piece.shape[0] // 2
    right, left = shift(piece, axis, 2), shift(piece, axis, -2)
    other = partner(piece, axis)
    far = (shift(right[:half], axis, 2), shift(left[half:], axis, -2))
    return [
        piece,
        right,
        left,
        far,
        other,
        partner(right, axis),
        partner(left, axis),
        tuple(partner(value, axis) for value in far),
    ]


def piece_senders(axis):
    count, here = lax.axis_size(axis), lax.axis_index(axis)
    other = here + 1 - 2 * (here % 2)
    return jnp.stack([(at - by) % count for at in (here, other) for by in (0, 2, -2, 4)]).astype(
        jnp.int32
    )


def place_kernel(at, *refs):
    pieces, out = refs[:-1], refs[-1]
    for k, piece in enumerate(pieces):

        @pl.when(pl.program_id(0) // 2 == k)
        def _(piece=piece):
            out[...] = piece[pl.program_id(0) % 2]


def exchange_units(array, axis):
    count, here = lax.axis_size(axis), lax.axis_index(axis)
    chips, chip, core = count // 2, here // 2, here % 2
    rows, cols = array.shape[0] // count, array.shape[1]
    blocks = array.reshape(chips, 2, rows, cols)
    mine = lax.dynamic_slice_in_dim(blocks, core, 1, 1)
    theirs = partner(lax.dynamic_slice_in_dim(blocks, 1 - core, 1, 1), axis)
    both = jnp.concatenate([mine, theirs], axis=1)
    pieces = []
    for k in range(chips):
        block = lax.dynamic_slice_in_dim(both, (chip + k) % chips, 1, 0)[0]
        pieces.append(shift(block, axis, 2 * k) if k else block)
    places = [
        2 * ((chip - k) % chips) + side for k in range(chips) for side in (core, 1 - core)
    ]
    return pl.pallas_call(
        place_kernel,
        name="place",
        grid_spec=pltpu.PrefetchScalarGridSpec(
            num_scalar_prefetch=1,
            grid=(count,),
            in_specs=[pl.BlockSpec((2, rows, cols), lambda k, at: (0, 0, 0))] * chips,
            out_specs=pl.BlockSpec((rows, cols), lambda k, at: (0, at[k])),
        ),
        out_shape=jax.ShapeDtypeStruct((rows, count * cols), array.dtype),
        compiler_params=pltpu.CompilerParams(vmem_limit_bytes=8 * 1024 * 1024),
    )(jnp.stack(places).astype(jnp.int32), *pieces)


def after(value, *others):
    return lax.optimization_barrier((value, *others))[0]


def both_groups(array):
    copies = jnp.broadcast_to(array[None], (lax.axis_size("gr"), *array.shape))
    return copies.reshape(-1, *array.shape[1:])


def body(prompt, norm_gain, gate_weight, up_weight, down_weight, routes, route_weight):
    experts, _, cols = gate_weight.shape
    tok_count, width = prompt.shape
    slots_all = experts * SLOTS

    expert_ids = jnp.arange(experts, dtype=jnp.int32)[None, :]
    first = routes[:, 0:1] == expert_ids
    second = routes[:, 1:2] == expert_ids
    named = (first | second).astype(BF)
    order = jnp.arange(tok_count, dtype=jnp.int32)
    before = (order[None, :] < order[:, None]).astype(BF)
    earlier = jnp.dot(before, named, preferred_element_type=F32)
    slot_first = jnp.sum(jnp.where(first, earlier, 0.0), axis=1).astype(jnp.int32)
    slot_second = jnp.sum(jnp.where(second, earlier, 0.0), axis=1).astype(jnp.int32)
    target_first = routes[:, 0] * SLOTS + slot_first
    target_second = routes[:, 1] * SLOTS + slot_second
    slot_ids = jnp.arange(slots_all, dtype=jnp.int32)[None, :]
    select_first = (target_first[:, None] == slot_ids).astype(BF)
    select_second = (target_second[:, None] == slot_ids).astype(BF)
    weighted = jnp.where(
        target_first[:, None] == slot_ids,
        route_weight[:, 0:1],
        jnp.where(target_second[:, None] == slot_ids, route_weight[:, 1:2], 0.0),
    ).astype(BF)
    outbound = jnp.einsum(
        "ts,td->sd", select_first + select_second, prompt, preferred_element_type=F32
    ).astype(BF)
    moved = lax.all_to_all(
        outbound.reshape(experts, SLOTS, width), "fs", split_axis=0, concat_axis=0, tiled=True
    )
    arrived = gather_pieces(moved.reshape(slots_all, width), "tp")
    scale = row_scale(arrived)
    sender = piece_senders("tp")

    gain = norm_gain[None, :, None]
    gate_up = jnp.concatenate(
        [(gate_weight * gain).astype(BF), (up_weight * gain).astype(BF)], axis=2
    )
    gate_up = both_groups(gate_up)
    gate_up = after(gate_up, moved)
    gate_up = lax.all_to_all(gate_up, ("gr", "fs"), split_axis=0, concat_axis=0, tiled=True)
    gate_up = gate_up.reshape(-1, 2 * cols)
    gate_new, up_new = gate_up[None, :, :cols], gate_up[None, :, cols:]

    down = both_groups(down_weight.astype(BF))
    down = after(down, gate_up)
    down = lax.all_to_all(down, ("gr", "fs"), split_axis=0, concat_axis=0, tiled=True)
    down = down.reshape(-1, cols)

    hidden = row_call(hidden_kernel, sender, arrived, [scale], gate_up, cols)
    hidden_all = gather_pieces(hidden, "tp")
    summed = row_call(out_kernel, sender, hidden_all, [], down, cols)
    returned = lax.all_to_all(
        summed.reshape(experts, SLOTS, width), "fs", split_axis=0, concat_axis=0, tiled=True
    )
    returned = returned.reshape(slots_all, width)
    down_new = exchange_units(down, "tp")

    mixed = jnp.dot(weighted, returned, preferred_element_type=F32)
    return (gate_new, up_new, down_new[None], mixed.astype(BF))


def solution(mesh):
    return jax.shard_map(
        body,
        mesh=mesh,
        in_specs=(
            P(("gr", "fs"), "tp"),
            P(("gr", "fs")),
            P(None, ("gr", "fs"), "tp"),
            P(None, ("gr", "fs"), "tp"),
            P(None, ("gr", "fs"), "tp"),
            P(("gr", "fs"), None),
            P(("gr", "fs"), None),
        ),
        out_specs=(
            P("fs", None, "tp"),
            P("fs", None, "tp"),
            P("fs", "tp", None),
            P(("gr", "fs"), "tp"),
        ),
        check_vma=False,
    )
```

time: 212 us -> 229 us (1.080)
  waiting for transfers between devices: 61.9 us -> 80.5 us
    ppermute x15 -> x11, starting transfers between devices: 49.7 us -> 33.3 us  [partner(): lax.ppermute(value, axis, [(i, i ^ 1) for i in range(lax.axis_size(axis))])]
    ppermute x6 -> x11, starting transfers between devices: 19.9 us -> 34.7 us  [shift(): lax.ppermute(value, axis, [(i, (i + by) % count) for i in range(count)])]
    ppermute x6 -> x11, waiting for transfers between devices: 3.83 us -> 17.1 us  [shift(): lax.ppermute(value, axis, [(i, (i + by) % count) for i in range(count)])]
    all_to_all x1, waiting for transfers between devices: 37.4 us -> 47.5 us  [body(): lax.all_to_all(gate_up, ('gr', 'fs'), split_axis=0, concat_axis=0, tiled=...]
    ppermute x15 -> x11, waiting for transfers between devices: 5.92 us -> 1.1 us  [partner(): lax.ppermute(value, axis, [(i, i ^ 1) for i in range(lax.axis_size(axis))])]
  transfers between devices with their start and end apart: 25 -> 26, of which waited for: 6 -> 8; matrix products, arithmetic and copies ran while one was open for 4% -> 3% of each run, Pallas kernels for 6% -> 8%
where the time goes in v4:
time: 229 us; the launch traced here: 228 us
  starting transfers between devices  111 us (48%)
  waiting for transfers between devices  80.5 us (35%)
  Pallas kernels  18 us (8%)
  local copies, waits for them, and re-layouts  10.1 us (4%)
  matrix products  3.87 us (2%)
  other arithmetic  2.6 us (1%)
    all_to_all x1, waiting for transfers between devices, body(): lax.all_to_all(gate_up, ('gr', 'fs'), split_axis=0, concat_axis=0, tiled=...  47.5 us
    ppermute x11, starting transfers between devices, shift(): lax.ppermute(value, axis, [(i, (i + by) % count) for i in range(count)])  34.7 us
    ppermute x11, starting transfers between devices, partner(): lax.ppermute(value, axis, [(i, i ^ 1) for i in range(lax.axis_size(axis))])  33.3 us
    ppermute x11, waiting for transfers between devices, shift(): lax.ppermute(value, axis, [(i, (i + by) % count) for i in range(count)])  17.1 us
    all_to_all x1, waiting for transfers between devices, body(): lax.all_to_all(outbound.reshape(experts, SLOTS, width), 'fs', split_axis=...  14.8 us
    all_to_all x1, starting transfers between devices, body(): lax.all_to_all(outbound.reshape(experts, SLOTS, width), 'fs', split_axis=...  13.5 us
    pallas_call x2, Pallas kernels, row_call(): pl.pallas_call(functools.partial(kernel, pieces), grid_spec=pltpu.Prefetc...  11.9 us
    all_to_all x1, starting transfers between devices, body(): lax.all_to_all(gate_up, ('gr', 'fs'), split_axis=0, concat_axis=0, tiled=...  11.3 us
  transfers between devices with their start and end apart: 26, of which 8 were waited for; matrix products, arithmetic and copies ran while one was open for 3% of the time, Pallas kernels for 8%

profile of v4, /device:TPU:1, one launch (start us, length us, event | category | flops | bytes accessed | tf_op | source)
XLA Modules:
  0.0 227.7 jit_solution(4196385568093224701)
XLA Ops:
  0.6 0.8 slice_reduce_fusion.3
  1.7 0.8 add_reduce_fusion.1
  2.5 1.4 convolution_convert_fusion
  3.9 13.5 %all-to-all-start = ((bf16[32,32,256]{2,1,0:T(8,128)(2,1)}), bf16[32,32,256]{2,1,0:T(8,128)(2,1)S(1)}, u32[]{:S(2)}, u32[]{:S(2)}) async-start(bf16[32,32,256]{2,1,0:T(8,128)(2,1)} %bitcast.1), calls=%async_computation | async-start | bytes 1048576 | tf_op jit(solution)/shard_map/all_to_all | solution.py:213
  17.8 14.8 %all-to-all-done = bf16[32,32,256]{2,1,0:T(8,128)(2,1)S(1)} async-done(((bf16[32,32,256]{2,1,0:T(8,128)(2,1)}), bf16[32,32,256]{2,1,0:T(8,128)(2,1)S(1)}, u32[]{:S(2)}, u32[]{:S(2)}) %all-to-all-start) | async-done | bytes 524320 | tf_op jit(solution)/shard_map/all_to_all | solution.py:213
  32.6 1.7 broadcast_in_dim.59
  34.3 11.3 %all-to-all-start.1 = ((bf16[64,32,512]{2,1,0:T(8,128)(2,1)}), bf16[64,32,512]{2,1,0:T(8,128)(2,1)S(1)}, u32[]{:S(2)}, u32[]{:S(2)}) async-start(bf16[64,32,512]{2,1,0:T(8,128)(2,1)} %bitcast.47), calls=%async_computation.1 | async-start | bytes 4194304 | tf_op jit(solution)/shard_map/all_to_all | solution.py:226
  45.6 1.3 convert_element_type.61
  46.9 47.5 %all-to-all-done.1 = bf16[64,32,512]{2,1,0:T(8,128)(2,1)S(1)} async-done(((bf16[64,32,512]{2,1,0:T(8,128)(2,1)}), bf16[64,32,512]{2,1,0:T(8,128)(2,1)S(1)}, u32[]{:S(2)}, u32[]{:S(2)}) %all-to-all-start.1) | async-done | bytes 2097184 | tf_op jit(solution)/shard_map/all_to_all | solution.py:226
  94.4 1.2 broadcast_in_dim.63
  96.1 8.9 %all-to-all-start.2 = ((bf16[64,32,256]{2,1,0:T(8,128)(2,1)}), bf16[64,32,256]{2,1,0:T(8,128)(2,1)}, u32[]{:S(2)}, u32[]{:S(2)}) async-start(bf16[64,32,256]{2,1,0:T(8,128)(2,1)} %bitcast.48), calls=%async_computation.2 | async-start | bytes 2097152 | tf_op jit(solution)/shard_map/all_to_all | solution.py:232
  105.0 3.1 %collective-permute-start.4 = (bf16[1024,256]{1,0:T(8,128)(2,1)S(1)}, bf16[1024,256]{1,0:T(8,128)(2,1)S(1)}, u32[]{:S(2)}, u32[]{:S(2)}) collective-permute-start(bf16[1024,256]{1,0:T(8,128)(2,1)S(1)} %bitcast.40), channel_id=1, source_target_pairs={{0,2},{1,3},{2,4},{3,5},{4,6},{5,7},{6,0},{7,1},{8,10},{9,11},{10,... | collective-permute-start | bytes 1572872 | tf_op jit(solution)/shard_map/ppermute | solution.py:107
  108.2 3.4 %collective-permute-start.5 = (bf16[1024,256]{1,0:T(8,128)(2,1)S(1)}, bf16[1024,256]{1,0:T(8,128)(2,1)S(1)}, u32[]{:S(2)}, u32[]{:S(2)}) collective-permute-start(bf16[1024,256]{1,0:T(8,128)(2,1)S(1)} %bitcast.41), channel_id=1, source_target_pairs={{0,6},{1,7},{2,0},{3,1},{4,2},{5,3},{6,4},{7,5},{8,14},{9,15},{10,... | collective-permute-start | bytes 1572872 | tf_op jit(solution)/shard_map/ppermute | solution.py:107
  111.5 5.8 %collective-permute-start.8 = (bf16[1024,256]{1,0:T(8,128)(2,1)S(1)}, bf16[1024,256]{1,0:T(8,128)(2,1)S(1)}, u32[]{:S(2)}, u32[]{:S(2)}) collective-permute-start(bf16[1024,256]{1,0:T(8,128)(2,1)S(1)} %bitcast.42), channel_id=1, source_target_pairs={{0,1},{1,0},{2,3},{3,2},{4,5},{5,4},{6,7},{7,6},{8,9},{9,8},{10,11... | collective-permute-start | bytes 1572872 | tf_op jit(solution)/shard_map/ppermute | solution.py:111
  117.3 1.1 collective-permute-done.4.refs_1_
  118.4 1.9 collective-permute-start.6
  120.4 4.6 %collective-permute-start.7 = (bf16[512,256]{1,0:T(8,128)(2,1)S(1)}, bf16[512,256]{1,0:T(8,128)(2,1)}, u32[]{:S(2)}, u32[]{:S(2)}) collective-permute-start(bf16[512,256]{1,0:T(8,128)(2,1)S(1)} %slice.45), channel_id=1, source_target_pairs={{0,6},{1,7},{2,0},{3,1},{4,2},{5,3},{6,4},{7,5},{8,14},{9,15},{10,... | collective-permute-start | bytes 786440 | tf_op jit(solution)/shard_map/ppermute | solution.py:107
  125.0 6.5 %collective-permute-start.10 = (bf16[1024,256]{1,0:T(8,128)(2,1)S(1)}, bf16[1024,256]{1,0:T(8,128)(2,1)S(1)}, u32[]{:S(2)}, u32[]{:S(2)}) collective-permute-start(bf16[1024,256]{1,0:T(8,128)(2,1)S(1)} %collective-permute-done.5.refs_2_), channel_id=1, source_target_pairs={{0,1},{1,0},{2,3},{3,2},{4,5},{5,4},{6,7},{7,6},{8,9},{9,8},{10,11... | collective-permute-start | bytes 1572872 | tf_op jit(solution)/shard_map/ppermute | solution.py:111
  131.5 1.9 collective-permute-start.9
  133.5 2.4 %collective-permute-start.11 = (bf16[512,256]{1,0:T(8,128)(2,1)}, bf16[512,256]{1,0:T(8,128)(2,1)}, u32[]{:S(2)}, u32[]{:S(2)}) collective-permute-start(bf16[512,256]{1,0:T(8,128)(2,1)} %collective-permute-done.6.refs_3_), channel_id=1, source_target_pairs={{0,1},{1,0},{2,3},{3,2},{4,5},{5,4},{6,7},{7,6},{8,9},{9,8},{10,11... | collective-permute-start | bytes 786440 | tf_op jit(solution)/shard_map/ppermute | solution.py:111
  135.9 1.9 collective-permute-start.12
  138.6 1.1 collective-permute-done.12.refs_9_
  139.7 2.8 %row_scale.1.refs_10_ = f32[1024,128]{1,0:T(8,128)S(1)} custom-call(bf16[1024,256]{1,0:T(8,128)(2,1)S(1)} %bitcast.43, bf16[1024,256]{1,0:T(8,128)(2,1)S(1)} %collective-permute-done.4.refs_1_, bf16[1024,256]{1,0:T(8,128)(2,1)S(1)} %collective-permute-done.5.refs_2_, bf16[512,256]{1,0:T(8,128)(2,1)} %collective-permute-done.6.refs_3_, ...), custom_call_target="tpu_custom_call" | custom-call | tf_op jit(solution)/shard_map/row_scale/pallas_call | solution.py:65
  142.6 0.8 copy-done.7
  143.4 6.8 %shard_map.102.refs_0_ = bf16[1024,256]{1,0:T(8,128)(2,1)} custom-call(s32[8]{0:T(128)} %stack.71.sender, bf16[1024,256]{1,0:T(8,128)(2,1)} %bitcast.44, bf16[1024,256]{1,0:T(8,128)(2,1)} %copy-done.2, bf16[1024,256]{1,0:T(8,128)(2,1)} %copy-done.3, bf16[512,256]{1,0:T(8,128)(2,1)} %collective-permute-done.6.refs_3_, ...), custom_call_target="tpu_custom_call" | custom-call | tf_op jit(solution)/shard_map/pallas_call | solution.py:92
  150.1 1.9 collective-permute-start.13
  152.1 4.6 %collective-permute-start.14 = (bf16[1024,256]{1,0:T(8,128)(2,1)}, bf16[1024,256]{1,0:T(8,128)(2,1)S(1)}, u32[]{:S(2)}, u32[]{:S(2)}) collective-permute-start(bf16[1024,256]{1,0:T(8,128)(2,1)} %shard_map.102.refs_0_), channel_id=1, source_target_pairs={{0,6},{1,7},{2,0},{3,1},{4,2},{5,3},{6,4},{7,5},{8,14},{9,15},{10,... | collective-permute-start | bytes 1572872 | tf_op jit(solution)/shard_map/ppermute | solution.py:107
  156.6 2.6 %collective-permute-start.17 = (bf16[1024,256]{1,0:T(8,128)(2,1)}, bf16[1024,256]{1,0:T(8,128)(2,1)S(1)}, u32[]{:S(2)}, u32[]{:S(2)}) collective-permute-start(bf16[1024,256]{1,0:T(8,128)(2,1)} %shard_map.102.refs_0_), channel_id=1, source_target_pairs={{0,1},{1,0},{2,3},{3,2},{4,5},{5,4},{6,7},{7,6},{8,9},{9,8},{10,11... | collective-permute-start | bytes 1572872 | tf_op jit(solution)/shard_map/ppermute | solution.py:111
  159.3 7.5 %collective-permute-done.13.refs_1_ = bf16[1024,256]{1,0:T(8,128)(2,1)S(1)} collective-permute-done((bf16[1024,256]{1,0:T(8,128)(2,1)}, bf16[1024,256]{1,0:T(8,128)(2,1)S(1)}, u32[]{:S(2)}, u32[]{:S(2)}) %collective-permute-start.13) | collective-permute-done | bytes 524320 | tf_op jit(solution)/shard_map/ppermute | solution.py:107
  166.8 1.9 collective-permute-start.15
  168.8 4.6 %collective-permute-start.16 = (bf16[512,256]{1,0:T(8,128)(2,1)S(1)}, bf16[512,256]{1,0:T(8,128)(2,1)}, u32[]{:S(2)}, u32[]{:S(2)}) collective-permute-start(bf16[512,256]{1,0:T(8,128)(2,1)S(1)} %slice.47), channel_id=1, source_target_pairs={{0,6},{1,7},{2,0},{3,1},{4,2},{5,3},{6,4},{7,5},{8,14},{9,15},{10,... | collective-permute-start | bytes 786440 | tf_op jit(solution)/shard_map/ppermute | solution.py:107
  173.4 3.5 %collective-permute-start.18 = (bf16[1024,256]{1,0:T(8,128)(2,1)S(1)}, bf16[1024,256]{1,0:T(8,128)(2,1)S(1)}, u32[]{:S(2)}, u32[]{:S(2)}) collective-permute-start(bf16[1024,256]{1,0:T(8,128)(2,1)S(1)} %collective-permute-done.13.refs_1_), channel_id=1, source_target_pairs={{0,1},{1,0},{2,3},{3,2},{4,5},{5,4},{6,7},{7,6},{8,9},{9,8},{10,11... | collective-permute-start | bytes 1572872 | tf_op jit(solution)/shard_map/ppermute | solution.py:111
  176.8 1.9 collective-permute-start.19
  178.8 2.4 %collective-permute-start.20 = (bf16[512,256]{1,0:T(8,128)(2,1)}, bf16[512,256]{1,0:T(8,128)(2,1)}, u32[]{:S(2)}, u32[]{:S(2)}) collective-permute-start(bf16[512,256]{1,0:T(8,128)(2,1)} %collective-permute-done.15.refs_3_), channel_id=1, source_target_pairs={{0,1},{1,0},{2,3},{3,2},{4,5},{5,4},{6,7},{7,6},{8,9},{9,8},{10,11... | collective-permute-start | bytes 786440 | tf_op jit(solution)/shard_map/ppermute | solution.py:111
  181.2 1.9 collective-permute-start.21
  183.2 2.1 constant_dynamic-slice_fusion
  185.3 2.4 %collective-permute-start = (bf16[4,1,256,256]{3,2,1,0:T(8,128)(2,1)}, bf16[4,1,256,256]{3,2,1,0:T(8,128)(2,1)S(1)}, u32[]{:S(2)}, u32[]{:S(2)}) collective-permute-start(bf16[4,1,256,256]{3,2,1,0:T(8,128)(2,1)} %get-tuple-element.22), channel_id=1, source_target_pairs={{0,1},{1,0},{2,3},{3,2},{4,5},{5,4},{6,7},{7,6},{8,9},{9,8},{10,11... | collective-permute-start | bytes 1572872 | tf_op jit(solution)/shard_map/ppermute | solution.py:111
  188.5 5.1 %shard_map.103 = bf16[1024,256]{1,0:T(8,128)(2,1)} custom-call(s32[8]{0:T(128)} %stack.71.sender, bf16[1024,256]{1,0:T(8,128)(2,1)} %shard_map.102.refs_0_, bf16[1024,256]{1,0:T(8,128)(2,1)} %copy-done.10, bf16[1024,256]{1,0:T(8,128)(2,1)} %copy-done.11, bf16[512,256]{1,0:T(8,128)(2,1)} %collective-permute-done.15.refs_3_, ...), custom_call_target="tpu_custom_call" | custom-call | tf_op jit(solution)/shard_map/pallas_call | solution.py:92
  193.6 9.4 %all-to-all-start.3 = ((bf16[32,32,256]{2,1,0:T(8,128)(2,1)}), bf16[32,32,256]{2,1,0:T(8,128)(2,1)}, u32[]{:S(2)}, u32[]{:S(2)}) async-start(bf16[32,32,256]{2,1,0:T(8,128)(2,1)} %bitcast.49), calls=%async_computation.3 | async-start | bytes 1048576 | tf_op jit(solution)/shard_map/all_to_all | solution.py:238
  203.4 2.1 collective-permute-start.1
  205.5 4.7 %collective-permute-start.2 = (bf16[2,256,256]{2,1,0:T(8,128)(2,1)S(1)}, bf16[2,256,256]{2,1,0:T(8,128)(2,1)S(1)}, u32[]{:S(2)}, u32[]{:S(2)}) collective-permute-start(bf16[2,256,256]{2,1,0:T(8,128)(2,1)S(1)} %get-tuple-element.21), channel_id=1, source_target_pairs={{0,4},{1,5},{2,6},{3,7},{4,0},{5,1},{6,2},{7,3},{8,12},{9,13},{10,... | collective-permute-start | bytes 786440 | tf_op jit(solution)/shard_map/ppermute | solution.py:107
  210.3 1.9 collective-permute-start.3
  212.2 1.5 slice_bitcast_fusion
  213.6 1.0 collective-permute-done.1.refs_1_
  214.7 5.0 %collective-permute-done.2.refs_2_ = bf16[2,256,256]{2,1,0:T(8,128)(2,1)S(1)} collective-permute-done((bf16[2,256,256]{2,1,0:T(8,128)(2,1)S(1)}, bf16[2,256,256]{2,1,0:T(8,128)(2,1)S(1)}, u32[]{:S(2)}, u32[]{:S(2)}) %collective-permute-start.2) | collective-permute-done | bytes 262176 | tf_op jit(solution)/shard_map/ppermute | solution.py:107
  219.7 2.5 %collective-permute-done.3.refs_3_ = bf16[2,256,256]{2,1,0:T(8,128)(2,1)S(1)} collective-permute-done((bf16[2,256,256]{2,1,0:T(8,128)(2,1)S(1)}, bf16[2,256,256]{2,1,0:T(8,128)(2,1)S(1)}, u32[]{:S(2)}, u32[]{:S(2)}) %collective-permute-start.3) | collective-permute-done | bytes 262176 | tf_op jit(solution)/shard_map/ppermute | solution.py:107
  222.1 3.3 %place.1 = bf16[256,2048]{1,0:T(8,128)(2,1)} custom-call(s32[8]{0:T(128)S(1)} %stack.62.at, bf16[2,256,256]{2,1,0:T(8,128)(2,1)S(1)} %get-tuple-element.19.refs_0_, bf16[2,256,256]{2,1,0:T(8,128)(2,1)S(1)} %collective-permute-done.1.refs_1_, bf16[2,256,256]{2,1,0:T(8,128)(2,1)S(1)} %collective-permute-done.2.refs_2_, ...), custom_call_target="tpu_custom_call" | custom-call | tf_op jit(solution)/shard_map/place/pallas_call | solution.py:163
  225.4 2.2 convolution_convert_fusion.1
  (66 shorter events, 2.9 us)
Async XLA Ops:
  0.6 1.8 copy-start
  2.5 14.9 %copy-start.12 = (f32[32,32,256]{2,1,0:T(8,128)S(1)}, f32[32,32,256]{2,1,0:T(8,128)}, u32[]{:S(2)}) copy-start(f32[32,32,256]{2,1,0:T(8,128)} %param.9) | copy-start | bytes 3145732
  2.5 14.9 %copy-start.13 = (f32[32,32,256]{2,1,0:T(8,128)S(1)}, f32[32,32,256]{2,1,0:T(8,128)}, u32[]{:S(2)}) copy-start(f32[32,32,256]{2,1,0:T(8,128)} %param.10) | copy-start | bytes 3145732
  2.5 14.9 %copy-start.17 = (f32[32]{0:T(128)S(1)}, f32[32]{0:T(128)}, u32[]{:S(2)}) copy-start(f32[32]{0:T(128)} %param.8) | copy-start | bytes 388
  3.9 28.7 %all-to-all-start = ((bf16[32,32,256]{2,1,0:T(8,128)(2,1)}), bf16[32,32,256]{2,1,0:T(8,128)(2,1)S(1)}, u32[]{:S(2)}, u32[]{:S(2)}) async-start(bf16[32,32,256]{2,1,0:T(8,128)(2,1)} %bitcast.1), calls=%async_computation | async-start | bytes 1048576 | tf_op jit(solution)/shard_map/all_to_all | solution.py:213
  32.6 107.1 %copy-start.1 = (bf16[32,32,256]{2,1,0:T(8,128)(2,1)}, bf16[32,32,256]{2,1,0:T(8,128)(2,1)S(1)}, u32[]{:S(2)}) copy-start(bf16[32,32,256]{2,1,0:T(8,128)(2,1)S(1)} %all-to-all-done) | copy-start | bytes 1572868
  34.3 60.1 %all-to-all-start.1 = ((bf16[64,32,512]{2,1,0:T(8,128)(2,1)}), bf16[64,32,512]{2,1,0:T(8,128)(2,1)S(1)}, u32[]{:S(2)}, u32[]{:S(2)}) async-start(bf16[64,32,512]{2,1,0:T(8,128)(2,1)} %bitcast.47), calls=%async_computation.1 | async-start | bytes 4194304 | tf_op jit(solution)/shard_map/all_to_all | solution.py:226
  94.4 1.7 copy-start.8
  96.1 87.1 %all-to-all-start.2 = ((bf16[64,32,256]{2,1,0:T(8,128)(2,1)}), bf16[64,32,256]{2,1,0:T(8,128)(2,1)}, u32[]{:S(2)}, u32[]{:S(2)}) async-start(bf16[64,32,256]{2,1,0:T(8,128)(2,1)} %bitcast.48), calls=%async_computation.2 | async-start | bytes 2097152 | tf_op jit(solution)/shard_map/all_to_all | solution.py:232
  105.0 13.4 %collective-permute-start.4 = (bf16[1024,256]{1,0:T(8,128)(2,1)S(1)}, bf16[1024,256]{1,0:T(8,128)(2,1)S(1)}, u32[]{:S(2)}, u32[]{:S(2)}) collective-permute-start(bf16[1024,256]{1,0:T(8,128)(2,1)S(1)} %bitcast.40), channel_id=1, source_target_pairs={{0,2},{1,3},{2,4},{3,5},{4,6},{5,7},{6,0},{7,1},{8,10},{9,11},{10,... | collective-permute-start | bytes 1572872 | tf_op jit(solution)/shard_map/ppermute | solution.py:107
  108.2 12.2 %collective-permute-start.5 = (bf16[1024,256]{1,0:T(8,128)(2,1)S(1)}, bf16[1024,256]{1,0:T(8,128)(2,1)S(1)}, u32[]{:S(2)}, u32[]{:S(2)}) collective-permute-start(bf16[1024,256]{1,0:T(8,128)(2,1)S(1)} %bitcast.41), channel_id=1, source_target_pairs={{0,6},{1,7},{2,0},{3,1},{4,2},{5,3},{6,4},{7,5},{8,14},{9,15},{10,... | collective-permute-start | bytes 1572872 | tf_op jit(solution)/shard_map/ppermute | solution.py:107
  111.5 27.0 %collective-permute-start.8 = (bf16[1024,256]{1,0:T(8,128)(2,1)S(1)}, bf16[1024,256]{1,0:T(8,128)(2,1)S(1)}, u32[]{:S(2)}, u32[]{:S(2)}) collective-permute-start(bf16[1024,256]{1,0:T(8,128)(2,1)S(1)} %bitcast.42), channel_id=1, source_target_pairs={{0,1},{1,0},{2,3},{3,2},{4,5},{5,4},{6,7},{7,6},{8,9},{9,8},{10,11... | collective-permute-start | bytes 1572872 | tf_op jit(solution)/shard_map/ppermute | solution.py:111
  118.4 24.1 %copy-start.2 = (bf16[1024,256]{1,0:T(8,128)(2,1)}, bf16[1024,256]{1,0:T(8,128)(2,1)S(1)}, u32[]{:S(2)}) copy-start(bf16[1024,256]{1,0:T(8,128)(2,1)S(1)} %collective-permute-done.4.refs_1_) | copy-start | bytes 1572868
  118.4 15.0 %collective-permute-start.6 = (bf16[512,256]{1,0:T(8,128)(2,1)S(1)}, bf16[512,256]{1,0:T(8,128)(2,1)}, u32[]{:S(2)}, u32[]{:S(2)}) collective-permute-start(bf16[512,256]{1,0:T(8,128)(2,1)S(1)} %slice.44), channel_id=1, source_target_pairs={{0,2},{1,3},{2,4},{3,5},{4,6},{5,7},{6,0},{7,1},{8,10},{9,11},{10,... | collective-permute-start | bytes 786440 | tf_op jit(solution)/shard_map/ppermute | solution.py:107
  120.4 22.2 %copy-start.3 = (bf16[1024,256]{1,0:T(8,128)(2,1)}, bf16[1024,256]{1,0:T(8,128)(2,1)S(1)}, u32[]{:S(2)}) copy-start(bf16[1024,256]{1,0:T(8,128)(2,1)S(1)} %collective-permute-done.5.refs_2_) | copy-start | bytes 1572868
  120.4 15.5 %collective-permute-start.7 = (bf16[512,256]{1,0:T(8,128)(2,1)S(1)}, bf16[512,256]{1,0:T(8,128)(2,1)}, u32[]{:S(2)}, u32[]{:S(2)}) collective-permute-start(bf16[512,256]{1,0:T(8,128)(2,1)S(1)} %slice.45), channel_id=1, source_target_pairs={{0,6},{1,7},{2,0},{3,1},{4,2},{5,3},{6,4},{7,5},{8,14},{9,15},{10,... | collective-permute-start | bytes 786440 | tf_op jit(solution)/shard_map/ppermute | solution.py:107
  125.0 14.7 %collective-permute-start.10 = (bf16[1024,256]{1,0:T(8,128)(2,1)S(1)}, bf16[1024,256]{1,0:T(8,128)(2,1)S(1)}, u32[]{:S(2)}, u32[]{:S(2)}) collective-permute-start(bf16[1024,256]{1,0:T(8,128)(2,1)S(1)} %collective-permute-done.5.refs_2_), channel_id=1, source_target_pairs={{0,1},{1,0},{2,3},{3,2},{4,5},{5,4},{6,7},{7,6},{8,9},{9,8},{10,11... | collective-permute-start | bytes 1572872 | tf_op jit(solution)/shard_map/ppermute | solution.py:111
  131.5 8.1 %collective-permute-start.9 = (bf16[1024,256]{1,0:T(8,128)(2,1)S(1)}, bf16[1024,256]{1,0:T(8,128)(2,1)S(1)}, u32[]{:S(2)}, u32[]{:S(2)}) collective-permute-start(bf16[1024,256]{1,0:T(8,128)(2,1)S(1)} %collective-permute-done.4.refs_1_), channel_id=1, source_target_pairs={{0,1},{1,0},{2,3},{3,2},{4,5},{5,4},{6,7},{7,6},{8,9},{9,8},{10,11... | collective-permute-start | bytes 1572872 | tf_op jit(solution)/shard_map/ppermute | solution.py:111
  133.5 5.1 %collective-permute-start.11 = (bf16[512,256]{1,0:T(8,128)(2,1)}, bf16[512,256]{1,0:T(8,128)(2,1)}, u32[]{:S(2)}, u32[]{:S(2)}) collective-permute-start(bf16[512,256]{1,0:T(8,128)(2,1)} %collective-permute-done.6.refs_3_), channel_id=1, source_target_pairs={{0,1},{1,0},{2,3},{3,2},{4,5},{5,4},{6,7},{7,6},{8,9},{9,8},{10,11... | collective-permute-start | bytes 786440 | tf_op jit(solution)/shard_map/ppermute | solution.py:111
  135.9 3.8 %collective-permute-start.12 = (bf16[512,256]{1,0:T(8,128)(2,1)}, bf16[512,256]{1,0:T(8,128)(2,1)}, u32[]{:S(2)}, u32[]{:S(2)}) collective-permute-start(bf16[512,256]{1,0:T(8,128)(2,1)} %collective-permute-done.7.refs_4_), channel_id=1, source_target_pairs={{0,1},{1,0},{2,3},{3,2},{4,5},{5,4},{6,7},{7,6},{8,9},{9,8},{10,11... | collective-permute-start | bytes 786440 | tf_op jit(solution)/shard_map/ppermute | solution.py:111
  138.6 4.0 %copy-start.4 = (bf16[1024,256]{1,0:T(8,128)(2,1)}, bf16[1024,256]{1,0:T(8,128)(2,1)S(1)}, u32[]{:S(2)}) copy-start(bf16[1024,256]{1,0:T(8,128)(2,1)S(1)} %collective-permute-done.8.refs_5_) | copy-start | bytes 1572868
  139.7 2.9 %copy-start.5 = (bf16[1024,256]{1,0:T(8,128)(2,1)}, bf16[1024,256]{1,0:T(8,128)(2,1)S(1)}, u32[]{:S(2)}) copy-start(bf16[1024,256]{1,0:T(8,128)(2,1)S(1)} %collective-permute-done.10.refs_7_) | copy-start | bytes 1572868
  139.7 2.9 %copy-start.6 = (bf16[1024,256]{1,0:T(8,128)(2,1)}, bf16[1024,256]{1,0:T(8,128)(2,1)S(1)}, u32[]{:S(2)}) copy-start(bf16[1024,256]{1,0:T(8,128)(2,1)S(1)} %collective-permute-done.9.refs_6_) | copy-start | bytes 1572868
  142.6 0.8 copy-start.7
  150.1 16.6 %collective-permute-start.13 = (bf16[1024,256]{1,0:T(8,128)(2,1)}, bf16[1024,256]{1,0:T(8,128)(2,1)S(1)}, u32[]{:S(2)}, u32[]{:S(2)}) collective-permute-start(bf16[1024,256]{1,0:T(8,128)(2,1)} %shard_map.102.refs_0_), channel_id=1, source_target_pairs={{0,2},{1,3},{2,4},{3,5},{4,6},{5,7},{6,0},{7,1},{8,10},{9,11},{10,... | collective-permute-start | bytes 1572872 | tf_op jit(solution)/shard_map/ppermute | solution.py:107
  152.1 16.7 %collective-permute-start.14 = (bf16[1024,256]{1,0:T(8,128)(2,1)}, bf16[1024,256]{1,0:T(8,128)(2,1)S(1)}, u32[]{:S(2)}, u32[]{:S(2)}) collective-permute-start(bf16[1024,256]{1,0:T(8,128)(2,1)} %shard_map.102.refs_0_), channel_id=1, source_target_pairs={{0,6},{1,7},{2,0},{3,1},{4,2},{5,3},{6,4},{7,5},{8,14},{9,15},{10,... | collective-permute-start | bytes 1572872 | tf_op jit(solution)/shard_map/ppermute | solution.py:107
  156.6 28.6 %collective-permute-start.17 = (bf16[1024,256]{1,0:T(8,128)(2,1)}, bf16[1024,256]{1,0:T(8,128)(2,1)S(1)}, u32[]{:S(2)}, u32[]{:S(2)}) collective-permute-start(bf16[1024,256]{1,0:T(8,128)(2,1)} %shard_map.102.refs_0_), channel_id=1, source_target_pairs={{0,1},{1,0},{2,3},{3,2},{4,5},{5,4},{6,7},{7,6},{8,9},{9,8},{10,11... | collective-permute-start | bytes 1572872 | tf_op jit(solution)/shard_map/ppermute | solution.py:111
  166.8 18.4 %copy-start.10 = (bf16[1024,256]{1,0:T(8,128)(2,1)}, bf16[1024,256]{1,0:T(8,128)(2,1)S(1)}, u32[]{:S(2)}) copy-start(bf16[1024,256]{1,0:T(8,128)(2,1)S(1)} %collective-permute-done.13.refs_1_) | copy-start | bytes 1572868
  166.8 12.0 %collective-permute-start.15 = (bf16[512,256]{1,0:T(8,128)(2,1)S(1)}, bf16[512,256]{1,0:T(8,128)(2,1)}, u32[]{:S(2)}, u32[]{:S(2)}) collective-permute-start(bf16[512,256]{1,0:T(8,128)(2,1)S(1)} %slice.46), channel_id=1, source_target_pairs={{0,2},{1,3},{2,4},{3,5},{4,6},{5,7},{6,0},{7,1},{8,10},{9,11},{10,... | collective-permute-start | bytes 786440 | tf_op jit(solution)/shard_map/ppermute | solution.py:107
  168.8 16.5 %copy-start.11 = (bf16[1024,256]{1,0:T(8,128)(2,1)}, bf16[1024,256]{1,0:T(8,128)(2,1)S(1)}, u32[]{:S(2)}) copy-start(bf16[1024,256]{1,0:T(8,128)(2,1)S(1)} %collective-permute-done.14.refs_2_) | copy-start | bytes 1572868
  168.8 12.4 %collective-permute-start.16 = (bf16[512,256]{1,0:T(8,128)(2,1)S(1)}, bf16[512,256]{1,0:T(8,128)(2,1)}, u32[]{:S(2)}, u32[]{:S(2)}) collective-permute-start(bf16[512,256]{1,0:T(8,128)(2,1)S(1)} %slice.47), channel_id=1, source_target_pairs={{0,6},{1,7},{2,0},{3,1},{4,2},{5,3},{6,4},{7,5},{8,14},{9,15},{10,... | collective-permute-start | bytes 786440 | tf_op jit(solution)/shard_map/ppermute | solution.py:107
  173.4 14.3 %collective-permute-start.18 = (bf16[1024,256]{1,0:T(8,128)(2,1)S(1)}, bf16[1024,256]{1,0:T(8,128)(2,1)S(1)}, u32[]{:S(2)}, u32[]{:S(2)}) collective-permute-start(bf16[1024,256]{1,0:T(8,128)(2,1)S(1)} %collective-permute-done.13.refs_1_), channel_id=1, source_target_pairs={{0,1},{1,0},{2,3},{3,2},{4,5},{5,4},{6,7},{7,6},{8,9},{9,8},{10,11... | collective-permute-start | bytes 1572872 | tf_op jit(solution)/shard_map/ppermute | solution.py:111
  176.8 10.8 %collective-permute-start.19 = (bf16[1024,256]{1,0:T(8,128)(2,1)S(1)}, bf16[1024,256]{1,0:T(8,128)(2,1)}, u32[]{:S(2)}, u32[]{:S(2)}) collective-permute-start(bf16[1024,256]{1,0:T(8,128)(2,1)S(1)} %collective-permute-done.14.refs_2_), channel_id=1, source_target_pairs={{0,1},{1,0},{2,3},{3,2},{4,5},{5,4},{6,7},{7,6},{8,9},{9,8},{10,11... | collective-permute-start | bytes 1572872 | tf_op jit(solution)/shard_map/ppermute | solution.py:111
  178.8 8.9 %collective-permute-start.20 = (bf16[512,256]{1,0:T(8,128)(2,1)}, bf16[512,256]{1,0:T(8,128)(2,1)}, u32[]{:S(2)}, u32[]{:S(2)}) collective-permute-start(bf16[512,256]{1,0:T(8,128)(2,1)} %collective-permute-done.15.refs_3_), channel_id=1, source_target_pairs={{0,1},{1,0},{2,3},{3,2},{4,5},{5,4},{6,7},{7,6},{8,9},{9,8},{10,11... | collective-permute-start | bytes 786440 | tf_op jit(solution)/shard_map/ppermute | solution.py:111
  181.2 6.5 %collective-permute-start.21 = (bf16[512,256]{1,0:T(8,128)(2,1)}, bf16[512,256]{1,0:T(8,128)(2,1)}, u32[]{:S(2)}, u32[]{:S(2)}) collective-permute-start(bf16[512,256]{1,0:T(8,128)(2,1)} %collective-permute-done.16.refs_4_), channel_id=1, source_target_pairs={{0,1},{1,0},{2,3},{3,2},{4,5},{5,4},{6,7},{7,6},{8,9},{9,8},{10,11... | collective-permute-start | bytes 786440 | tf_op jit(solution)/shard_map/ppermute | solution.py:111
  185.3 2.5 %copy-start.14 = (bf16[1024,256]{1,0:T(8,128)(2,1)}, bf16[1024,256]{1,0:T(8,128)(2,1)S(1)}, u32[]{:S(2)}) copy-start(bf16[1024,256]{1,0:T(8,128)(2,1)S(1)} %collective-permute-done.17.refs_5_) | copy-start | bytes 1572868
  185.3 18.1 %collective-permute-start = (bf16[4,1,256,256]{3,2,1,0:T(8,128)(2,1)}, bf16[4,1,256,256]{3,2,1,0:T(8,128)(2,1)S(1)}, u32[]{:S(2)}, u32[]{:S(2)}) collective-permute-start(bf16[4,1,256,256]{3,2,1,0:T(8,128)(2,1)} %get-tuple-element.22), channel_id=1, source_target_pairs={{0,1},{1,0},{2,3},{3,2},{4,5},{5,4},{6,7},{7,6},{8,9},{9,8},{10,11... | collective-permute-start | bytes 1572872 | tf_op jit(solution)/shard_map/ppermute | solution.py:111
  187.7 0.8 copy-start.15
  188.5 14.8 %copy-start.16 = (f32[320,2]{0,1:T(2,128)S(1)}, f32[320,2]{0,1:T(2,128)}, u32[]{:S(2)}) copy-start(f32[320,2]{0,1:T(2,128)} %param.13) | copy-start | bytes 7684
  193.6 31.8 %all-to-all-start.3 = ((bf16[32,32,256]{2,1,0:T(8,128)(2,1)}), bf16[32,32,256]{2,1,0:T(8,128)(2,1)}, u32[]{:S(2)}, u32[]{:S(2)}) async-start(bf16[32,32,256]{2,1,0:T(8,128)(2,1)} %bitcast.49), calls=%async_computation.3 | async-start | bytes 1048576 | tf_op jit(solution)/shard_map/all_to_all | solution.py:238
  203.1 9.1 %copy-start.9 = (bf16[64,32,512]{2,1,0:T(8,128)(2,1)S(1)}, bf16[64,32,512]{2,1,0:T(8,128)(2,1)}, u32[]{:S(2)}) copy-start(bf16[64,32,512]{2,1,0:T(8,128)(2,1)} %copy-done.8) | copy-start | bytes 6291460
  203.4 11.2 %collective-permute-start.1 = (bf16[2,256,256]{2,1,0:T(8,128)(2,1)S(1)}, bf16[2,256,256]{2,1,0:T(8,128)(2,1)S(1)}, u32[]{:S(2)}, u32[]{:S(2)}) collective-permute-start(bf16[2,256,256]{2,1,0:T(8,128)(2,1)S(1)} %get-tuple-element.20), channel_id=1, source_target_pairs={{0,2},{1,3},{2,4},{3,5},{4,6},{5,7},{6,0},{7,1},{8,10},{9,11},{10,... | collective-permute-start | bytes 786440 | tf_op jit(solution)/shard_map/ppermute | solution.py:107
  205.5 14.1 %collective-permute-start.2 = (bf16[2,256,256]{2,1,0:T(8,128)(2,1)S(1)}, bf16[2,256,256]{2,1,0:T(8,128)(2,1)S(1)}, u32[]{:S(2)}, u32[]{:S(2)}) collective-permute-start(bf16[2,256,256]{2,1,0:T(8,128)(2,1)S(1)} %get-tuple-element.21), channel_id=1, source_target_pairs={{0,4},{1,5},{2,6},{3,7},{4,0},{5,1},{6,2},{7,3},{8,12},{9,13},{10,... | collective-permute-start | bytes 786440 | tf_op jit(solution)/shard_map/ppermute | solution.py:107
  210.3 11.9 %collective-permute-start.3 = (bf16[2,256,256]{2,1,0:T(8,128)(2,1)S(1)}, bf16[2,256,256]{2,1,0:T(8,128)(2,1)S(1)}, u32[]{:S(2)}, u32[]{:S(2)}) collective-permute-start(bf16[2,256,256]{2,1,0:T(8,128)(2,1)S(1)} %get-tuple-element.18), channel_id=1, source_target_pairs={{0,6},{1,7},{2,0},{3,1},{4,2},{5,3},{6,4},{7,5},{8,14},{9,15},{10,... | collective-permute-start | bytes 786440 | tf_op jit(solution)/shard_map/ppermute | solution.py:107

commit v5 on v2

v5 whole, which is shorter than its diff:
```python
import jax
import jax.numpy as jnp
from jax import lax
from jax.experimental import pallas as pl
from jax.experimental.pallas import tpu as pltpu
from jax.sharding import Mesh
from jax.sharding import PartitionSpec as P


SLOTS = 32
HALF = SLOTS // 2
LANES = 128
BF = jnp.bfloat16
F32 = jnp.float32
ANY = pl.BlockSpec(memory_space=pl.ANY)
WHOLE = pl.BlockSpec(memory_space=pltpu.VMEM)
SCALARS = pl.BlockSpec(memory_space=pltpu.SMEM)


def scale_kernel(*refs):
    pieces, out = refs[:-1], refs[-1]
    squares, total = None, 0
    for piece in pieces:
        for j in range(2):
            values = piece[j].astype(F32)
            total += values.shape[1]
            part = jnp.sum(values * values, axis=-1, keepdims=True)
            squares = part if squares is None else squares + part
    out[...] = jnp.broadcast_to(lax.rsqrt(squares / total + 1e-06), out.shape)


def row_scale(pieces):
    count = pieces[0].shape[1]
    return pl.pallas_call(
        scale_kernel,
        name="row_scale",
        in_specs=[WHOLE] * len(pieces),
        out_specs=WHOLE,
        out_shape=jax.ShapeDtypeStruct((count, LANES), F32),
        compiler_params=pltpu.CompilerParams(vmem_limit_bytes=12 * 1024 * 1024),
    )(*pieces)


def fetch(source, target, sem):
    copy = pltpu.make_async_copy(source, target, sem)
    copy.start()
    return copy


def joined(rows, k):
    return jnp.concatenate([rows[k, 0], rows[k, 1]], axis=1)


def hidden_kernel(chip, *refs):
    pieces, (scale, mine, theirs, out, rows, weights, row_sems, weight_sems) = refs[:-8], refs[-8:]
    chips = len(pieces)
    width = 2 * rows.shape[3]
    row_copies, weight_copies = [], {}
    for j, source in enumerate((mine, theirs)):
        for k in range(chips):
            if j == 0:
                row_copies.append(fetch(pieces[k], rows.at[k], row_sems.at[k]))
            at = pl.multiple_of(chip[k] * width, width)
            weight_copies[j, k] = fetch(
                source.at[pl.ds(at, width)], weights.at[j, k], weight_sems.at[j, k]
            )
    half = out.shape[2]
    for j in range(2):
        acc = None
        for k in range(chips):
            if j == 0:
                row_copies[k].wait()
            weight_copies[j, k].wait()
            part = jnp.dot(joined(rows, k), weights[j, k], preferred_element_type=F32)
            acc = part if acc is None else acc + part
        acc = acc * scale[:, :1]
        gate, up = acc[:, :half], acc[:, half:]
        out[j] = (gate / (1.0 + jnp.exp(-gate)) * up).astype(out.dtype)


def hidden_call(chip, pieces, scale, mine, theirs):
    sides, count, width = pieces[0].shape
    chips = len(pieces)
    return pl.pallas_call(
        hidden_kernel,
        name="hidden",
        in_specs=[SCALARS] + [ANY] * chips + [WHOLE, ANY, ANY],
        out_specs=WHOLE,
        out_shape=jax.ShapeDtypeStruct((2, count, mine.shape[1] // 2), BF),
        scratch_shapes=[
            pltpu.VMEM((chips, sides, count, width), BF),
            pltpu.VMEM((2, chips, sides * width, mine.shape[1]), BF),
            pltpu.SemaphoreType.DMA((chips,)),
            pltpu.SemaphoreType.DMA((2, chips)),
        ],
    )(chip, *pieces, scale, mine, theirs)


def out_kernel(block, leaving, core, *refs):
    chips = leaving.shape[0]
    pieces, mine, theirs, out = refs[:chips], *refs[chips : chips + 3]
    blocks = refs[chips + 3 : 2 * chips + 3]
    rows, weights, row_sems, weight_sems, block_sems = refs[2 * chips + 3 :]
    width = rows.shape[3]
    cols = out.shape[2]
    row_copies, weight_copies = [], {}
    for k in range(chips):
        row_copies.append(fetch(pieces[k], rows.at[k], row_sems.at[k]))
        for side in range(2):
            at = pl.multiple_of(block[2 * k + side] * width, width)
            for j, source in enumerate((mine, theirs)):
                weight_copies[k, side, j] = fetch(
                    source.at[pl.ds(at, width)],
                    weights.at[k, pl.ds(side * width, width), pl.ds(j * cols, cols)],
                    weight_sems.at[k, side, j],
                )
    block_copies = []
    for k in range(chips):
        at = pl.multiple_of(leaving[k] * width, width)
        for j, source in enumerate((mine, theirs)):
            block_copies.append(
                fetch(source.at[pl.ds(at, width)], blocks[k].at[j], block_sems.at[k, j])
            )
    acc = None
    for k in range(chips):
        row_copies[k].wait()
        for side in range(2):
            for j in range(2):
                weight_copies[k, side, j].wait()
        part = jnp.dot(joined(rows, k), weights[k], preferred_element_type=F32)
        acc = part if acc is None else acc + part
    out[core[0]] = acc[:, :cols].astype(out.dtype)
    out[1 - core[0]] = acc[:, cols:].astype(out.dtype)
    for copy in block_copies:
        copy.wait()


def out_call(block, leaving, core, pieces, mine, theirs):
    sides, count, width = pieces[0].shape
    chips, cols = len(pieces), mine.shape[1]
    return pl.pallas_call(
        out_kernel,
        name="expert_out",
        in_specs=[SCALARS] * 3 + [ANY] * (chips + 2),
        out_specs=[WHOLE] + [ANY] * chips,
        out_shape=[jax.ShapeDtypeStruct((2, count, cols), BF)]
        + [jax.ShapeDtypeStruct((2, width, cols), BF)] * chips,
        scratch_shapes=[
            pltpu.VMEM((chips, sides, count, width), BF),
            pltpu.VMEM((chips, sides * width, 2 * cols), BF),
            pltpu.SemaphoreType.DMA((chips,)),
            pltpu.SemaphoreType.DMA((chips, 2, 2)),
            pltpu.SemaphoreType.DMA((chips, 2)),
        ],
    )(block, leaving, core, *pieces, mine, theirs)


def place_kernel(chip, core, *refs):
    pieces, out = refs[:-1], refs[-1]
    for k, piece in enumerate(pieces):

        @pl.when(pl.program_id(0) == k)
        def _(piece=piece):
            out[...] = jnp.concatenate([piece[core[0]], piece[1 - core[0]]], axis=1)


def place_call(chip, core, pieces):
    sides, rows, cols = pieces[0].shape
    chips = len(pieces)
    return pl.pallas_call(
        place_kernel,
        name="place",
        grid_spec=pltpu.PrefetchScalarGridSpec(
            num_scalar_prefetch=2,
            grid=(chips,),
            in_specs=[pl.BlockSpec((sides, rows, cols), lambda k, *_: (0, 0, 0))] * chips,
            out_specs=pl.BlockSpec((rows, sides * cols), lambda k, chip, core: (0, chip[k])),
        ),
        out_shape=jax.ShapeDtypeStruct((rows, chips * sides * cols), BF),
        compiler_params=pltpu.CompilerParams(vmem_limit_bytes=8 * 1024 * 1024),
    )(chip, core, *pieces)


def shift(value, by):
    count = lax.axis_size("x")
    return lax.ppermute(value, "x", [(i, (i + by) % count) for i in range(count)])


def swap(value):
    return lax.ppermute(value, "c", [(0, 1), (1, 0)])


def spread(value, offsets):
    return [shift(value, by) if by else value for by in offsets]


def spread_each(values):
    return [shift(value, by) if by else value for by, value in enumerate(values)]


def exchange(value, axes):
    return lax.all_to_all(value, axes, split_axis=0, concat_axis=0, tiled=True)


def after(value, *others):
    return lax.optimization_barrier((value, *others))[0]


def both_groups(array):
    copies = jnp.broadcast_to(array[None], (lax.axis_size("gr"), *array.shape))
    return copies.reshape(-1, *array.shape[1:])


def body(prompt, norm_gain, gate_weight, up_weight, down_weight, routes, route_weight):
    experts, _, cols = gate_weight.shape
    tok_count, width = prompt.shape
    slots_all = experts * SLOTS
    half_all = slots_all // 2
    chips = lax.axis_size("x")
    chip, core = lax.axis_index("x"), lax.axis_index("c")
    offsets = [0, 1, chips - 1] + list(range(2, chips - 1))
    senders = [(chip - by) % chips for by in offsets]
    sender = jnp.stack(senders).astype(jnp.int32)
    units = jnp.stack([2 * at + side for at in senders for side in (core, 1 - core)])
    units = units.astype(jnp.int32)
    core_id = core.reshape(1).astype(jnp.int32)

    expert_ids = jnp.arange(experts, dtype=jnp.int32)[None, :]
    first = routes[:, 0:1] == expert_ids
    second = routes[:, 1:2] == expert_ids
    named = (first | second).astype(BF)
    order = jnp.arange(tok_count, dtype=jnp.int32)
    before = (order[None, :] < order[:, None]).astype(BF)
    earlier = jnp.dot(before, named, preferred_element_type=F32)
    slot_first = jnp.sum(jnp.where(first, earlier, 0.0), axis=1).astype(jnp.int32)
    slot_second = jnp.sum(jnp.where(second, earlier, 0.0), axis=1).astype(jnp.int32)

    def row_of(expert, slot):
        return slot // HALF * half_all + expert * HALF + slot % HALF

    target_first = row_of(routes[:, 0], slot_first)
    target_second = row_of(routes[:, 1], slot_second)
    slot_ids = jnp.arange(slots_all, dtype=jnp.int32)[None, :]
    is_first = target_first[:, None] == slot_ids
    is_second = target_second[:, None] == slot_ids
    weighted = jnp.where(
        is_first, route_weight[:, 0:1], jnp.where(is_second, route_weight[:, 1:2], 0.0)
    ).astype(BF)
    outbound = jnp.einsum(
        "ts,td->sd", (is_first | is_second).astype(BF), prompt, preferred_element_type=F32
    ).astype(BF)
    moved = exchange(outbound.reshape(2 * experts, HALF, width), ("c", "fs"))
    arrived = spread(moved.reshape(2, half_all, width), offsets)
    scale = row_scale(arrived)

    gain = norm_gain[None, :, None]
    gate_up = jnp.concatenate(
        [(gate_weight * gain).astype(BF), (up_weight * gain).astype(BF)], axis=2
    )
    gate_up = both_groups(gate_up)
    gate_up = after(gate_up, moved)
    gate_up = exchange(gate_up, ("gr", "fs"))
    gate_up = gate_up.reshape(-1, 2 * cols)
    gate_up_other = swap(gate_up)
    gate_new, up_new = gate_up[None, :, :cols], gate_up[None, :, cols:]

    down = both_groups(down_weight.astype(BF))
    down = after(down, gate_up)
    down = exchange(down, ("gr", "fs"))
    down = down.reshape(-1, cols)
    down_other = swap(down)

    hidden = hidden_call(sender, arrived, scale, gate_up, gate_up_other)
    hidden_all = spread(hidden, offsets)
    leaving = jnp.stack([2 * ((chip + by) % chips) + core for by in range(chips)])
    summed, *blocks = out_call(
        units, leaving.astype(jnp.int32), core_id, hidden_all, down, down_other
    )

    returned = exchange(summed.reshape(2 * experts, HALF, width), ("c", "fs"))
    returned = returned.reshape(slots_all, width)
    pieces = spread_each(blocks)
    places = jnp.stack([(chip - by) % chips for by in range(chips)]).astype(jnp.int32)
    down_new = place_call(places, core_id, pieces)

    mixed = jnp.dot(weighted, returned, preferred_element_type=F32)
    return (gate_new, up_new, down_new[None], mixed.astype(BF))


def solution(mesh):
    groups, servers, shards = mesh.devices.shape
    devices = mesh.devices.reshape(groups, servers, shards // 2, 2)
    tp = ("x", "c")
    return jax.shard_map(
        body,
        mesh=Mesh(devices, ("gr", "fs", "x", "c")),
        in_specs=(
            P(("gr", "fs"), tp),
            P(("gr", "fs")),
            P(None, ("gr", "fs"), tp),
            P(None, ("gr", "fs"), tp),
            P(None, ("gr", "fs"), tp),
            P(("gr", "fs"), None),
            P(("gr", "fs"), None),
        ),
        out_specs=(
            P("fs", None, tp),
            P("fs", None, tp),
            P("fs", tp, None),
            P(("gr", "fs"), tp),
        ),
        check_vma=False,
    )
```

time: 197 us -> 254 us (1.29)
  the two profiles are of different devices: /device:TPU:1 before, /device:TPU:8 now
where the time goes in v5:
time: 254 us; the launch traced here: 253 us
  waiting for transfers between devices  113 us (44%)
  starting transfers between devices  81 us (32%)
  Pallas kernels  44.3 us (17%)
  local copies, waits for them, and re-layouts  8.66 us (3%)
  matrix products  2.91 us (1%)
  other arithmetic  2.59 us (1%)
    all_to_all x4, waiting for transfers between devices, exchange(): return lax.all_to_all(value, axes, split_axis=0, concat_axis=0, tiled=True)  86.1 us
    all_to_all x4, starting transfers between devices, exchange(): return lax.all_to_all(value, axes, split_axis=0, concat_axis=0, tiled=True)  43.9 us
    pallas_call x1, Pallas kernels, out_call(): pl.pallas_call(out_kernel, name='expert_out', in_specs=[SCALARS] * 3 + [A...  34.8 us
    ppermute x9, starting transfers between devices, shift(): lax.ppermute(value, 'x', [(i, (i + by) % count) for i in range(count)])  33.3 us
    ppermute x9, waiting for transfers between devices, shift(): lax.ppermute(value, 'x', [(i, (i + by) % count) for i in range(count)])  26.9 us
    pallas_call x1, Pallas kernels, hidden_call(): pl.pallas_call(hidden_kernel, name='hidden', in_specs=[SCALARS] + [ANY] *...  6.77 us
  transfers between devices with their start and end apart: 15, of which 8 were waited for; matrix products, arithmetic and copies ran while one was open for 2% of the time, Pallas kernels for 4%

profile of v5, /device:TPU:8, one launch (start us, length us, event | category | flops | bytes accessed | tf_op | source)
XLA Modules:
  0.0 253.5 jit_solution(16160434385695910503)
XLA Ops:
  0.6 0.0 copy-start
  0.6 0.8 slice_reduce_fusion.3
  1.4 0.2 select_reduce_fusion.1
  1.7 0.8 fusion.21
  2.5 0.0 copy-start.9
  2.5 0.0 copy-start.10
  2.5 0.0 copy-start.15
  2.5 1.5 fusion.3
  4.0 13.5 %all-to-all-start = ((bf16[64,16,256]{2,1,0:T(8,128)(2,1)}), bf16[64,16,256]{2,1,0:T(8,128)(2,1)S(1)}, u32[]{:S(2)}, u32[]{:S(2)}) async-start(bf16[64,16,256]{2,1,0:T(8,128)(2,1)} %bitcast.1), calls=%async_computation | async-start | bytes 1048576 | tf_op jit(solution)/shard_map/all_to_all | solution.py:202
  17.6 0.3 multiply_convert_fusion.1
  17.9 0.1 pad_maximum_fusion
  18.0 18.1 %all-to-all-done = bf16[64,16,256]{2,1,0:T(8,128)(2,1)S(1)} async-done(((bf16[64,16,256]{2,1,0:T(8,128)(2,1)}), bf16[64,16,256]{2,1,0:T(8,128)(2,1)S(1)}, u32[]{:S(2)}, u32[]{:S(2)}) %all-to-all-start) | async-done | bytes 524320 | tf_op jit(solution)/shard_map/all_to_all | solution.py:202
  36.2 1.6 broadcast_in_dim.57
  37.7 10.9 %all-to-all-start.1 = ((bf16[64,32,512]{2,1,0:T(8,128)(2,1)}), bf16[64,32,512]{2,1,0:T(8,128)(2,1)}, u32[]{:S(2)}, u32[]{:S(2)}) async-start(bf16[64,32,512]{2,1,0:T(8,128)(2,1)} %bitcast), calls=%async_computation.1 | async-start | bytes 4194304 | tf_op jit(solution)/shard_map/all_to_all | solution.py:202
  48.6 0.1 convert_element_type.60
  48.7 52.5 %all-to-all-done.1 = bf16[64,32,512]{2,1,0:T(8,128)(2,1)} async-done(((bf16[64,32,512]{2,1,0:T(8,128)(2,1)}), bf16[64,32,512]{2,1,0:T(8,128)(2,1)}, u32[]{:S(2)}, u32[]{:S(2)}) %all-to-all-start.1) | async-done | bytes 2097184 | tf_op jit(solution)/shard_map/all_to_all | solution.py:202
  101.2 1.1 broadcast_in_dim.61
  102.3 9.0 %all-to-all-start.2 = ((bf16[64,32,256]{2,1,0:T(8,128)(2,1)}), bf16[64,32,256]{2,1,0:T(8,128)(2,1)S(1)}, u32[]{:S(2)}, u32[]{:S(2)}) async-start(bf16[64,32,256]{2,1,0:T(8,128)(2,1)} %bitcast.22), calls=%async_computation.2 | async-start | bytes 2097152 | tf_op jit(solution)/shard_map/all_to_all | solution.py:202
  111.3 1.9 collective-permute-start.3
  113.2 3.4 %collective-permute-start = (bf16[2,512,256]{2,1,0:T(8,128)(2,1)S(1)}, bf16[2,512,256]{2,1,0:T(8,128)(2,1)S(1)}, u32[]{:S(2)}, u32[]{:S(2)}) collective-permute-start(bf16[2,512,256]{2,1,0:T(8,128)(2,1)S(1)} %bitcast.31), channel_id=1, source_target_pairs={{0,2},{2,4},{4,6},{6,0},{1,3},{3,5},{5,7},{7,1},{8,10},{10,12},{12... | collective-permute-start | bytes 1572872 | tf_op jit(solution)/shard_map/ppermute | solution.py:186
  116.6 3.7 %collective-permute-start.1 = (bf16[2,512,256]{2,1,0:T(8,128)(2,1)S(1)}, bf16[2,512,256]{2,1,0:T(8,128)(2,1)S(1)}, u32[]{:S(2)}, u32[]{:S(2)}) collective-permute-start(bf16[2,512,256]{2,1,0:T(8,128)(2,1)S(1)} %bitcast.32), channel_id=1, source_target_pairs={{0,6},{2,0},{4,2},{6,4},{1,7},{3,1},{5,3},{7,5},{8,14},{10,8},{12,... | collective-permute-start | bytes 1572872 | tf_op jit(solution)/shard_map/ppermute | solution.py:186
  120.3 3.7 %collective-permute-start.2 = (bf16[2,512,256]{2,1,0:T(8,128)(2,1)S(1)}, bf16[2,512,256]{2,1,0:T(8,128)(2,1)S(1)}, u32[]{:S(2)}, u32[]{:S(2)}) collective-permute-start(bf16[2,512,256]{2,1,0:T(8,128)(2,1)S(1)} %bitcast.33), channel_id=1, source_target_pairs={{0,4},{2,6},{4,0},{6,2},{1,5},{3,7},{5,1},{7,3},{8,12},{10,14},{12... | collective-permute-start | bytes 1572872 | tf_op jit(solution)/shard_map/ppermute | solution.py:186
  124.0 15.4 %all-to-all-done.2 = bf16[64,32,256]{2,1,0:T(8,128)(2,1)S(1)} async-done(((bf16[64,32,256]{2,1,0:T(8,128)(2,1)}), bf16[64,32,256]{2,1,0:T(8,128)(2,1)S(1)}, u32[]{:S(2)}, u32[]{:S(2)}) %all-to-all-start.2) | async-done | bytes 1048608 | tf_op jit(solution)/shard_map/all_to_all | solution.py:202
  139.5 1.9 collective-permute-start.7
  141.4 0.6 pad_add_fusion.3.chip
  142.0 1.1 collective-permute-done.1.refs_2_
  143.1 0.6 row_scale.1.refs_4_
  143.8 0.7 copy-done.5
  144.5 6.8 %hidden.1.refs_0_ = bf16[2,512,256]{2,1,0:T(8,128)(2,1)} custom-call(s32[4]{0:T(128)} %pad_add_fusion.3.chip, bf16[2,512,256]{2,1,0:T(8,128)(2,1)} %bitcast.35, bf16[2,512,256]{2,1,0:T(8,128)(2,1)} %copy-done.2, bf16[2,512,256]{2,1,0:T(8,128)(2,1)} %copy-done.3, bf16[2,512,256]{2,1,0:T(8,128)(2,1)} %copy-done.4, f32[512,128]{1,0:T(8,128)} %copy-done.5, ...), custom_call_target="tpu_custom_call" | custom-call | tf_op jit(solution)/shard_map/hidden/pallas_call | solution.py:84
  151.3 4.7 %collective-permute-start.4 = (bf16[2,512,256]{2,1,0:T(8,128)(2,1)}, bf16[2,512,256]{2,1,0:T(8,128)(2,1)S(1)}, u32[]{:S(2)}, u32[]{:S(2)}) collective-permute-start(bf16[2,512,256]{2,1,0:T(8,128)(2,1)} %hidden.1.refs_0_), channel_id=1, source_target_pairs={{0,2},{2,4},{4,6},{6,0},{1,3},{3,5},{5,7},{7,1},{8,10},{10,12},{12... | collective-permute-start | bytes 1572872 | tf_op jit(solution)/shard_map/ppermute | solution.py:186
  156.0 2.8 %collective-permute-start.5 = (bf16[2,512,256]{2,1,0:T(8,128)(2,1)}, bf16[2,512,256]{2,1,0:T(8,128)(2,1)S(1)}, u32[]{:S(2)}, u32[]{:S(2)}) collective-permute-start(bf16[2,512,256]{2,1,0:T(8,128)(2,1)} %hidden.1.refs_0_), channel_id=1, source_target_pairs={{0,6},{2,0},{4,2},{6,4},{1,7},{3,1},{5,3},{7,5},{8,14},{10,8},{12,... | collective-permute-start | bytes 1572872 | tf_op jit(solution)/shard_map/ppermute | solution.py:186
  158.8 3.4 %collective-permute-start.6 = (bf16[2,512,256]{2,1,0:T(8,128)(2,1)}, bf16[2,512,256]{2,1,0:T(8,128)(2,1)S(1)}, u32[]{:S(2)}, u32[]{:S(2)}) collective-permute-start(bf16[2,512,256]{2,1,0:T(8,128)(2,1)} %hidden.1.refs_0_), channel_id=1, source_target_pairs={{0,4},{2,6},{4,0},{6,2},{1,5},{3,7},{5,1},{7,3},{8,12},{10,14},{12... | collective-permute-start | bytes 1572872 | tf_op jit(solution)/shard_map/ppermute | solution.py:186
  162.2 0.6 stack.75.block
  162.8 0.6 pad_add_fusion.2.leaving
  163.5 5.5 %collective-permute-done.4.refs_1_ = bf16[2,512,256]{2,1,0:T(8,128)(2,1)S(1)} collective-permute-done((bf16[2,512,256]{2,1,0:T(8,128)(2,1)}, bf16[2,512,256]{2,1,0:T(8,128)(2,1)S(1)}, u32[]{:S(2)}, u32[]{:S(2)}) %collective-permute-start.4) | collective-permute-done | bytes 524320 | tf_op jit(solution)/shard_map/ppermute | solution.py:186
  168.9 4.0 %collective-permute-done.5.refs_2_ = bf16[2,512,256]{2,1,0:T(8,128)(2,1)S(1)} collective-permute-done((bf16[2,512,256]{2,1,0:T(8,128)(2,1)}, bf16[2,512,256]{2,1,0:T(8,128)(2,1)S(1)}, u32[]{:S(2)}, u32[]{:S(2)}) %collective-permute-start.5) | collective-permute-done | bytes 524320 | tf_op jit(solution)/shard_map/ppermute | solution.py:186
  172.9 7.7 %collective-permute-done.6.refs_3_ = bf16[2,512,256]{2,1,0:T(8,128)(2,1)S(1)} collective-permute-done((bf16[2,512,256]{2,1,0:T(8,128)(2,1)}, bf16[2,512,256]{2,1,0:T(8,128)(2,1)S(1)}, u32[]{:S(2)}, u32[]{:S(2)}) %collective-permute-start.6) | collective-permute-done | bytes 524320 | tf_op jit(solution)/shard_map/ppermute | solution.py:186
  180.7 0.8 copy-done.13
  181.4 34.8 %expert_out.1 = (bf16[2,512,256]{2,1,0:T(8,128)(2,1)}, bf16[2,256,256]{2,1,0:T(8,128)(2,1)}, bf16[2,256,256]{2,1,0:T(8,128)(2,1)}, bf16[2,256,256]{2,1,0:T(8,128)(2,1)}, bf16[2,256,256]{2,1,0:T(8,128)(2,1)}) custom-call(s32[8]{0:T(128)} %stack.75.block, s32[4]{0:T(128)} %pad_add_fusion.2.leaving, s32[1]{0:T(128)} %bitcast.9.core, ...), custom_call_target="tpu_custom_call" | custom-call | tf_op jit(solution)/shard_map/expert_out/pallas_call | solution.py:141
  216.2 10.5 %all-to-all-start.3 = ((bf16[64,16,256]{2,1,0:T(8,128)(2,1)}), bf16[64,16,256]{2,1,0:T(8,128)(2,1)S(1)}, u32[]{:S(2)}, u32[]{:S(2)}) async-start(bf16[64,16,256]{2,1,0:T(8,128)(2,1)} %bitcast.39), calls=%async_computation.3 | async-start | bytes 1048576 | tf_op jit(solution)/shard_map/all_to_all | solution.py:202
  226.8 0.1 pad_add_fusion.chip
  226.9 6.2 %collective-permute-start.10 = (bf16[2,256,256]{2,1,0:T(8,128)(2,1)}, bf16[2,256,256]{2,1,0:T(8,128)(2,1)S(1)}, u32[]{:S(2)}, u32[]{:S(2)}) collective-permute-start(bf16[2,256,256]{2,1,0:T(8,128)(2,1)} %get-tuple-element.16), channel_id=1, source_target_pairs={{0,6},{2,0},{4,2},{6,4},{1,7},{3,1},{5,3},{7,5},{8,14},{10,8},{12,... | collective-permute-start | bytes 786440 | tf_op jit(solution)/shard_map/ppermute | solution.py:186
  233.1 1.9 collective-permute-start.8
  235.0 3.5 %collective-permute-start.9 = (bf16[2,256,256]{2,1,0:T(8,128)(2,1)}, bf16[2,256,256]{2,1,0:T(8,128)(2,1)S(1)}, u32[]{:S(2)}, u32[]{:S(2)}) collective-permute-start(bf16[2,256,256]{2,1,0:T(8,128)(2,1)} %get-tuple-element.15), channel_id=1, source_target_pairs={{0,4},{2,6},{4,0},{6,2},{1,5},{3,7},{5,1},{7,3},{8,12},{10,14},{12... | collective-permute-start | bytes 786440 | tf_op jit(solution)/shard_map/ppermute | solution.py:186
  238.5 3.0 %slice_bitcast_fusion = (bf16[1,2048,256]{2,1,0:T(8,128)(2,1)}, bf16[1,2048,256]{2,1,0:T(8,128)(2,1)}) fusion(bf16[2048,512]{1,0:T(8,128)(2,1)} %bitcast.2.refs_5_), kind=kLoop, calls=%fused_computation.7 | loop fusion | bytes 4194304 | tf_op jit(solution)/shard_map/broadcast_in_dim | solution.py:265
  241.5 8.6 %collective-permute-done.8.refs_1_ = bf16[2,256,256]{2,1,0:T(8,128)(2,1)S(1)} collective-permute-done((bf16[2,256,256]{2,1,0:T(8,128)(2,1)}, bf16[2,256,256]{2,1,0:T(8,128)(2,1)S(1)}, u32[]{:S(2)}, u32[]{:S(2)}) %collective-permute-start.8) | collective-permute-done | bytes 262176 | tf_op jit(solution)/shard_map/ppermute | solution.py:186
  250.2 2.1 place.1
  252.3 1.2 convolution_convert_fusion
  (36 shorter events, 0.1 us)
Async XLA Ops:
  0.6 1.8 copy-start
  2.5 15.1 %copy-start.9 = (f32[32,32,256]{2,1,0:T(8,128)S(1)}, f32[32,32,256]{2,1,0:T(8,128)}, u32[]{:S(2)}) copy-start(f32[32,32,256]{2,1,0:T(8,128)} %param.9) | copy-start | bytes 3145732
  2.5 15.1 %copy-start.10 = (f32[32,32,256]{2,1,0:T(8,128)S(1)}, f32[32,32,256]{2,1,0:T(8,128)}, u32[]{:S(2)}) copy-start(f32[32,32,256]{2,1,0:T(8,128)} %param.10) | copy-start | bytes 3145732
  2.5 15.1 %copy-start.15 = (f32[32]{0:T(128)S(1)}, f32[32]{0:T(128)}, u32[]{:S(2)}) copy-start(f32[32]{0:T(128)} %param.8) | copy-start | bytes 388
  4.0 32.1 %all-to-all-start = ((bf16[64,16,256]{2,1,0:T(8,128)(2,1)}), bf16[64,16,256]{2,1,0:T(8,128)(2,1)S(1)}, u32[]{:S(2)}, u32[]{:S(2)}) async-start(bf16[64,16,256]{2,1,0:T(8,128)(2,1)} %bitcast.1), calls=%async_computation | async-start | bytes 1048576 | tf_op jit(solution)/shard_map/all_to_all | solution.py:202
  36.2 107.0 %copy-start.1 = (bf16[64,16,256]{2,1,0:T(8,128)(2,1)}, bf16[64,16,256]{2,1,0:T(8,128)(2,1)S(1)}, u32[]{:S(2)}) copy-start(bf16[64,16,256]{2,1,0:T(8,128)(2,1)S(1)} %all-to-all-done) | copy-start | bytes 1572868
  37.7 10.9 %copy-start.8 = (f32[32,32,256]{2,1,0:T(8,128)S(1)}, f32[32,32,256]{2,1,0:T(8,128)}, u32[]{:S(2)}) copy-start(f32[32,32,256]{2,1,0:T(8,128)} %param.11) | copy-start | bytes 3145732
  37.7 63.5 %all-to-all-start.1 = ((bf16[64,32,512]{2,1,0:T(8,128)(2,1)}), bf16[64,32,512]{2,1,0:T(8,128)(2,1)}, u32[]{:S(2)}, u32[]{:S(2)}) async-start(bf16[64,32,512]{2,1,0:T(8,128)(2,1)} %bitcast), calls=%async_computation.1 | async-start | bytes 4194304 | tf_op jit(solution)/shard_map/all_to_all | solution.py:202
  102.3 37.1 %all-to-all-start.2 = ((bf16[64,32,256]{2,1,0:T(8,128)(2,1)}), bf16[64,32,256]{2,1,0:T(8,128)(2,1)S(1)}, u32[]{:S(2)}, u32[]{:S(2)}) async-start(bf16[64,32,256]{2,1,0:T(8,128)(2,1)} %bitcast.22), calls=%async_computation.2 | async-start | bytes 2097152 | tf_op jit(solution)/shard_map/all_to_all | solution.py:202
  111.3 33.2 %collective-permute-start.3 = (bf16[2048,512]{1,0:T(8,128)(2,1)}, bf16[2048,512]{1,0:T(8,128)(2,1)}, u32[]{:S(2)}, u32[]{:S(2)}) collective-permute-start(bf16[2048,512]{1,0:T(8,128)(2,1)} %bitcast.2.refs_5_), channel_id=1, source_target_pairs={{0,1},{1,0},{2,3},{3,2},{4,5},{5,4},{6,7},{7,6},{8,9},{9,8},{10,11... | collective-permute-start | bytes 6291464 | tf_op jit(solution)/shard_map/ppermute | solution.py:190
  113.2 28.8 %collective-permute-start = (bf16[2,512,256]{2,1,0:T(8,128)(2,1)S(1)}, bf16[2,512,256]{2,1,0:T(8,128)(2,1)S(1)}, u32[]{:S(2)}, u32[]{:S(2)}) collective-permute-start(bf16[2,512,256]{2,1,0:T(8,128)(2,1)S(1)} %bitcast.31), channel_id=1, source_target_pairs={{0,2},{2,4},{4,6},{6,0},{1,3},{3,5},{5,7},{7,1},{8,10},{10,12},{12... | collective-permute-start | bytes 1572872 | tf_op jit(solution)/shard_map/ppermute | solution.py:186
  116.6 26.5 %collective-permute-start.1 = (bf16[2,512,256]{2,1,0:T(8,128)(2,1)S(1)}, bf16[2,512,256]{2,1,0:T(8,128)(2,1)S(1)}, u32[]{:S(2)}, u32[]{:S(2)}) collective-permute-start(bf16[2,512,256]{2,1,0:T(8,128)(2,1)S(1)} %bitcast.32), channel_id=1, source_target_pairs={{0,6},{2,0},{4,2},{6,4},{1,7},{3,1},{5,3},{7,5},{8,14},{10,8},{12,... | collective-permute-start | bytes 1572872 | tf_op jit(solution)/shard_map/ppermute | solution.py:186
  120.3 22.8 %collective-permute-start.2 = (bf16[2,512,256]{2,1,0:T(8,128)(2,1)S(1)}, bf16[2,512,256]{2,1,0:T(8,128)(2,1)S(1)}, u32[]{:S(2)}, u32[]{:S(2)}) collective-permute-start(bf16[2,512,256]{2,1,0:T(8,128)(2,1)S(1)} %bitcast.33), channel_id=1, source_target_pairs={{0,4},{2,6},{4,0},{6,2},{1,5},{3,7},{5,1},{7,3},{8,12},{10,14},{12... | collective-permute-start | bytes 1572872 | tf_op jit(solution)/shard_map/ppermute | solution.py:186
  139.5 11.8 %copy-start.7 = (bf16[64,32,256]{2,1,0:T(8,128)(2,1)}, bf16[64,32,256]{2,1,0:T(8,128)(2,1)S(1)}, u32[]{:S(2)}) copy-start(bf16[64,32,256]{2,1,0:T(8,128)(2,1)S(1)} %all-to-all-done.2) | copy-start | bytes 3145732
  139.5 41.2 %collective-permute-start.7 = (bf16[2048,256]{1,0:T(8,128)(2,1)S(1)}, bf16[2048,256]{1,0:T(8,128)(2,1)}, u32[]{:S(2)}, u32[]{:S(2)}) collective-permute-start(bf16[2048,256]{1,0:T(8,128)(2,1)S(1)} %bitcast.36), channel_id=1, source_target_pairs={{0,1},{1,0},{2,3},{3,2},{4,5},{5,4},{6,7},{7,6},{8,9},{9,8},{10,11... | collective-permute-start | bytes 3145736 | tf_op jit(solution)/shard_map/ppermute | solution.py:190
  142.0 2.4 copy-start.2
  143.1 1.4 copy-start.3
  143.1 1.4 copy-start.4
  143.7 0.7 copy-start.5
  151.3 17.7 %collective-permute-start.4 = (bf16[2,512,256]{2,1,0:T(8,128)(2,1)}, bf16[2,512,256]{2,1,0:T(8,128)(2,1)S(1)}, u32[]{:S(2)}, u32[]{:S(2)}) collective-permute-start(bf16[2,512,256]{2,1,0:T(8,128)(2,1)} %hidden.1.refs_0_), channel_id=1, source_target_pairs={{0,2},{2,4},{4,6},{6,0},{1,3},{3,5},{5,7},{7,1},{8,10},{10,12},{12... | collective-permute-start | bytes 1572872 | tf_op jit(solution)/shard_map/ppermute | solution.py:186
  156.0 16.9 %collective-permute-start.5 = (bf16[2,512,256]{2,1,0:T(8,128)(2,1)}, bf16[2,512,256]{2,1,0:T(8,128)(2,1)S(1)}, u32[]{:S(2)}, u32[]{:S(2)}) collective-permute-start(bf16[2,512,256]{2,1,0:T(8,128)(2,1)} %hidden.1.refs_0_), channel_id=1, source_target_pairs={{0,6},{2,0},{4,2},{6,4},{1,7},{3,1},{5,3},{7,5},{8,14},{10,8},{12,... | collective-permute-start | bytes 1572872 | tf_op jit(solution)/shard_map/ppermute | solution.py:186
  158.8 21.9 %collective-permute-start.6 = (bf16[2,512,256]{2,1,0:T(8,128)(2,1)}, bf16[2,512,256]{2,1,0:T(8,128)(2,1)S(1)}, u32[]{:S(2)}, u32[]{:S(2)}) collective-permute-start(bf16[2,512,256]{2,1,0:T(8,128)(2,1)} %hidden.1.refs_0_), channel_id=1, source_target_pairs={{0,4},{2,6},{4,0},{6,2},{1,5},{3,7},{5,1},{7,3},{8,12},{10,14},{12... | collective-permute-start | bytes 1572872 | tf_op jit(solution)/shard_map/ppermute | solution.py:186
  168.9 11.7 %copy-start.11 = (bf16[2,512,256]{2,1,0:T(8,128)(2,1)}, bf16[2,512,256]{2,1,0:T(8,128)(2,1)S(1)}, u32[]{:S(2)}) copy-start(bf16[2,512,256]{2,1,0:T(8,128)(2,1)S(1)} %collective-permute-done.4.refs_1_) | copy-start | bytes 1572868
  172.9 7.8 %copy-start.12 = (bf16[2,512,256]{2,1,0:T(8,128)(2,1)}, bf16[2,512,256]{2,1,0:T(8,128)(2,1)S(1)}, u32[]{:S(2)}) copy-start(bf16[2,512,256]{2,1,0:T(8,128)(2,1)S(1)} %collective-permute-done.5.refs_2_) | copy-start | bytes 1572868
  180.6 0.8 copy-start.13
  181.4 45.4 %copy-start.14 = (f32[320,2]{0,1:T(2,128)S(1)}, f32[320,2]{0,1:T(2,128)}, u32[]{:S(2)}) copy-start(f32[320,2]{0,1:T(2,128)} %param.13) | copy-start | bytes 7684
  216.2 36.1 %all-to-all-start.3 = ((bf16[64,16,256]{2,1,0:T(8,128)(2,1)}), bf16[64,16,256]{2,1,0:T(8,128)(2,1)S(1)}, u32[]{:S(2)}, u32[]{:S(2)}) async-start(bf16[64,16,256]{2,1,0:T(8,128)(2,1)} %bitcast.39), calls=%async_computation.3 | async-start | bytes 1048576 | tf_op jit(solution)/shard_map/all_to_all | solution.py:202
  226.9 14.6 %collective-permute-start.10 = (bf16[2,256,256]{2,1,0:T(8,128)(2,1)}, bf16[2,256,256]{2,1,0:T(8,128)(2,1)S(1)}, u32[]{:S(2)}, u32[]{:S(2)}) collective-permute-start(bf16[2,256,256]{2,1,0:T(8,128)(2,1)} %get-tuple-element.16), channel_id=1, source_target_pairs={{0,6},{2,0},{4,2},{6,4},{1,7},{3,1},{5,3},{7,5},{8,14},{10,8},{12,... | collective-permute-start | bytes 786440 | tf_op jit(solution)/shard_map/ppermute | solution.py:186
  233.1 17.1 %collective-permute-start.8 = (bf16[2,256,256]{2,1,0:T(8,128)(2,1)}, bf16[2,256,256]{2,1,0:T(8,128)(2,1)S(1)}, u32[]{:S(2)}, u32[]{:S(2)}) collective-permute-start(bf16[2,256,256]{2,1,0:T(8,128)(2,1)} %get-tuple-element.14), channel_id=1, source_target_pairs={{0,2},{2,4},{4,6},{6,0},{1,3},{3,5},{5,7},{7,1},{8,10},{10,12},{12... | collective-permute-start | bytes 786440 | tf_op jit(solution)/shard_map/ppermute | solution.py:186
  235.0 15.2 %copy-start.6 = (bf16[2,256,256]{2,1,0:T(8,128)(2,1)S(1)}, bf16[2,256,256]{2,1,0:T(8,128)(2,1)}, u32[]{:S(2)}) copy-start(bf16[2,256,256]{2,1,0:T(8,128)(2,1)} %get-tuple-element.13.refs_0_) | copy-start | bytes 786436
  235.0 15.2 %collective-permute-start.9 = (bf16[2,256,256]{2,1,0:T(8,128)(2,1)}, bf16[2,256,256]{2,1,0:T(8,128)(2,1)S(1)}, u32[]{:S(2)}, u32[]{:S(2)}) collective-permute-start(bf16[2,256,256]{2,1,0:T(8,128)(2,1)} %get-tuple-element.15), channel_id=1, source_target_pairs={{0,4},{2,6},{4,0},{6,2},{1,5},{3,7},{5,1},{7,3},{8,12},{10,14},{12... | collective-permute-start | bytes 786440 | tf_op jit(solution)/shard_map/ppermute | solution.py:186

commit v6 on v5

--- a/solution.py
+++ b/solution.py
@@ -51,26 +51,30 @@
     return jnp.concatenate([rows[k, 0], rows[k, 1]], axis=1)
 
 
-def hidden_kernel(chip, *refs):
+def hidden_kernel(block, *refs):
     pieces, (scale, mine, theirs, out, rows, weights, row_sems, weight_sems) = refs[:-8], refs[-8:]
     chips = len(pieces)
-    width = 2 * rows.shape[3]
+    width = rows.shape[3]
     row_copies, weight_copies = [], {}
     for j, source in enumerate((mine, theirs)):
         for k in range(chips):
             if j == 0:
                 row_copies.append(fetch(pieces[k], rows.at[k], row_sems.at[k]))
-            at = pl.multiple_of(chip[k] * width, width)
-            weight_copies[j, k] = fetch(
-                source.at[pl.ds(at, width)], weights.at[j, k], weight_sems.at[j, k]
-            )
+            for side in range(2):
+                at = pl.multiple_of(block[2 * k + side] * width, width)
+                weight_copies[j, k, side] = fetch(
+                    source.at[pl.ds(at, width)],
+                    weights.at[j, k, pl.ds(side * width, width)],
+                    weight_sems.at[j, k, side],
+                )
     half = out.shape[2]
     for j in range(2):
         acc = None
         for k in range(chips):
             if j == 0:
                 row_copies[k].wait()
-            weight_copies[j, k].wait()
+            for side in range(2):
+                weight_copies[j, k, side].wait()
             part = jnp.dot(joined(rows, k), weights[j, k], preferred_element_type=F32)
             acc = part if acc is None else acc + part
         acc = acc * scale[:, :1]
@@ -78,7 +82,7 @@
         out[j] = (gate / (1.0 + jnp.exp(-gate)) * up).astype(out.dtype)
 
 
-def hidden_call(chip, pieces, scale, mine, theirs):
+def hidden_call(block, pieces, scale, mine, theirs):
     sides, count, width = pieces[0].shape
     chips = len(pieces)
     return pl.pallas_call(
@@ -91,16 +95,14 @@
             pltpu.VMEM((chips, sides, count, width), BF),
             pltpu.VMEM((2, chips, sides * width, mine.shape[1]), BF),
             pltpu.SemaphoreType.DMA((chips,)),
-            pltpu.SemaphoreType.DMA((2, chips)),
+            pltpu.SemaphoreType.DMA((2, chips, 2)),
         ],
-    )(chip, *pieces, scale, mine, theirs)
-
-
-def out_kernel(block, leaving, core, *refs):
-    chips = leaving.shape[0]
-    pieces, mine, theirs, out = refs[:chips], *refs[chips : chips + 3]
-    blocks = refs[chips + 3 : 2 * chips + 3]
-    rows, weights, row_sems, weight_sems, block_sems = refs[2 * chips + 3 :]
+    )(block, *pieces, scale, mine, theirs)
+
+
+def out_kernel(block, core, *refs):
+    pieces, (mine, theirs, out, rows, weights, row_sems, weight_sems) = refs[:-7], refs[-7:]
+    chips = len(pieces)
     width = rows.shape[3]
     cols = out.shape[2]
     row_copies, weight_copies = [], {}
@@ -114,13 +116,6 @@
                     weights.at[k, pl.ds(side * width, width), pl.ds(j * cols, cols)],
                     weight_sems.at[k, side, j],
                 )
-    block_copies = []
-    for k in range(chips):
-        at = pl.multiple_of(leaving[k] * width, width)
-        for j, source in enumerate((mine, theirs)):
-            block_copies.append(
-                fetch(source.at[pl.ds(at, width)], blocks[k].at[j], block_sems.at[k, j])
-            )
     acc = None
     for k in range(chips):
         row_copies[k].wait()
@@ -131,28 +126,45 @@
         acc = part if acc is None else acc + part
     out[core[0]] = acc[:, :cols].astype(out.dtype)
     out[1 - core[0]] = acc[:, cols:].astype(out.dtype)
-    for copy in block_copies:
-        copy.wait()
-
-
-def out_call(block, leaving, core, pieces, mine, theirs):
+
+
+def out_call(block, core, pieces, mine, theirs):
     sides, count, width = pieces[0].shape
     chips, cols = len(pieces), mine.shape[1]
     return pl.pallas_call(
         out_kernel,
         name="expert_out",
-        in_specs=[SCALARS] * 3 + [ANY] * (chips + 2),
-        out_specs=[WHOLE] + [ANY] * chips,
-        out_shape=[jax.ShapeDtypeStruct((2, count, cols), BF)]
-        + [jax.ShapeDtypeStruct((2, width, cols), BF)] * chips,
+        in_specs=[SCALARS, SCALARS] + [ANY] * (chips + 2),
+        out_specs=WHOLE,
+        out_shape=jax.ShapeDtypeStruct((2, count, cols), BF),
         scratch_shapes=[
             pltpu.VMEM((chips, sides, count, width), BF),
             pltpu.VMEM((chips, sides * width, 2 * cols), BF),
             pltpu.SemaphoreType.DMA((chips,)),
             pltpu.SemaphoreType.DMA((chips, 2, 2)),
-            pltpu.SemaphoreType.DMA((chips, 2)),
         ],
-    )(block, leaving, core, *pieces, mine, theirs)
+        compiler_params=pltpu.CompilerParams(vmem_limit_bytes=20 * 1024 * 1024),
+    )(block, core, *pieces, mine, theirs)
+
+
+def cut_kernel(leaving, mine, theirs, *outs):
+    width = outs[0].shape[1]
+    for k, out in enumerate(outs):
+        at = pl.multiple_of(leaving[k] * width, width)
+        out[0] = mine[pl.ds(at, width), :]
+        out[1] = theirs[pl.ds(at, width), :]
+
+
+def cut_call(leaving, mine, theirs, width):
+    count = leaving.shape[0]
+    return pl.pallas_call(
+        cut_kernel,
+        name="cut",
+        in_specs=[SCALARS, WHOLE, WHOLE],
+        out_specs=[WHOLE] * count,
+        out_shape=[jax.ShapeDtypeStruct((2, width, mine.shape[1]), BF)] * count,
+        compiler_params=pltpu.CompilerParams(vmem_limit_bytes=12 * 1024 * 1024),
+    )(leaving, mine, theirs)
 
 
 def place_kernel(chip, core, *refs):
@@ -194,10 +206,6 @@
     return [shift(value, by) if by else value for by in offsets]
 
 
-def spread_each(values):
-    return [shift(value, by) if by else value for by, value in enumerate(values)]
-
-
 def exchange(value, axes):
     return lax.all_to_all(value, axes, split_axis=0, concat_axis=0, tiled=True)
 
@@ -220,7 +228,6 @@
     chip, core = lax.axis_index("x"), lax.axis_index("c")
     offsets = [0, 1, chips - 1] + list(range(2, chips - 1))
     senders = [(chip - by) % chips for by in offsets]
-    sender = jnp.stack(senders).astype(jnp.int32)
     units = jnp.stack([2 * at + side for at in senders for side in (core, 1 - core)])
     units = units.astype(jnp.int32)
     core_id = core.reshape(1).astype(jnp.int32)
@@ -235,22 +242,29 @@
     slot_first = jnp.sum(jnp.where(first, earlier, 0.0), axis=1).astype(jnp.int32)
     slot_second = jnp.sum(jnp.where(second, earlier, 0.0), axis=1).astype(jnp.int32)
 
-    def row_of(expert, slot):
-        return slot // HALF * half_all + expert * HALF + slot % HALF
-
-    target_first = row_of(routes[:, 0], slot_first)
-    target_second = row_of(routes[:, 1], slot_second)
     slot_ids = jnp.arange(slots_all, dtype=jnp.int32)[None, :]
-    is_first = target_first[:, None] == slot_ids
-    is_second = target_second[:, None] == slot_ids
+
+    def picks(place):
+        at_first = place(routes[:, 0], slot_first)[:, None] == slot_ids
+        return at_first, place(routes[:, 1], slot_second)[:, None] == slot_ids
+
+    is_first, is_second = picks(lambda expert, slot: expert * SLOTS + slot)
+    outbound = jnp.einsum(
+        "ts,td->sd", (is_first | is_second).astype(BF), prompt, preferred_element_type=F32
+    ).astype(BF)
+    moved = exchange(outbound.reshape(experts, SLOTS, width), "fs")
+    halves = moved.reshape(experts, 2, HALF, width)
+    mine, theirs = (
+        lax.dynamic_slice_in_dim(halves, at, 1, 1).reshape(half_all, width)
+        for at in (core, 1 - core)
+    )
+    arrived = spread(jnp.stack([mine, swap(theirs)]), offsets)
+    is_first, is_second = picks(
+        lambda expert, slot: slot // HALF * half_all + expert * HALF + slot % HALF
+    )
     weighted = jnp.where(
         is_first, route_weight[:, 0:1], jnp.where(is_second, route_weight[:, 1:2], 0.0)
     ).astype(BF)
-    outbound = jnp.einsum(
-        "ts,td->sd", (is_first | is_second).astype(BF), prompt, preferred_element_type=F32
-    ).astype(BF)
-    moved = exchange(outbound.reshape(2 * experts, HALF, width), ("c", "fs"))
-    arrived = spread(moved.reshape(2, half_all, width), offsets)
     scale = row_scale(arrived)
 
     gain = norm_gain[None, :, None]
@@ -270,16 +284,17 @@
     down = down.reshape(-1, cols)
     down_other = swap(down)
 
-    hidden = hidden_call(sender, arrived, scale, gate_up, gate_up_other)
+    hidden = hidden_call(units, arrived, scale, gate_up, gate_up_other)
     hidden_all = spread(hidden, offsets)
     leaving = jnp.stack([2 * ((chip + by) % chips) + core for by in range(chips)])
-    summed, *blocks = out_call(
-        units, leaving.astype(jnp.int32), core_id, hidden_all, down, down_other
-    )
+    blocks = list(cut_call(leaving.astype(jnp.int32), down, down_other, cols))
+    far = chips // 2
+    blocks[far] = shift(blocks[far], far)
+    summed = out_call(units, core_id, hidden_all, down, down_other)
 
     returned = exchange(summed.reshape(2 * experts, HALF, width), ("c", "fs"))
     returned = returned.reshape(slots_all, width)
-    pieces = spread_each(blocks)
+    pieces = [shift(value, by) if by not in (0, far) else value for by, value in enumerate(blocks)]
     places = jnp.stack([(chip - by) % chips for by in range(chips)]).astype(jnp.int32)
     down_new = place_call(places, core_id, pieces)
 

time: 254 us -> 225 us (0.89)
  the two profiles are of different devices: /device:TPU:8 before, /device:TPU:15 now
where the time goes in v6:
time: 225 us; the launch traced here: 224 us
  waiting for transfers between devices  109 us (48%)
  starting transfers between devices  84.6 us (38%)
  Pallas kernels  14.9 us (7%)
  local copies, waits for them, and re-layouts  7.99 us (4%)
  other arithmetic  3.96 us (2%)
  matrix products  2.91 us (1%)
    all_to_all x4, waiting for transfers between devices, exchange(): return lax.all_to_all(value, axes, split_axis=0, concat_axis=0, tiled=True)  69.3 us
    all_to_all x4, starting transfers between devices, exchange(): return lax.all_to_all(value, axes, split_axis=0, concat_axis=0, tiled=True)  43.3 us
    ppermute x9, waiting for transfers between devices, shift(): lax.ppermute(value, 'x', [(i, (i + by) % count) for i in range(count)])  37 us
    ppermute x9, starting transfers between devices, shift(): lax.ppermute(value, 'x', [(i, (i + by) % count) for i in range(count)])  26.6 us
    ppermute x3, starting transfers between devices, swap(): return lax.ppermute(value, 'c', [(0, 1), (1, 0)])  14.7 us
    pallas_call x1, Pallas kernels, hidden_call(): pl.pallas_call(hidden_kernel, name='hidden', in_specs=[SCALARS] + [ANY] *...  7.06 us
  transfers between devices with their start and end apart: 16, of which 11 were waited for; matrix products, arithmetic and copies ran while one was open for 2% of the time, Pallas kernels for 5%

profile of v6, /device:TPU:15, one launch (start us, length us, event | category | flops | bytes accessed | tf_op | source)
XLA Modules:
  0.0 224.1 jit_solution(5978903088440908099)
XLA Ops:
  0.6 0.8 slice_reduce_fusion.3
  1.4 0.2 select_reduce_fusion.1
  1.7 0.8 fusion.21
  2.5 1.5 fusion.3
  4.0 12.6 %all-to-all-start = ((bf16[32,32,256]{2,1,0:T(8,128)(2,1)}), bf16[32,32,256]{2,1,0:T(8,128)(2,1)S(1)}, u32[]{:S(2)}, u32[]{:S(2)}) async-start(bf16[32,32,256]{2,1,0:T(8,128)(2,1)} %bitcast.1), calls=%async_computation | async-start | bytes 1048576 | tf_op jit(solution)/shard_map/all_to_all | solution.py:210
  16.6 1.6 multiply_convert_fusion.1
  18.2 0.1 pad_maximum_fusion
  18.3 14.2 %all-to-all-done = bf16[32,32,256]{2,1,0:T(8,128)(2,1)S(1)} async-done(((bf16[32,32,256]{2,1,0:T(8,128)(2,1)}), bf16[32,32,256]{2,1,0:T(8,128)(2,1)S(1)}, u32[]{:S(2)}, u32[]{:S(2)}) %all-to-all-start) | async-done | bytes 524320 | tf_op jit(solution)/shard_map/all_to_all | solution.py:210
  32.5 1.6 broadcast_in_dim.59
  34.1 10.4 %all-to-all-start.1 = ((bf16[64,32,512]{2,1,0:T(8,128)(2,1)}), bf16[64,32,512]{2,1,0:T(8,128)(2,1)S(1)}, u32[]{:S(2)}, u32[]{:S(2)}) async-start(bf16[64,32,512]{2,1,0:T(8,128)(2,1)} %bitcast.40), calls=%async_computation.1 | async-start | bytes 4194304 | tf_op jit(solution)/shard_map/all_to_all | solution.py:210
  44.5 1.3 convert_element_type.68
  45.8 47.5 %all-to-all-done.1 = bf16[64,32,512]{2,1,0:T(8,128)(2,1)S(1)} async-done(((bf16[64,32,512]{2,1,0:T(8,128)(2,1)}), bf16[64,32,512]{2,1,0:T(8,128)(2,1)S(1)}, u32[]{:S(2)}, u32[]{:S(2)}) %all-to-all-start.1) | async-done | bytes 2097184 | tf_op jit(solution)/shard_map/all_to_all | solution.py:210
  93.3 1.2 broadcast_in_dim.63
  94.5 0.5 copy-done.6
  95.0 8.7 %all-to-all-start.2 = ((bf16[64,32,256]{2,1,0:T(8,128)(2,1)}), bf16[64,32,256]{2,1,0:T(8,128)(2,1)S(1)}, u32[]{:S(2)}, u32[]{:S(2)}) async-start(bf16[64,32,256]{2,1,0:T(8,128)(2,1)} %bitcast.14), calls=%async_computation.2 | async-start | bytes 2097152 | tf_op jit(solution)/shard_map/all_to_all | solution.py:210
  103.6 5.5 %collective-permute-start.8 = (bf16[2048,512]{1,0:T(8,128)(2,1)}, bf16[2048,512]{1,0:T(8,128)(2,1)}, u32[]{:S(2)}, u32[]{:S(2)}) collective-permute-start(bf16[2048,512]{1,0:T(8,128)(2,1)} %bitcast.37), channel_id=1, source_target_pairs={{0,1},{1,0},{2,3},{3,2},{4,5},{5,4},{6,7},{7,6},{8,9},{9,8},{10,11... | collective-permute-start | bytes 6291464 | tf_op jit(solution)/shard_map/ppermute | solution.py:202
  109.2 1.9 collective-permute-start.4
  111.1 2.4 %collective-permute-done.4 = bf16[512,256]{1,0:T(8,128)(2,1)S(1)} collective-permute-done((bf16[512,256]{1,0:T(8,128)(2,1)S(1)}, bf16[512,256]{1,0:T(8,128)(2,1)S(1)}, u32[]{:S(2)}, u32[]{:S(2)}) %collective-permute-start.4) | collective-permute-done | bytes 262176 | tf_op jit(solution)/shard_map/ppermute | solution.py:202
  113.6 2.2 collective-permute-start.5
  115.7 3.1 %collective-permute-start.6 = (bf16[2,512,256]{2,1,0:T(8,128)(2,1)S(1)}, bf16[2,512,256]{2,1,0:T(8,128)(2,1)}, u32[]{:S(2)}, u32[]{:S(2)}) collective-permute-start(bf16[2,512,256]{2,1,0:T(8,128)(2,1)S(1)} %pad_maximum_fusion.1.refs_0_), channel_id=1, source_target_pairs={{0,6},{2,0},{4,2},{6,4},{1,7},{3,1},{5,3},{7,5},{8,14},{10,8},{12,... | collective-permute-start | bytes 1572872 | tf_op jit(solution)/shard_map/ppermute | solution.py:198
  118.9 3.0 %collective-permute-start.7 = (bf16[2,512,256]{2,1,0:T(8,128)(2,1)S(1)}, bf16[2,512,256]{2,1,0:T(8,128)(2,1)}, u32[]{:S(2)}, u32[]{:S(2)}) collective-permute-start(bf16[2,512,256]{2,1,0:T(8,128)(2,1)S(1)} %pad_maximum_fusion.1.refs_0_), channel_id=1, source_target_pairs={{0,4},{2,6},{4,0},{6,2},{1,5},{3,7},{5,1},{7,3},{8,12},{10,14},{12... | collective-permute-start | bytes 1572872 | tf_op jit(solution)/shard_map/ppermute | solution.py:198
  121.9 7.6 %all-to-all-done.2 = bf16[64,32,256]{2,1,0:T(8,128)(2,1)S(1)} async-done(((bf16[64,32,256]{2,1,0:T(8,128)(2,1)}), bf16[64,32,256]{2,1,0:T(8,128)(2,1)S(1)}, u32[]{:S(2)}, u32[]{:S(2)}) %all-to-all-start.2) | async-done | bytes 1048608 | tf_op jit(solution)/shard_map/all_to_all | solution.py:210
  129.5 7.3 %collective-permute-start = (bf16[2048,256]{1,0:T(8,128)(2,1)S(1)}, bf16[2048,256]{1,0:T(8,128)(2,1)S(1)}, u32[]{:S(2)}, u32[]{:S(2)}) collective-permute-start(bf16[2048,256]{1,0:T(8,128)(2,1)S(1)} %bitcast.34), channel_id=1, source_target_pairs={{0,1},{1,0},{2,3},{3,2},{4,5},{5,4},{6,7},{7,6},{8,9},{9,8},{10,11... | collective-permute-start | bytes 3145736 | tf_op jit(solution)/shard_map/ppermute | solution.py:202
  136.8 0.6 stack.78.block
  137.4 5.3 %collective-permute-done.7.refs_3_ = bf16[2,512,256]{2,1,0:T(8,128)(2,1)} collective-permute-done((bf16[2,512,256]{2,1,0:T(8,128)(2,1)S(1)}, bf16[2,512,256]{2,1,0:T(8,128)(2,1)}, u32[]{:S(2)}, u32[]{:S(2)}) %collective-permute-start.7) | collective-permute-done | bytes 524320 | tf_op jit(solution)/shard_map/ppermute | solution.py:198
  142.7 1.8 row_scale.1.refs_4_
  144.5 0.7 copy-done.4
  145.3 7.1 %hidden.1.refs_0_ = bf16[2,512,256]{2,1,0:T(8,128)(2,1)} custom-call(s32[8]{0:T(128)} %stack.78.block, bf16[2,512,256]{2,1,0:T(8,128)(2,1)} %copy-done.1, bf16[2,512,256]{2,1,0:T(8,128)(2,1)} %copy-done.3, bf16[2,512,256]{2,1,0:T(8,128)(2,1)} %collective-permute-done.6.refs_2_, bf16[2,512,256]{2,1,0:T(8,128)(2,1)} %collective-permute-done.7.refs_3_, ...), custom_call_target="tpu_custom_call" | custom-call | tf_op jit(solution)/shard_map/hidden/pallas_call | solution.py:88
  152.3 1.9 collective-permute-start.10
  154.3 3.7 %collective-permute-start.11 = (bf16[2,512,256]{2,1,0:T(8,128)(2,1)}, bf16[2,512,256]{2,1,0:T(8,128)(2,1)S(1)}, u32[]{:S(2)}, u32[]{:S(2)}) collective-permute-start(bf16[2,512,256]{2,1,0:T(8,128)(2,1)} %hidden.1.refs_0_), channel_id=1, source_target_pairs={{0,4},{2,6},{4,0},{6,2},{1,5},{3,7},{5,1},{7,3},{8,12},{10,14},{12... | collective-permute-start | bytes 1572872 | tf_op jit(solution)/shard_map/ppermute | solution.py:198
  158.0 4.0 %collective-permute-start.9 = (bf16[2,512,256]{2,1,0:T(8,128)(2,1)}, bf16[2,512,256]{2,1,0:T(8,128)(2,1)S(1)}, u32[]{:S(2)}, u32[]{:S(2)}) collective-permute-start(bf16[2,512,256]{2,1,0:T(8,128)(2,1)} %hidden.1.refs_0_), channel_id=1, source_target_pairs={{0,2},{2,4},{4,6},{6,0},{1,3},{3,5},{5,7},{7,1},{8,10},{10,12},{12... | collective-permute-start | bytes 1572872 | tf_op jit(solution)/shard_map/ppermute | solution.py:198
  162.0 5.7 %collective-permute-done.10.refs_2_ = bf16[2,512,256]{2,1,0:T(8,128)(2,1)S(1)} collective-permute-done((bf16[2,512,256]{2,1,0:T(8,128)(2,1)}, bf16[2,512,256]{2,1,0:T(8,128)(2,1)S(1)}, u32[]{:S(2)}, u32[]{:S(2)}) %collective-permute-start.10) | collective-permute-done | bytes 524320 | tf_op jit(solution)/shard_map/ppermute | solution.py:198
  167.6 10.7 %collective-permute-done.11.refs_3_ = bf16[2,512,256]{2,1,0:T(8,128)(2,1)S(1)} collective-permute-done((bf16[2,512,256]{2,1,0:T(8,128)(2,1)}, bf16[2,512,256]{2,1,0:T(8,128)(2,1)S(1)}, u32[]{:S(2)}, u32[]{:S(2)}) %collective-permute-start.11) | collective-permute-done | bytes 524320 | tf_op jit(solution)/shard_map/ppermute | solution.py:198
  178.3 4.0 %collective-permute-done.9.refs_1_ = bf16[2,512,256]{2,1,0:T(8,128)(2,1)S(1)} collective-permute-done((bf16[2,512,256]{2,1,0:T(8,128)(2,1)}, bf16[2,512,256]{2,1,0:T(8,128)(2,1)S(1)}, u32[]{:S(2)}, u32[]{:S(2)}) %collective-permute-start.9) | collective-permute-done | bytes 524320 | tf_op jit(solution)/shard_map/ppermute | solution.py:198
  182.3 1.0 copy-done.2
  183.4 3.3 %expert_out.1 = bf16[2,512,256]{2,1,0:T(8,128)(2,1)} custom-call(s32[8]{0:T(128)S(1)} %copy-done.5, s32[1]{0:T(128)} %bitcast.9.core, bf16[2,512,256]{2,1,0:T(8,128)(2,1)S(1)} %copy-done.2, bf16[2,512,256]{2,1,0:T(8,128)(2,1)S(1)} %collective-permute-done.9.refs_1_, bf16[2,512,256]{2,1,0:T(8,128)(2,1)S(1)} %collective-permute-done.10.refs_2_, ...), custom_call_target="tpu_custom_call" | custom-call | tf_op jit(solution)/shard_map/expert_out/pallas_call | solution.py:134
  186.7 11.7 %all-to-all-start.3 = ((bf16[64,16,256]{2,1,0:T(8,128)(2,1)}), bf16[64,16,256]{2,1,0:T(8,128)(2,1)S(1)}, u32[]{:S(2)}, u32[]{:S(2)}) async-start(bf16[64,16,256]{2,1,0:T(8,128)(2,1)} %bitcast.28), calls=%async_computation.3 | async-start | bytes 1048576 | tf_op jit(solution)/shard_map/all_to_all | solution.py:210
  198.5 0.1 pad_add_fusion.1.leaving
  198.5 0.1 pad_add_fusion.chip
  198.6 0.6 cut.1
  199.3 4.3 %collective-permute-start.1 = (bf16[2,256,256]{2,1,0:T(8,128)(2,1)S(1)}, bf16[2,256,256]{2,1,0:T(8,128)(2,1)S(1)}, u32[]{:S(2)}, u32[]{:S(2)}) collective-permute-start(bf16[2,256,256]{2,1,0:T(8,128)(2,1)S(1)} %get-tuple-element.13), channel_id=1, source_target_pairs={{0,2},{2,4},{4,6},{6,0},{1,3},{3,5},{5,7},{7,1},{8,10},{10,12},{12... | collective-permute-start | bytes 786440 | tf_op jit(solution)/shard_map/ppermute | solution.py:198
  203.5 2.5 %collective-permute-start.2 = (bf16[2,256,256]{2,1,0:T(8,128)(2,1)S(1)}, bf16[2,256,256]{2,1,0:T(8,128)(2,1)S(1)}, u32[]{:S(2)}, u32[]{:S(2)}) collective-permute-start(bf16[2,256,256]{2,1,0:T(8,128)(2,1)S(1)} %get-tuple-element.14), channel_id=1, source_target_pairs={{0,4},{2,6},{4,0},{6,2},{1,5},{3,7},{5,1},{7,3},{8,12},{10,14},{12... | collective-permute-start | bytes 786440 | tf_op jit(solution)/shard_map/ppermute | solution.py:198
  206.0 1.9 collective-permute-start.3
  208.0 1.5 slice_bitcast_fusion
  209.5 4.8 %collective-permute-done.2.refs_2_ = bf16[2,256,256]{2,1,0:T(8,128)(2,1)S(1)} collective-permute-done((bf16[2,256,256]{2,1,0:T(8,128)(2,1)S(1)}, bf16[2,256,256]{2,1,0:T(8,128)(2,1)S(1)}, u32[]{:S(2)}, u32[]{:S(2)}) %collective-permute-start.2) | collective-permute-done | bytes 262176 | tf_op jit(solution)/shard_map/ppermute | solution.py:198
  214.3 6.5 %collective-permute-done.3.refs_3_ = bf16[2,256,256]{2,1,0:T(8,128)(2,1)S(1)} collective-permute-done((bf16[2,256,256]{2,1,0:T(8,128)(2,1)S(1)}, bf16[2,256,256]{2,1,0:T(8,128)(2,1)S(1)}, u32[]{:S(2)}, u32[]{:S(2)}) %collective-permute-start.3) | collective-permute-done | bytes 262176 | tf_op jit(solution)/shard_map/ppermute | solution.py:198
  220.8 2.1 place.1
  222.9 1.2 convolution_convert_fusion
  (30 shorter events, 0.3 us)
Async XLA Ops:
  0.6 1.8 copy-start
  2.5 14.1 %copy-start.8 = (f32[32,32,256]{2,1,0:T(8,128)S(1)}, f32[32,32,256]{2,1,0:T(8,128)}, u32[]{:S(2)}) copy-start(f32[32,32,256]{2,1,0:T(8,128)} %param.9) | copy-start | bytes 3145732
  2.5 14.1 %copy-start.10 = (f32[32]{0:T(128)S(1)}, f32[32]{0:T(128)}, u32[]{:S(2)}) copy-start(f32[32]{0:T(128)} %param.8) | copy-start | bytes 388
  4.0 28.5 %all-to-all-start = ((bf16[32,32,256]{2,1,0:T(8,128)(2,1)}), bf16[32,32,256]{2,1,0:T(8,128)(2,1)S(1)}, u32[]{:S(2)}, u32[]{:S(2)}) async-start(bf16[32,32,256]{2,1,0:T(8,128)(2,1)} %bitcast.1), calls=%async_computation | async-start | bytes 1048576 | tf_op jit(solution)/shard_map/all_to_all | solution.py:210
  34.1 59.2 %all-to-all-start.1 = ((bf16[64,32,512]{2,1,0:T(8,128)(2,1)}), bf16[64,32,512]{2,1,0:T(8,128)(2,1)S(1)}, u32[]{:S(2)}, u32[]{:S(2)}) async-start(bf16[64,32,512]{2,1,0:T(8,128)(2,1)} %bitcast.40), calls=%async_computation.1 | async-start | bytes 4194304 | tf_op jit(solution)/shard_map/all_to_all | solution.py:210
  93.3 1.7 copy-start.6
  95.0 34.5 %all-to-all-start.2 = ((bf16[64,32,256]{2,1,0:T(8,128)(2,1)}), bf16[64,32,256]{2,1,0:T(8,128)(2,1)S(1)}, u32[]{:S(2)}, u32[]{:S(2)}) async-start(bf16[64,32,256]{2,1,0:T(8,128)(2,1)} %bitcast.14), calls=%async_computation.2 | async-start | bytes 2097152 | tf_op jit(solution)/shard_map/all_to_all | solution.py:210
  103.6 41.6 %collective-permute-start.8 = (bf16[2048,512]{1,0:T(8,128)(2,1)}, bf16[2048,512]{1,0:T(8,128)(2,1)}, u32[]{:S(2)}, u32[]{:S(2)}) collective-permute-start(bf16[2048,512]{1,0:T(8,128)(2,1)} %bitcast.37), channel_id=1, source_target_pairs={{0,1},{1,0},{2,3},{3,2},{4,5},{5,4},{6,7},{7,6},{8,9},{9,8},{10,11... | collective-permute-start | bytes 6291464 | tf_op jit(solution)/shard_map/ppermute | solution.py:202
  109.2 4.3 %collective-permute-start.4 = (bf16[512,256]{1,0:T(8,128)(2,1)S(1)}, bf16[512,256]{1,0:T(8,128)(2,1)S(1)}, u32[]{:S(2)}, u32[]{:S(2)}) collective-permute-start(bf16[512,256]{1,0:T(8,128)(2,1)S(1)} %bitcast.45), channel_id=1, source_target_pairs={{0,1},{1,0},{2,3},{3,2},{4,5},{5,4},{6,7},{7,6},{8,9},{9,8},{10,11... | collective-permute-start | bytes 786440 | tf_op jit(solution)/shard_map/ppermute | solution.py:202
  113.5 31.7 %copy-start.1 = (bf16[2,512,256]{2,1,0:T(8,128)(2,1)}, bf16[2,512,256]{2,1,0:T(8,128)(2,1)S(1)}, u32[]{:S(2)}) copy-start(bf16[2,512,256]{2,1,0:T(8,128)(2,1)S(1)} %pad_maximum_fusion.1.refs_0_) | copy-start | bytes 1572868
  113.6 23.9 %collective-permute-start.5 = (bf16[2,512,256]{2,1,0:T(8,128)(2,1)S(1)}, bf16[2,512,256]{2,1,0:T(8,128)(2,1)S(1)}, u32[]{:S(2)}, u32[]{:S(2)}) collective-permute-start(bf16[2,512,256]{2,1,0:T(8,128)(2,1)S(1)} %pad_maximum_fusion.1.refs_0_), channel_id=1, source_target_pairs={{0,2},{2,4},{4,6},{6,0},{1,3},{3,5},{5,7},{7,1},{8,10},{10,12},{12... | collective-permute-start | bytes 1572872 | tf_op jit(solution)/shard_map/ppermute | solution.py:198
  115.7 21.7 %collective-permute-start.6 = (bf16[2,512,256]{2,1,0:T(8,128)(2,1)S(1)}, bf16[2,512,256]{2,1,0:T(8,128)(2,1)}, u32[]{:S(2)}, u32[]{:S(2)}) collective-permute-start(bf16[2,512,256]{2,1,0:T(8,128)(2,1)S(1)} %pad_maximum_fusion.1.refs_0_), channel_id=1, source_target_pairs={{0,6},{2,0},{4,2},{6,4},{1,7},{3,1},{5,3},{7,5},{8,14},{10,8},{12,... | collective-permute-start | bytes 1572872 | tf_op jit(solution)/shard_map/ppermute | solution.py:198
  118.9 23.9 %collective-permute-start.7 = (bf16[2,512,256]{2,1,0:T(8,128)(2,1)S(1)}, bf16[2,512,256]{2,1,0:T(8,128)(2,1)}, u32[]{:S(2)}, u32[]{:S(2)}) collective-permute-start(bf16[2,512,256]{2,1,0:T(8,128)(2,1)S(1)} %pad_maximum_fusion.1.refs_0_), channel_id=1, source_target_pairs={{0,4},{2,6},{4,0},{6,2},{1,5},{3,7},{5,1},{7,3},{8,12},{10,14},{12... | collective-permute-start | bytes 1572872 | tf_op jit(solution)/shard_map/ppermute | solution.py:198
  129.5 52.8 %collective-permute-start = (bf16[2048,256]{1,0:T(8,128)(2,1)S(1)}, bf16[2048,256]{1,0:T(8,128)(2,1)S(1)}, u32[]{:S(2)}, u32[]{:S(2)}) collective-permute-start(bf16[2048,256]{1,0:T(8,128)(2,1)S(1)} %bitcast.34), channel_id=1, source_target_pairs={{0,1},{1,0},{2,3},{3,2},{4,5},{5,4},{6,7},{7,6},{8,9},{9,8},{10,11... | collective-permute-start | bytes 3145736 | tf_op jit(solution)/shard_map/ppermute | solution.py:202
  137.4 7.8 %copy-start.3 = (bf16[2,512,256]{2,1,0:T(8,128)(2,1)}, bf16[2,512,256]{2,1,0:T(8,128)(2,1)S(1)}, u32[]{:S(2)}) copy-start(bf16[2,512,256]{2,1,0:T(8,128)(2,1)S(1)} %collective-permute-done.5.refs_1_) | copy-start | bytes 1572868
  144.5 0.7 copy-start.4
  145.3 37.1 %copy-start.5 = (s32[8]{0:T(128)S(1)}, s32[8]{0:T(128)}, u32[]{:S(2)}) copy-start(s32[8]{0:T(128)} %stack.78.block) | copy-start | bytes 100
  152.3 15.3 %collective-permute-start.10 = (bf16[2,512,256]{2,1,0:T(8,128)(2,1)}, bf16[2,512,256]{2,1,0:T(8,128)(2,1)S(1)}, u32[]{:S(2)}, u32[]{:S(2)}) collective-permute-start(bf16[2,512,256]{2,1,0:T(8,128)(2,1)} %hidden.1.refs_0_), channel_id=1, source_target_pairs={{0,6},{2,0},{4,2},{6,4},{1,7},{3,1},{5,3},{7,5},{8,14},{10,8},{12,... | collective-permute-start | bytes 1572872 | tf_op jit(solution)/shard_map/ppermute | solution.py:198
  154.3 24.0 %collective-permute-start.11 = (bf16[2,512,256]{2,1,0:T(8,128)(2,1)}, bf16[2,512,256]{2,1,0:T(8,128)(2,1)S(1)}, u32[]{:S(2)}, u32[]{:S(2)}) collective-permute-start(bf16[2,512,256]{2,1,0:T(8,128)(2,1)} %hidden.1.refs_0_), channel_id=1, source_target_pairs={{0,4},{2,6},{4,0},{6,2},{1,5},{3,7},{5,1},{7,3},{8,12},{10,14},{12... | collective-permute-start | bytes 1572872 | tf_op jit(solution)/shard_map/ppermute | solution.py:198
  158.0 24.3 %collective-permute-start.9 = (bf16[2,512,256]{2,1,0:T(8,128)(2,1)}, bf16[2,512,256]{2,1,0:T(8,128)(2,1)S(1)}, u32[]{:S(2)}, u32[]{:S(2)}) collective-permute-start(bf16[2,512,256]{2,1,0:T(8,128)(2,1)} %hidden.1.refs_0_), channel_id=1, source_target_pairs={{0,2},{2,4},{4,6},{6,0},{1,3},{3,5},{5,7},{7,1},{8,10},{10,12},{12... | collective-permute-start | bytes 1572872 | tf_op jit(solution)/shard_map/ppermute | solution.py:198
  182.3 1.0 copy-start.2
  183.4 15.2 %copy-start.9 = (f32[320,2]{0,1:T(2,128)S(1)}, f32[320,2]{0,1:T(2,128)}, u32[]{:S(2)}) copy-start(f32[320,2]{0,1:T(2,128)} %param.13) | copy-start | bytes 7684
  186.7 36.2 %all-to-all-start.3 = ((bf16[64,16,256]{2,1,0:T(8,128)(2,1)}), bf16[64,16,256]{2,1,0:T(8,128)(2,1)S(1)}, u32[]{:S(2)}, u32[]{:S(2)}) async-start(bf16[64,16,256]{2,1,0:T(8,128)(2,1)} %bitcast.28), calls=%async_computation.3 | async-start | bytes 1048576 | tf_op jit(solution)/shard_map/all_to_all | solution.py:210
  198.4 9.5 %copy-start.7 = (bf16[64,32,512]{2,1,0:T(8,128)(2,1)S(1)}, bf16[64,32,512]{2,1,0:T(8,128)(2,1)}, u32[]{:S(2)}) copy-start(bf16[64,32,512]{2,1,0:T(8,128)(2,1)} %copy-done.6) | copy-start | bytes 6291460
  199.3 10.2 %collective-permute-start.1 = (bf16[2,256,256]{2,1,0:T(8,128)(2,1)S(1)}, bf16[2,256,256]{2,1,0:T(8,128)(2,1)S(1)}, u32[]{:S(2)}, u32[]{:S(2)}) collective-permute-start(bf16[2,256,256]{2,1,0:T(8,128)(2,1)S(1)} %get-tuple-element.13), channel_id=1, source_target_pairs={{0,2},{2,4},{4,6},{6,0},{1,3},{3,5},{5,7},{7,1},{8,10},{10,12},{12... | collective-permute-start | bytes 786440 | tf_op jit(solution)/shard_map/ppermute | solution.py:198
  203.5 10.7 %collective-permute-start.2 = (bf16[2,256,256]{2,1,0:T(8,128)(2,1)S(1)}, bf16[2,256,256]{2,1,0:T(8,128)(2,1)S(1)}, u32[]{:S(2)}, u32[]{:S(2)}) collective-permute-start(bf16[2,256,256]{2,1,0:T(8,128)(2,1)S(1)} %get-tuple-element.14), channel_id=1, source_target_pairs={{0,4},{2,6},{4,0},{6,2},{1,5},{3,7},{5,1},{7,3},{8,12},{10,14},{12... | collective-permute-start | bytes 786440 | tf_op jit(solution)/shard_map/ppermute | solution.py:198
  206.0 14.7 %collective-permute-start.3 = (bf16[2,256,256]{2,1,0:T(8,128)(2,1)S(1)}, bf16[2,256,256]{2,1,0:T(8,128)(2,1)S(1)}, u32[]{:S(2)}, u32[]{:S(2)}) collective-permute-start(bf16[2,256,256]{2,1,0:T(8,128)(2,1)S(1)} %get-tuple-element.15), channel_id=1, source_target_pairs={{0,6},{2,0},{4,2},{6,4},{1,7},{3,1},{5,3},{7,5},{8,14},{10,8},{12,... | collective-permute-start | bytes 786440 | tf_op jit(solution)/shard_map/ppermute | solution.py:198

commit v7 on v6

--- a/solution.py
+++ b/solution.py
@@ -286,15 +286,20 @@
 
     hidden = hidden_call(units, arrived, scale, gate_up, gate_up_other)
     hidden_all = spread(hidden, offsets)
-    leaving = jnp.stack([2 * ((chip + by) % chips) + core for by in range(chips)])
-    blocks = list(cut_call(leaving.astype(jnp.int32), down, down_other, cols))
     far = chips // 2
+    near = [by for by in range(chips) if by != far]
+    leaving = jnp.stack([2 * ((chip + by) % chips) + core for by in [far, *near]])
+    leaving = leaving.astype(jnp.int32)
+    blocks = {far: cut_call(leaving[:1], down, down_other, cols)[0]}
     blocks[far] = shift(blocks[far], far)
     summed = out_call(units, core_id, hidden_all, down, down_other)
 
     returned = exchange(summed.reshape(2 * experts, HALF, width), ("c", "fs"))
     returned = returned.reshape(slots_all, width)
-    pieces = [shift(value, by) if by not in (0, far) else value for by, value in enumerate(blocks)]
+    cut = cut_call(after(leaving[1:], summed), down, down_other, cols)
+    for by, value in zip(near, cut):
+        blocks[by] = shift(value, by) if by else value
+    pieces = [blocks[by] for by in range(chips)]
     places = jnp.stack([(chip - by) % chips for by in range(chips)]).astype(jnp.int32)
     down_new = place_call(places, core_id, pieces)
 

time: 225 us -> 225 us (level)
  the two profiles are of different devices: /device:TPU:15 before, /device:TPU:8 now
where the time goes in v7:
time: 225 us; the launch traced here: 224 us
  waiting for transfers between devices  112 us (50%)
  starting transfers between devices  81.2 us (36%)
  Pallas kernels  14.9 us (7%)
  local copies, waits for them, and re-layouts  7.99 us (4%)
  other arithmetic  3.95 us (2%)
  matrix products  2.91 us (1%)
    all_to_all x4, waiting for transfers between devices, exchange(): return lax.all_to_all(value, axes, split_axis=0, concat_axis=0, tiled=True)  75.2 us
    all_to_all x4, starting transfers between devices, exchange(): return lax.all_to_all(value, axes, split_axis=0, concat_axis=0, tiled=True)  41.7 us
    ppermute x9, waiting for transfers between devices, shift(): lax.ppermute(value, 'x', [(i, (i + by) % count) for i in range(count)])  34.2 us
    ppermute x9, starting transfers between devices, shift(): lax.ppermute(value, 'x', [(i, (i + by) % count) for i in range(count)])  33.3 us
    pallas_call x1, Pallas kernels, hidden_call(): pl.pallas_call(hidden_kernel, name='hidden', in_specs=[SCALARS] + [ANY] *...  7.05 us
    ppermute x3, starting transfers between devices, swap(): return lax.ppermute(value, 'c', [(0, 1), (1, 0)])  6.24 us
  transfers between devices with their start and end apart: 16, of which 9 were waited for; matrix products, arithmetic and copies ran while one was open for 2% of the time, Pallas kernels for 5%

profile of v7, /device:TPU:8, one launch (start us, length us, event | category | flops | bytes accessed | tf_op | source)
XLA Modules:
  0.0 223.8 jit_solution(1739113836985132274)
XLA Ops:
  0.6 0.8 slice_reduce_fusion.3
  1.4 0.2 select_reduce_fusion.1
  1.7 0.8 fusion.21
  2.5 1.5 fusion.3
  4.0 13.1 %all-to-all-start = ((bf16[32,32,256]{2,1,0:T(8,128)(2,1)}), bf16[32,32,256]{2,1,0:T(8,128)(2,1)S(1)}, u32[]{:S(2)}, u32[]{:S(2)}) async-start(bf16[32,32,256]{2,1,0:T(8,128)(2,1)} %bitcast.1), calls=%async_computation | async-start | bytes 1048576 | tf_op jit(solution)/shard_map/all_to_all | solution.py:210
  17.2 1.6 multiply_convert_fusion.1
  18.7 0.1 pad_maximum_fusion
  18.8 15.8 %all-to-all-done = bf16[32,32,256]{2,1,0:T(8,128)(2,1)S(1)} async-done(((bf16[32,32,256]{2,1,0:T(8,128)(2,1)}), bf16[32,32,256]{2,1,0:T(8,128)(2,1)S(1)}, u32[]{:S(2)}, u32[]{:S(2)}) %all-to-all-start) | async-done | bytes 524320 | tf_op jit(solution)/shard_map/all_to_all | solution.py:210
  34.7 1.6 broadcast_in_dim.59
  36.3 10.3 %all-to-all-start.1 = ((bf16[64,32,512]{2,1,0:T(8,128)(2,1)}), bf16[64,32,512]{2,1,0:T(8,128)(2,1)S(1)}, u32[]{:S(2)}, u32[]{:S(2)}) async-start(bf16[64,32,512]{2,1,0:T(8,128)(2,1)} %bitcast.41), calls=%async_computation.1 | async-start | bytes 4194304 | tf_op jit(solution)/shard_map/all_to_all | solution.py:210
  46.6 1.3 convert_element_type.68
  47.9 49.3 %all-to-all-done.1 = bf16[64,32,512]{2,1,0:T(8,128)(2,1)S(1)} async-done(((bf16[64,32,512]{2,1,0:T(8,128)(2,1)}), bf16[64,32,512]{2,1,0:T(8,128)(2,1)S(1)}, u32[]{:S(2)}, u32[]{:S(2)}) %all-to-all-start.1) | async-done | bytes 2097184 | tf_op jit(solution)/shard_map/all_to_all | solution.py:210
  97.2 1.2 broadcast_in_dim.63
  98.4 0.5 copy-done.6
  98.9 7.7 %all-to-all-start.2 = ((bf16[64,32,256]{2,1,0:T(8,128)(2,1)}), bf16[64,32,256]{2,1,0:T(8,128)(2,1)S(1)}, u32[]{:S(2)}, u32[]{:S(2)}) async-start(bf16[64,32,256]{2,1,0:T(8,128)(2,1)} %bitcast.24), calls=%async_computation.2 | async-start | bytes 2097152 | tf_op jit(solution)/shard_map/all_to_all | solution.py:210
  106.6 1.9 collective-permute-start.4
  108.6 2.4 %collective-permute-start = (bf16[512,256]{1,0:T(8,128)(2,1)S(1)}, bf16[512,256]{1,0:T(8,128)(2,1)S(1)}, u32[]{:S(2)}, u32[]{:S(2)}) collective-permute-start(bf16[512,256]{1,0:T(8,128)(2,1)S(1)} %bitcast.46), channel_id=1, source_target_pairs={{0,1},{1,0},{2,3},{3,2},{4,5},{5,4},{6,7},{7,6},{8,9},{9,8},{10,11... | collective-permute-start | bytes 786440 | tf_op jit(solution)/shard_map/ppermute | solution.py:202
  111.0 2.2 %collective-permute-done = bf16[512,256]{1,0:T(8,128)(2,1)S(1)} collective-permute-done((bf16[512,256]{1,0:T(8,128)(2,1)S(1)}, bf16[512,256]{1,0:T(8,128)(2,1)S(1)}, u32[]{:S(2)}, u32[]{:S(2)}) %collective-permute-start) | collective-permute-done | bytes 262176 | tf_op jit(solution)/shard_map/ppermute | solution.py:202
  113.2 0.1 pad_maximum_fusion.1.refs_0_
  113.3 3.3 %collective-permute-start.1 = (bf16[2,512,256]{2,1,0:T(8,128)(2,1)S(1)}, bf16[2,512,256]{2,1,0:T(8,128)(2,1)S(1)}, u32[]{:S(2)}, u32[]{:S(2)}) collective-permute-start(bf16[2,512,256]{2,1,0:T(8,128)(2,1)S(1)} %pad_maximum_fusion.1.refs_0_), channel_id=1, source_target_pairs={{0,2},{2,4},{4,6},{6,0},{1,3},{3,5},{5,7},{7,1},{8,10},{10,12},{12... | collective-permute-start | bytes 1572872 | tf_op jit(solution)/shard_map/ppermute | solution.py:198
  116.7 3.7 %collective-permute-start.2 = (bf16[2,512,256]{2,1,0:T(8,128)(2,1)S(1)}, bf16[2,512,256]{2,1,0:T(8,128)(2,1)}, u32[]{:S(2)}, u32[]{:S(2)}) collective-permute-start(bf16[2,512,256]{2,1,0:T(8,128)(2,1)S(1)} %pad_maximum_fusion.1.refs_0_), channel_id=1, source_target_pairs={{0,6},{2,0},{4,2},{6,4},{1,7},{3,1},{5,3},{7,5},{8,14},{10,8},{12,... | collective-permute-start | bytes 1572872 | tf_op jit(solution)/shard_map/ppermute | solution.py:198
  120.4 3.7 %collective-permute-start.3 = (bf16[2,512,256]{2,1,0:T(8,128)(2,1)S(1)}, bf16[2,512,256]{2,1,0:T(8,128)(2,1)}, u32[]{:S(2)}, u32[]{:S(2)}) collective-permute-start(bf16[2,512,256]{2,1,0:T(8,128)(2,1)S(1)} %pad_maximum_fusion.1.refs_0_), channel_id=1, source_target_pairs={{0,4},{2,6},{4,0},{6,2},{1,5},{3,7},{5,1},{7,3},{8,12},{10,14},{12... | collective-permute-start | bytes 1572872 | tf_op jit(solution)/shard_map/ppermute | solution.py:198
  124.1 10.1 %all-to-all-done.2 = bf16[64,32,256]{2,1,0:T(8,128)(2,1)S(1)} async-done(((bf16[64,32,256]{2,1,0:T(8,128)(2,1)}), bf16[64,32,256]{2,1,0:T(8,128)(2,1)S(1)}, u32[]{:S(2)}, u32[]{:S(2)}) %all-to-all-start.2) | async-done | bytes 1048608 | tf_op jit(solution)/shard_map/all_to_all | solution.py:210
  134.1 1.9 collective-permute-start.8
  136.1 0.6 stack.77.block
  136.8 6.1 %collective-permute-done.2.refs_2_ = bf16[2,512,256]{2,1,0:T(8,128)(2,1)} collective-permute-done((bf16[2,512,256]{2,1,0:T(8,128)(2,1)S(1)}, bf16[2,512,256]{2,1,0:T(8,128)(2,1)}, u32[]{:S(2)}, u32[]{:S(2)}) %collective-permute-start.2) | collective-permute-done | bytes 524320 | tf_op jit(solution)/shard_map/ppermute | solution.py:198
  142.8 1.8 row_scale.1.refs_4_
  144.7 0.7 copy-done.4
  145.4 7.1 %hidden.1.refs_0_ = bf16[2,512,256]{2,1,0:T(8,128)(2,1)} custom-call(s32[8]{0:T(128)} %stack.77.block, bf16[2,512,256]{2,1,0:T(8,128)(2,1)} %copy-done.1, bf16[2,512,256]{2,1,0:T(8,128)(2,1)} %copy-done.3, bf16[2,512,256]{2,1,0:T(8,128)(2,1)} %collective-permute-done.2.refs_2_, bf16[2,512,256]{2,1,0:T(8,128)(2,1)} %collective-permute-done.3.refs_3_, ...), custom_call_target="tpu_custom_call" | custom-call | tf_op jit(solution)/shard_map/hidden/pallas_call | solution.py:88
  152.5 4.8 %collective-permute-start.5 = (bf16[2,512,256]{2,1,0:T(8,128)(2,1)}, bf16[2,512,256]{2,1,0:T(8,128)(2,1)S(1)}, u32[]{:S(2)}, u32[]{:S(2)}) collective-permute-start(bf16[2,512,256]{2,1,0:T(8,128)(2,1)} %hidden.1.refs_0_), channel_id=1, source_target_pairs={{0,2},{2,4},{4,6},{6,0},{1,3},{3,5},{5,7},{7,1},{8,10},{10,12},{12... | collective-permute-start | bytes 1572872 | tf_op jit(solution)/shard_map/ppermute | solution.py:198
  157.3 2.8 %collective-permute-start.6 = (bf16[2,512,256]{2,1,0:T(8,128)(2,1)}, bf16[2,512,256]{2,1,0:T(8,128)(2,1)S(1)}, u32[]{:S(2)}, u32[]{:S(2)}) collective-permute-start(bf16[2,512,256]{2,1,0:T(8,128)(2,1)} %hidden.1.refs_0_), channel_id=1, source_target_pairs={{0,6},{2,0},{4,2},{6,4},{1,7},{3,1},{5,3},{7,5},{8,14},{10,8},{12,... | collective-permute-start | bytes 1572872 | tf_op jit(solution)/shard_map/ppermute | solution.py:198
  160.1 3.4 %collective-permute-start.7 = (bf16[2,512,256]{2,1,0:T(8,128)(2,1)}, bf16[2,512,256]{2,1,0:T(8,128)(2,1)S(1)}, u32[]{:S(2)}, u32[]{:S(2)}) collective-permute-start(bf16[2,512,256]{2,1,0:T(8,128)(2,1)} %hidden.1.refs_0_), channel_id=1, source_target_pairs={{0,4},{2,6},{4,0},{6,2},{1,5},{3,7},{5,1},{7,3},{8,12},{10,14},{12... | collective-permute-start | bytes 1572872 | tf_op jit(solution)/shard_map/ppermute | solution.py:198
  163.5 6.8 %collective-permute-done.5.refs_1_ = bf16[2,512,256]{2,1,0:T(8,128)(2,1)S(1)} collective-permute-done((bf16[2,512,256]{2,1,0:T(8,128)(2,1)}, bf16[2,512,256]{2,1,0:T(8,128)(2,1)S(1)}, u32[]{:S(2)}, u32[]{:S(2)}) %collective-permute-start.5) | collective-permute-done | bytes 524320 | tf_op jit(solution)/shard_map/ppermute | solution.py:198
  170.2 3.9 %collective-permute-done.6.refs_2_ = bf16[2,512,256]{2,1,0:T(8,128)(2,1)S(1)} collective-permute-done((bf16[2,512,256]{2,1,0:T(8,128)(2,1)}, bf16[2,512,256]{2,1,0:T(8,128)(2,1)S(1)}, u32[]{:S(2)}, u32[]{:S(2)}) %collective-permute-start.6) | collective-permute-done | bytes 524320 | tf_op jit(solution)/shard_map/ppermute | solution.py:198
  174.2 7.4 %collective-permute-done.7.refs_3_ = bf16[2,512,256]{2,1,0:T(8,128)(2,1)S(1)} collective-permute-done((bf16[2,512,256]{2,1,0:T(8,128)(2,1)}, bf16[2,512,256]{2,1,0:T(8,128)(2,1)S(1)}, u32[]{:S(2)}, u32[]{:S(2)}) %collective-permute-start.7) | collective-permute-done | bytes 524320 | tf_op jit(solution)/shard_map/ppermute | solution.py:198
  181.5 1.0 copy-done.2
  182.6 3.3 %expert_out.1 = bf16[2,512,256]{2,1,0:T(8,128)(2,1)} custom-call(s32[8]{0:T(128)S(1)} %copy-done.5, s32[1]{0:T(128)} %bitcast.9.core, bf16[2,512,256]{2,1,0:T(8,128)(2,1)S(1)} %copy-done.2, bf16[2,512,256]{2,1,0:T(8,128)(2,1)S(1)} %collective-permute-done.5.refs_1_, bf16[2,512,256]{2,1,0:T(8,128)(2,1)S(1)} %collective-permute-done.6.refs_2_, ...), custom_call_target="tpu_custom_call" | custom-call | tf_op jit(solution)/shard_map/expert_out/pallas_call | solution.py:134
  185.9 10.5 %all-to-all-start.3 = ((bf16[64,16,256]{2,1,0:T(8,128)(2,1)}), bf16[64,16,256]{2,1,0:T(8,128)(2,1)S(1)}, u32[]{:S(2)}, u32[]{:S(2)}) async-start(bf16[64,16,256]{2,1,0:T(8,128)(2,1)} %bitcast.28), calls=%async_computation.3 | async-start | bytes 1048576 | tf_op jit(solution)/shard_map/all_to_all | solution.py:210
  196.5 0.1 pad_add_fusion.1.leaving
  196.6 0.1 pad_add_fusion.chip
  196.7 0.6 cut.2
  197.3 6.3 %collective-permute-start.11 = (bf16[2,256,256]{2,1,0:T(8,128)(2,1)S(1)}, bf16[2,256,256]{2,1,0:T(8,128)(2,1)S(1)}, u32[]{:S(2)}, u32[]{:S(2)}) collective-permute-start(bf16[2,256,256]{2,1,0:T(8,128)(2,1)S(1)} %get-tuple-element.15), channel_id=1, source_target_pairs={{0,6},{2,0},{4,2},{6,4},{1,7},{3,1},{5,3},{7,5},{8,14},{10,8},{12,... | collective-permute-start | bytes 786440 | tf_op jit(solution)/shard_map/ppermute | solution.py:198
  203.6 1.9 collective-permute-start.9
  205.6 3.4 %collective-permute-start.10 = (bf16[2,256,256]{2,1,0:T(8,128)(2,1)S(1)}, bf16[2,256,256]{2,1,0:T(8,128)(2,1)S(1)}, u32[]{:S(2)}, u32[]{:S(2)}) collective-permute-start(bf16[2,256,256]{2,1,0:T(8,128)(2,1)S(1)} %cut.3), channel_id=1, source_target_pairs={{0,4},{2,6},{4,0},{6,2},{1,5},{3,7},{5,1},{7,3},{8,12},{10,14},{12... | collective-permute-start | bytes 786440 | tf_op jit(solution)/shard_map/ppermute | solution.py:198
  209.0 1.5 slice_bitcast_fusion
  210.4 10.1 %collective-permute-done.9.refs_1_ = bf16[2,256,256]{2,1,0:T(8,128)(2,1)S(1)} collective-permute-done((bf16[2,256,256]{2,1,0:T(8,128)(2,1)S(1)}, bf16[2,256,256]{2,1,0:T(8,128)(2,1)S(1)}, u32[]{:S(2)}, u32[]{:S(2)}) %collective-permute-start.9) | collective-permute-done | bytes 262176 | tf_op jit(solution)/shard_map/ppermute | solution.py:198
  220.5 2.1 place.1
  222.6 1.2 convolution_convert_fusion
  (31 shorter events, 0.2 us)
Async XLA Ops:
  0.6 1.8 copy-start
  2.5 14.7 %copy-start.8 = (f32[32,32,256]{2,1,0:T(8,128)S(1)}, f32[32,32,256]{2,1,0:T(8,128)}, u32[]{:S(2)}) copy-start(f32[32,32,256]{2,1,0:T(8,128)} %param.9) | copy-start | bytes 3145732
  2.5 14.7 %copy-start.10 = (f32[32]{0:T(128)S(1)}, f32[32]{0:T(128)}, u32[]{:S(2)}) copy-start(f32[32]{0:T(128)} %param.8) | copy-start | bytes 388
  4.0 30.6 %all-to-all-start = ((bf16[32,32,256]{2,1,0:T(8,128)(2,1)}), bf16[32,32,256]{2,1,0:T(8,128)(2,1)S(1)}, u32[]{:S(2)}, u32[]{:S(2)}) async-start(bf16[32,32,256]{2,1,0:T(8,128)(2,1)} %bitcast.1), calls=%async_computation | async-start | bytes 1048576 | tf_op jit(solution)/shard_map/all_to_all | solution.py:210
  36.3 60.9 %all-to-all-start.1 = ((bf16[64,32,512]{2,1,0:T(8,128)(2,1)}), bf16[64,32,512]{2,1,0:T(8,128)(2,1)S(1)}, u32[]{:S(2)}, u32[]{:S(2)}) async-start(bf16[64,32,512]{2,1,0:T(8,128)(2,1)} %bitcast.41), calls=%async_computation.1 | async-start | bytes 4194304 | tf_op jit(solution)/shard_map/all_to_all | solution.py:210
  97.2 1.7 copy-start.6
  98.9 35.3 %all-to-all-start.2 = ((bf16[64,32,256]{2,1,0:T(8,128)(2,1)}), bf16[64,32,256]{2,1,0:T(8,128)(2,1)S(1)}, u32[]{:S(2)}, u32[]{:S(2)}) async-start(bf16[64,32,256]{2,1,0:T(8,128)(2,1)} %bitcast.24), calls=%async_computation.2 | async-start | bytes 2097152 | tf_op jit(solution)/shard_map/all_to_all | solution.py:210
  106.6 38.8 %collective-permute-start.4 = (bf16[2048,512]{1,0:T(8,128)(2,1)}, bf16[2048,512]{1,0:T(8,128)(2,1)}, u32[]{:S(2)}, u32[]{:S(2)}) collective-permute-start(bf16[2048,512]{1,0:T(8,128)(2,1)} %bitcast.38), channel_id=1, source_target_pairs={{0,1},{1,0},{2,3},{3,2},{4,5},{5,4},{6,7},{7,6},{8,9},{9,8},{10,11... | collective-permute-start | bytes 6291464 | tf_op jit(solution)/shard_map/ppermute | solution.py:202
  108.6 4.7 %collective-permute-start = (bf16[512,256]{1,0:T(8,128)(2,1)S(1)}, bf16[512,256]{1,0:T(8,128)(2,1)S(1)}, u32[]{:S(2)}, u32[]{:S(2)}) collective-permute-start(bf16[512,256]{1,0:T(8,128)(2,1)S(1)} %bitcast.46), channel_id=1, source_target_pairs={{0,1},{1,0},{2,3},{3,2},{4,5},{5,4},{6,7},{7,6},{8,9},{9,8},{10,11... | collective-permute-start | bytes 786440 | tf_op jit(solution)/shard_map/ppermute | solution.py:202
  113.3 32.1 %copy-start.1 = (bf16[2,512,256]{2,1,0:T(8,128)(2,1)}, bf16[2,512,256]{2,1,0:T(8,128)(2,1)S(1)}, u32[]{:S(2)}) copy-start(bf16[2,512,256]{2,1,0:T(8,128)(2,1)S(1)} %pad_maximum_fusion.1.refs_0_) | copy-start | bytes 1572868
  113.3 23.4 %collective-permute-start.1 = (bf16[2,512,256]{2,1,0:T(8,128)(2,1)S(1)}, bf16[2,512,256]{2,1,0:T(8,128)(2,1)S(1)}, u32[]{:S(2)}, u32[]{:S(2)}) collective-permute-start(bf16[2,512,256]{2,1,0:T(8,128)(2,1)S(1)} %pad_maximum_fusion.1.refs_0_), channel_id=1, source_target_pairs={{0,2},{2,4},{4,6},{6,0},{1,3},{3,5},{5,7},{7,1},{8,10},{10,12},{12... | collective-permute-start | bytes 1572872 | tf_op jit(solution)/shard_map/ppermute | solution.py:198
  116.7 26.2 %collective-permute-start.2 = (bf16[2,512,256]{2,1,0:T(8,128)(2,1)S(1)}, bf16[2,512,256]{2,1,0:T(8,128)(2,1)}, u32[]{:S(2)}, u32[]{:S(2)}) collective-permute-start(bf16[2,512,256]{2,1,0:T(8,128)(2,1)S(1)} %pad_maximum_fusion.1.refs_0_), channel_id=1, source_target_pairs={{0,6},{2,0},{4,2},{6,4},{1,7},{3,1},{5,3},{7,5},{8,14},{10,8},{12,... | collective-permute-start | bytes 1572872 | tf_op jit(solution)/shard_map/ppermute | solution.py:198
  120.4 22.5 %collective-permute-start.3 = (bf16[2,512,256]{2,1,0:T(8,128)(2,1)S(1)}, bf16[2,512,256]{2,1,0:T(8,128)(2,1)}, u32[]{:S(2)}, u32[]{:S(2)}) collective-permute-start(bf16[2,512,256]{2,1,0:T(8,128)(2,1)S(1)} %pad_maximum_fusion.1.refs_0_), channel_id=1, source_target_pairs={{0,4},{2,6},{4,0},{6,2},{1,5},{3,7},{5,1},{7,3},{8,12},{10,14},{12... | collective-permute-start | bytes 1572872 | tf_op jit(solution)/shard_map/ppermute | solution.py:198
  134.1 47.4 %collective-permute-start.8 = (bf16[2048,256]{1,0:T(8,128)(2,1)S(1)}, bf16[2048,256]{1,0:T(8,128)(2,1)S(1)}, u32[]{:S(2)}, u32[]{:S(2)}) collective-permute-start(bf16[2048,256]{1,0:T(8,128)(2,1)S(1)} %bitcast.34), channel_id=1, source_target_pairs={{0,1},{1,0},{2,3},{3,2},{4,5},{5,4},{6,7},{7,6},{8,9},{9,8},{10,11... | collective-permute-start | bytes 3145736 | tf_op jit(solution)/shard_map/ppermute | solution.py:202
  136.8 8.6 %copy-start.3 = (bf16[2,512,256]{2,1,0:T(8,128)(2,1)}, bf16[2,512,256]{2,1,0:T(8,128)(2,1)S(1)}, u32[]{:S(2)}) copy-start(bf16[2,512,256]{2,1,0:T(8,128)(2,1)S(1)} %collective-permute-done.1.refs_1_) | copy-start | bytes 1572868
  144.7 0.7 copy-start.4
  145.4 36.2 %copy-start.5 = (s32[8]{0:T(128)S(1)}, s32[8]{0:T(128)}, u32[]{:S(2)}) copy-start(s32[8]{0:T(128)} %stack.77.block) | copy-start | bytes 100
  152.5 17.8 %collective-permute-start.5 = (bf16[2,512,256]{2,1,0:T(8,128)(2,1)}, bf16[2,512,256]{2,1,0:T(8,128)(2,1)S(1)}, u32[]{:S(2)}, u32[]{:S(2)}) collective-permute-start(bf16[2,512,256]{2,1,0:T(8,128)(2,1)} %hidden.1.refs_0_), channel_id=1, source_target_pairs={{0,2},{2,4},{4,6},{6,0},{1,3},{3,5},{5,7},{7,1},{8,10},{10,12},{12... | collective-permute-start | bytes 1572872 | tf_op jit(solution)/shard_map/ppermute | solution.py:198
  157.3 16.9 %collective-permute-start.6 = (bf16[2,512,256]{2,1,0:T(8,128)(2,1)}, bf16[2,512,256]{2,1,0:T(8,128)(2,1)S(1)}, u32[]{:S(2)}, u32[]{:S(2)}) collective-permute-start(bf16[2,512,256]{2,1,0:T(8,128)(2,1)} %hidden.1.refs_0_), channel_id=1, source_target_pairs={{0,6},{2,0},{4,2},{6,4},{1,7},{3,1},{5,3},{7,5},{8,14},{10,8},{12,... | collective-permute-start | bytes 1572872 | tf_op jit(solution)/shard_map/ppermute | solution.py:198
  160.1 21.5 %collective-permute-start.7 = (bf16[2,512,256]{2,1,0:T(8,128)(2,1)}, bf16[2,512,256]{2,1,0:T(8,128)(2,1)S(1)}, u32[]{:S(2)}, u32[]{:S(2)}) collective-permute-start(bf16[2,512,256]{2,1,0:T(8,128)(2,1)} %hidden.1.refs_0_), channel_id=1, source_target_pairs={{0,4},{2,6},{4,0},{6,2},{1,5},{3,7},{5,1},{7,3},{8,12},{10,14},{12... | collective-permute-start | bytes 1572872 | tf_op jit(solution)/shard_map/ppermute | solution.py:198
  181.5 1.0 copy-start.2
  182.6 14.1 %copy-start.9 = (f32[320,2]{0,1:T(2,128)S(1)}, f32[320,2]{0,1:T(2,128)}, u32[]{:S(2)}) copy-start(f32[320,2]{0,1:T(2,128)} %param.13) | copy-start | bytes 7684
  185.9 36.7 %all-to-all-start.3 = ((bf16[64,16,256]{2,1,0:T(8,128)(2,1)}), bf16[64,16,256]{2,1,0:T(8,128)(2,1)S(1)}, u32[]{:S(2)}, u32[]{:S(2)}) async-start(bf16[64,16,256]{2,1,0:T(8,128)(2,1)} %bitcast.28), calls=%async_computation.3 | async-start | bytes 1048576 | tf_op jit(solution)/shard_map/all_to_all | solution.py:210
  197.3 11.7 %copy-start.7 = (bf16[64,32,512]{2,1,0:T(8,128)(2,1)S(1)}, bf16[64,32,512]{2,1,0:T(8,128)(2,1)}, u32[]{:S(2)}) copy-start(bf16[64,32,512]{2,1,0:T(8,128)(2,1)} %copy-done.6) | copy-start | bytes 6291460
  197.3 13.1 %collective-permute-start.11 = (bf16[2,256,256]{2,1,0:T(8,128)(2,1)S(1)}, bf16[2,256,256]{2,1,0:T(8,128)(2,1)S(1)}, u32[]{:S(2)}, u32[]{:S(2)}) collective-permute-start(bf16[2,256,256]{2,1,0:T(8,128)(2,1)S(1)} %get-tuple-element.15), channel_id=1, source_target_pairs={{0,6},{2,0},{4,2},{6,4},{1,7},{3,1},{5,3},{7,5},{8,14},{10,8},{12,... | collective-permute-start | bytes 786440 | tf_op jit(solution)/shard_map/ppermute | solution.py:198
  203.6 16.9 %collective-permute-start.9 = (bf16[2,256,256]{2,1,0:T(8,128)(2,1)S(1)}, bf16[2,256,256]{2,1,0:T(8,128)(2,1)S(1)}, u32[]{:S(2)}, u32[]{:S(2)}) collective-permute-start(bf16[2,256,256]{2,1,0:T(8,128)(2,1)S(1)} %get-tuple-element.14), channel_id=1, source_target_pairs={{0,2},{2,4},{4,6},{6,0},{1,3},{3,5},{5,7},{7,1},{8,10},{10,12},{12... | collective-permute-start | bytes 786440 | tf_op jit(solution)/shard_map/ppermute | solution.py:198
  205.6 14.9 %collective-permute-start.10 = (bf16[2,256,256]{2,1,0:T(8,128)(2,1)S(1)}, bf16[2,256,256]{2,1,0:T(8,128)(2,1)S(1)}, u32[]{:S(2)}, u32[]{:S(2)}) collective-permute-start(bf16[2,256,256]{2,1,0:T(8,128)(2,1)S(1)} %cut.3), channel_id=1, source_target_pairs={{0,4},{2,6},{4,0},{6,2},{1,5},{3,7},{5,1},{7,3},{8,12},{10,14},{12... | collective-permute-start | bytes 786440 | tf_op jit(solution)/shard_map/ppermute | solution.py:198
